TPU v7x, 32 devices: a whole 2x2x4 slice. The times are simulated.
32 devices in a mesh: sp: 4 (over y, x), tp: 8 (over z, core).
Axes of the slice: x: 2, y: 2, z: 4, core: 2. Of those that a mesh axis runs over, the one named last changes fastest.
Arguments:
- queries: bfloat16 [2048, 1536], P('sp', 'tp'), may hold values from -34 to 34
- latent: bfloat16 [2048, 512], P('sp'), may hold values from -6 to 6
- rot_key: bfloat16 [2048, 32], P('sp'), may hold values from -34 to 34
- latent_gain: float32 [512], replicated, may hold values from 0.1 to 1.9
- key_up: bfloat16 [512, 1024], P(None, 'tp'), may hold values from -0.25 to 0.25
- value_up: bfloat16 [512, 1024], P(None, 'tp'), may hold values from -0.70710678 to 0.70710678
- query_gain: float32 [96], replicated, may hold values from 0.5 to 6
- key_gain: float32 [96], replicated, may hold values from 0.5 to 6
- out_gain: float32 [1024], replicated, may hold values from 0.1 to 1.9
- out_weight: bfloat16 [1024, 2048], replicated, may hold values from -0.1875 to 0.1875
- residual: bfloat16 [2048, 2048], P(('sp', 'tp')), may hold values from -6 to 6
- ffn_gain: float32 [2048], replicated, may hold values from 0.1 to 1.9
- routes: int32 [2048, 2], P(('sp', 'tp')), may hold values from 0 to 3, all different within a row; in each aligned block of 64 rows (0 to 63, 64 to 127, ...) at most 36 rows name the same one
- route_weights: float32 [2048, 2], P(('sp', 'tp')), may hold values from 0.2 to 1
- expert_gate: bfloat16 [4, 2048, 2048], P('sp', None, 'tp'), may hold values from -0.125 to 0.125
- expert_up: bfloat16 [4, 2048, 2048], P('sp', None, 'tp'), may hold values from -0.125 to 0.125
- expert_down: bfloat16 [4, 2048, 2048], P('sp', 'tp'), may hold values from -0.125 to 0.125
Outputs:
- layer_out: bfloat16 [2048, 2048], P(('sp', 'tp'))
Inputs may be any that keep to these rules, and one draw needn't show every extreme that they name: `routes`: the 2 experts of a token differ. Among the 64 rows of one device each expert is named by at most 36 rows, a bound that some block reaches.
All inputs are finite; a program needn't handle non-finite values.
Results may differ from a plain program's by a relative error of at most 0.02.
The roundings to bfloat16 on the way count: a program that leaves them out, or rounds other values in their place, can miss the bound.
Values may be sent and summed in bfloat16 or wider, within the bound.
No kernel may reach another device: no remote copies, remote signals or barrier semaphores. Data moves between devices by JAX's collectives and lax.ppermute only.
A program may use at most 128 MiB of HBM per device.

v0:
```python
import functools

import jax
import jax.numpy as jnp
import numpy as np
from jax import lax
from jax.experimental import pallas as pl
from jax.experimental.pallas import tpu as pltpu
from jax.sharding import PartitionSpec as P


NOPE = 64
ROPE = 32
VH = 64
TOPK = 2
QK = 96
LANES = 128
COL_CHUNKS = 2
ROOM = 60


epsilon = 1e-06
rope_base = 10000.0
f32 = jnp.float32
bf16 = jnp.bfloat16


def dot(a, b):
    return jnp.dot(a, b, preferred_element_type=f32)


def rope_select(offset, rows):
    direct = np.zeros((rows, LANES), np.float32)
    turned = np.zeros((rows, LANES), np.float32)
    half = ROPE // 2
    for lane in range(LANES):
        d = lane % ROPE
        direct[offset + d, lane] = 1.0
        turned[offset + (d + half) % ROPE, lane] = -1.0 if d < half else 1.0
    return direct, turned


def head_select(heads):
    parts = []
    for h in range(heads):
        nope = np.zeros((heads * QK, LANES), np.float32)
        for i in range(NOPE):
            nope[h * QK + i, i] = 1.0
        parts += [nope, *rope_select(h * QK + NOPE, heads * QK)]
    return np.concatenate(parts, axis=1)


def turn_tables(rows, blocks):
    inverse = rope_base ** (-np.arange(0, ROPE, 2, dtype=np.float64) / ROPE)
    inverse = np.tile(inverse, 2 * LANES // ROPE)[None, :]
    inner = np.arange(rows, dtype=np.float64)[:, None] * inverse
    first = np.arange(blocks, dtype=np.float64)[:, None] * rows * inverse
    return [
        np.concatenate([np.cos(a), np.sin(a)], axis=1).astype(np.float32) for a in (inner, first)
    ]


def dot_rows(a, b):
    return lax.dot_general(a, b, (((0,), (0,)), ((), ())), preferred_element_type=f32)


def prep_kernel(
    heads, lat, rot, lat_gain, key_up, value_up, queries, q_gain, k_gain, inner, first,
    selq, selk, selg, bundle, q1, q2,
):
    rows = lat.shape[0]
    pack = LANES // (ROPE * heads)
    sub = rows // pack
    me = lax.axis_index("sp")
    x = lat[...].astype(f32)
    scale = lax.rsqrt(jnp.mean(x * x, axis=-1, keepdims=True) + epsilon)
    normed = (x * scale * lat_gain[...]).astype(bf16)
    base = first[pl.ds(me, 1), :]
    base_cos, base_sin = base[:, :LANES], base[:, LANES:]
    in_cos, in_sin = inner[:, :LANES], inner[:, LANES:]
    cos = in_cos * base_cos - in_sin * base_sin
    sin = in_sin * base_cos + in_cos * base_sin
    spread_gain = lambda g: jnp.dot(
        g[...], selg[...], precision=lax.Precision.HIGHEST, preferred_element_type=f32
    )
    gq, gk = spread_gain(q_gain), spread_gain(k_gain)
    cut = lambda g, i: g[:, i * LANES : (i + 1) * LANES]
    lane = lax.broadcasted_iota(jnp.int32, (rows, LANES), 1)
    is_key = lane < NOPE
    turns = dot_rows(rot[...], selk[...])
    rot_a, rot_b = turns[:, :LANES], turns[:, LANES:]
    rot_sq = jnp.sum(rot_a * rot_a, axis=-1, keepdims=True) * (ROPE / LANES)
    spun = rot_a * cut(gk, 1) * cos + rot_b * cut(gk, 2) * sin
    key_scales = None
    for h in range(heads):
        weight = jnp.concatenate(
            [key_up[:, h * NOPE : (h + 1) * NOPE], value_up[:, h * VH : (h + 1) * VH]], axis=1
        )
        kv = dot(normed, weight).astype(bf16).astype(f32)
        sq = jnp.sum(jnp.where(is_key, kv * kv, 0.0), axis=-1, keepdims=True) + rot_sq
        r = lax.rsqrt(sq * (1.0 / QK) + epsilon)
        bundle[h * rows : (h + 1) * rows, :] = jnp.where(
            is_key, kv * r * cut(gk, 0), kv
        ).astype(bf16)
        spread = jnp.broadcast_to(r, (rows, LANES))
        key_scales = (
            spread
            if key_scales is None
            else jnp.where((lane // ROPE) % heads == h, spread, key_scales)
        )
    spun = spun * key_scales
    tile = spun[:sub]
    for p in range(1, pack):
        tile = jnp.where(
            lane[:sub] // (ROPE * heads) == p, spun[p * sub : (p + 1) * sub], tile
        )
    bundle[heads * rows :, :] = tile.astype(bf16)
    picked = dot_rows(queries[...], selq[...])
    for h in range(heads):
        base = h * 3 * LANES
        nope = picked[:, base : base + LANES]
        qa = picked[:, base + LANES : base + 2 * LANES]
        qb = picked[:, base + 2 * LANES : base + 3 * LANES]
        sq = jnp.sum(nope * nope + qa * qa * (ROPE / LANES), axis=-1, keepdims=True)
        r = lax.rsqrt(sq * (1.0 / QK) + epsilon)
        q1[h] = (nope * r * cut(gq, 0)).astype(bf16)
        turned = (qa * cut(gq, 1) * cos + qb * cut(gq, 2) * sin) * r
        for p in range(pack):
            q2[h * pack + p] = jnp.where(lane // ROPE == p * heads + h, turned, 0.0).astype(bf16)


def scores_of(heads, q1, q2, ref, h, top, count, parts):
    rows = q1.shape[1]
    pack = LANES // (ROPE * heads)
    sub = rows // pack
    out = []
    for p in range(parts):
        query = jnp.concatenate(
            [q1[h, top : top + count], q2[h * pack + p, top : top + count]], axis=1
        )
        key = jnp.concatenate(
            [
                ref[h * rows + p * sub : h * rows + (p + 1) * sub, :],
                ref[heads * rows : heads * rows + sub, :],
            ],
            axis=1,
        )
        out.append(
            lax.dot_general(key, query, (((1,), (1,)), ((), ())), preferred_element_type=f32)
        )
    return out[0] if parts == 1 else jnp.concatenate(out, axis=0)


FACTOR = float(QK ** (-0.5) * np.log2(np.e))


def attend_own(heads, q1, q2, ref, state):
    rows = q1.shape[1]
    pack = LANES // (ROPE * heads)
    sub = rows // pack
    for h in range(heads):
        for b in range(pack):
            scores = scores_of(heads, q1, q2, ref, h, b * sub, sub, b + 1)
            key = lax.broadcasted_iota(jnp.int32, scores.shape, 0)
            query = lax.broadcasted_iota(jnp.int32, scores.shape, 1) + b * sub
            scores = jnp.where(key <= query, scores, -1e30)
            peak = jnp.max(scores, axis=0, keepdims=True)
            weights = jnp.exp2((scores - peak) * FACTOR)
            total = jnp.sum(weights, axis=0, keepdims=True)
            part = dot_rows(ref[h * rows : h * rows + (b + 1) * sub, :], weights.astype(bf16))
            row = lax.broadcasted_iota(jnp.int32, part.shape, 0)
            state[h, :, b * sub : (b + 1) * sub] = jnp.where(
                row == 0, peak, jnp.where(row == 1, total, part)
            )


def attend_other(heads, q1, q2, ref, state):
    rows = q1.shape[1]
    pack = LANES // (ROPE * heads)
    for h in range(heads):
        scores = scores_of(heads, q1, q2, ref, h, 0, rows, pack)
        old = state[h, 0:1, :]
        peak = jnp.maximum(old, jnp.max(scores, axis=0, keepdims=True))
        fade = jnp.exp2((old - peak) * FACTOR)
        weights = jnp.exp2((scores - peak) * FACTOR)
        total = state[h, 1:2, :] * fade + jnp.sum(weights, axis=0, keepdims=True)
        part = dot_rows(ref[h * rows : (h + 1) * rows, :], weights.astype(bf16))
        part = part + state[h] * fade
        row = lax.broadcasted_iota(jnp.int32, part.shape, 0)
        state[h] = jnp.where(row == 0, peak, jnp.where(row == 1, total, part))


def attend_first_kernel(heads, sources, q1, q2, *refs):
    bundles, state = refs[: len(sources)], refs[-1]
    me = lax.axis_index("sp")
    attend_own(heads, q1, q2, bundles[0], state)
    for i, k in enumerate(sources):
        if k:

            @pl.when((me ^ k) < me)
            def _():
                attend_other(heads, q1, q2, bundles[i], state)


def attend_last_kernel(heads, tokens, groups, sources, q1, q2, before, *refs):
    bundles = refs[: len(sources)]
    keep, send, state, result = refs[len(sources) :]
    me = lax.axis_index("sp")
    core = lax.axis_index("tp") % 2
    state[...] = before[...]
    for i, k in enumerate(sources):

        @pl.when((me ^ k) < me)
        def _():
            attend_other(heads, q1, q2, bundles[i], state)

    outs = [state[h, NOPE:, :] / state[h, 1:2, :] for h in range(heads)]
    result[...] = (outs[0] if heads == 1 else jnp.concatenate(outs, axis=0)).T
    for g in range(groups):
        at = g * 2 * tokens
        keep[g * tokens : (g + 1) * tokens, :] = result[
            pl.ds(pl.multiple_of(at + core * tokens, tokens), tokens), :
        ].astype(bf16)
        send[g * tokens : (g + 1) * tokens, :] = result[
            pl.ds(pl.multiple_of(at + (1 - core) * tokens, tokens), tokens), :
        ].astype(bf16)


def pack_kernel(routes, weights, residual, flags, first, second):
    half = second.shape[1]
    rows = [routes[...].astype(f32)]
    for j in range(TOPK):
        rest = weights[j : j + 1, :]
        for _ in range(3):
            piece = rest.astype(bf16).astype(f32)
            rows.append(piece)
            rest = rest - piece
    stacked = jnp.concatenate(rows, axis=0)
    first[:, :half] = residual[:, :half]
    first[:, half:] = dot_rows(stacked.astype(bf16), flags[...]).astype(bf16)
    second[...] = residual[:, half:]


def residual_first_kernel(groups, sp, cap, lower, *refs):
    parts = refs[:groups]
    table, outs, everything = refs[groups], refs[groups + 1 : -1], refs[-1]
    tokens, width = parts[0].shape
    half = width - LANES
    slots = outs[0].shape[0]
    me = lax.axis_index("sp")
    z = lax.axis_index("tp") // 2
    for g in range(groups):
        everything[g * tokens : (g + 1) * tokens, :] = parts[g][...]
    ticket = everything[:, half:].astype(f32)
    lane = lax.broadcasted_iota(jnp.int32, ticket.shape, 1)
    row = lax.broadcasted_iota(jnp.int32, ticket.shape, 0)
    route = [ticket[:, j : j + 1].astype(jnp.int32) for j in range(TOPK)]
    named = me ^ lane
    hit = ((route[0] == named) | (route[1] == named)) & (lane < sp)
    rank = dot(lower[...], hit.astype(f32).astype(bf16)).astype(jnp.int32)
    slot = jnp.where(hit, rank + (z ^ (row // tokens)) * cap, -1)
    named = me ^ (lane // 3)
    tail = jnp.zeros(ticket.shape, f32)
    for j in range(TOPK):
        at = TOPK + 3 * j
        piece = jnp.where(
            lane % 3 == 0,
            ticket[:, at : at + 1],
            jnp.where(lane % 3 == 1, ticket[:, at + 1 : at + 2], ticket[:, at + 2 : at + 3]),
        )
        tail = tail + jnp.where((route[j] == named) & (lane < 3 * sp), piece, 0.0)
    everything[:, half:] = tail.astype(bf16)
    place = lax.broadcasted_iota(jnp.int32, (groups * tokens, slots), 1)
    for k, out in enumerate(outs):
        chosen = (slot[:, k : k + 1] == place).astype(f32).astype(bf16)
        table[k] = chosen
        out[...] = dot_rows(chosen, everything[...]).astype(bf16)


def residual_second_kernel(groups, table, *refs):
    parts = refs[:groups]
    outs, everything = refs[groups:-1], refs[-1]
    tokens = parts[0].shape[0]
    for g in range(groups):
        everything[g * tokens : (g + 1) * tokens, :] = parts[g][...]
    for k, out in enumerate(outs):
        out[...] = dot_rows(table[k], everything[...]).astype(bf16)


def choose_kernel(groups, tokens, gain, table, *refs):
    pieces = refs[: 2 * groups]
    outs = refs[2 * groups : -3]
    own, rows_ref, normed_ref = refs[-3:]
    place = lax.axis_index("tp")
    z, core = place // 2, place % 2
    width = 2 * pieces[0].shape[1]
    for g in range(groups):
        mine, other = pieces[2 * g][...].astype(f32), pieces[2 * g + 1][...].astype(f32)
        first = jnp.where(core == 0, mine, other)
        second = jnp.where(core == 0, other, mine)
        at = pl.multiple_of((z ^ g) * width, width)
        rows_ref[:, pl.ds(at, width)] = jnp.concatenate([first, second], axis=1)
    x = rows_ref[...]
    scale = lax.rsqrt(jnp.mean(x * x, axis=-1, keepdims=True) + epsilon)
    normed_ref[...] = (x * scale * gain[...]).astype(bf16)
    blocks = [
        normed_ref[pl.ds(pl.multiple_of((z ^ g) * tokens, tokens), tokens), :]
        for g in range(groups)
    ]
    own[...] = blocks[0]
    near = jnp.concatenate(blocks, axis=0)
    for k, out in enumerate(outs):
        out[...] = dot_rows(table[k], near).astype(bf16)


def expert_kernel(
    part, chunks, own, out_weight, ffn_gain, gate_a, up_a, down_a, gate_b, up_b, down_b, *refs
):
    count = len(part)
    resids, seconds, norms = refs[:count], refs[count : 2 * count], refs[2 * count : 3 * count]
    outs = refs[-count * chunks - (1 if own else 0) :]
    slots = resids[0].shape[0]
    total = count * slots
    half = seconds[0].shape[1]
    resid_rows = [jnp.concatenate([r[:, :half], t[...]], axis=1) for r, t in zip(resids, seconds)]
    norm_rows = [n[...] for n in norms]
    if own:
        resid_rows.append(refs[3 * count][...])
        norm_rows.append(refs[3 * count + 1][...])
    join = lambda parts: parts[0] if len(parts) == 1 else jnp.concatenate(parts)
    middle = join(resid_rows).astype(f32) + dot(join(norm_rows), out_weight[...])
    if own:
        outs[-1][...] = middle[total:]
        middle = middle[:total]
    scale = lax.rsqrt(jnp.mean(middle * middle, axis=-1, keepdims=True) + epsilon)
    x = (middle * scale * ffn_gain[...]).astype(bf16)
    hiddens = []
    for gate, up in ((gate_a, up_a), (gate_b, up_b)):
        g = dot(x, gate[0])
        u = dot(x, up[0])
        hiddens.append((g / (1.0 + jnp.exp(-g)) * u).astype(bf16))
    shares = []
    for k, r in zip(part, resids):
        tail = r[:, half:].astype(f32)
        lane = lax.broadcasted_iota(jnp.int32, tail.shape, 1)
        shares.append(jnp.sum(jnp.where(lane // 3 == k, tail, 0.0), axis=-1, keepdims=True))
    weight = join(shares)
    chunk = outs[0].shape[1]
    for j in range(chunks):
        cols = slice(j * chunk, (j + 1) * chunk)
        out = dot(hiddens[0], down_a[0, :, cols]) + dot(hiddens[1], down_b[0, :, cols])
        out = (out * weight).astype(bf16)
        for i in range(count):
            outs[i * chunks + j][...] = out[i * slots : (i + 1) * slots]


def combine_kernel(sources, tokens, table, *refs):
    rows, outs = refs[:sources], refs[sources:]
    total = None
    for k in range(sources):
        part = dot(table[k], rows[k][...])
        total = part if total is None else total + part
    for g, out in enumerate(outs):
        out[...] = total[g * tokens : (g + 1) * tokens].astype(out.dtype)


VM = pl.BlockSpec(memory_space=pltpu.VMEM)
ANY = pl.BlockSpec(memory_space=pl.ANY)


def call(body, args, outs, scratch=(), after=(), flops=0, trans=0, inside=(), room=32):
    size = lambda a: int(np.prod(a.shape)) * a.dtype.itemsize
    count = len(args)
    after = list(after)

    def kernel(*refs):
        body(*refs[:count], *refs[count + len(after) :])

    held = [
        pltpu.with_memory_space_constraint(a, pltpu.VMEM) if i in inside else a
        for i, a in enumerate(args)
    ]
    return pl.pallas_call(
        kernel,
        out_shape=outs,
        in_specs=[VM] * count + [ANY] * len(after),
        out_specs=jax.tree.map(lambda _: VM, outs),
        scratch_shapes=list(scratch),
        cost_estimate=pl.CostEstimate(
            flops=int(flops),
            transcendentals=int(trans),
            bytes_accessed=sum(map(size, args)) + sum(map(size, jax.tree.leaves(outs))),
        ),
        compiler_params=pltpu.CompilerParams(vmem_limit_bytes=room * 1024 * 1024),
    )(*held, *after)


def shape(dims, dtype):
    return jax.ShapeDtypeStruct(tuple(dims), dtype)


def program(
    queries, latent, rot_key, latent_gain, key_up, value_up, query_gain, key_gain, out_gain,
    out_weight, residual, ffn_gain, routes, route_weights, expert_gate, expert_up, expert_down,
):
    rows = queries.shape[0]
    heads = key_up.shape[1] // NOPE
    width = residual.shape[1]
    sp, tp = lax.axis_size("sp"), lax.axis_size("tp")
    groups = tp // 2
    tokens = residual.shape[0]
    all_tokens = groups * tokens
    att_width = out_weight.shape[0]
    cap = max(2, 9 * tokens * TOPK // (8 * sp))
    slots = groups * cap

    def swap(v, axis, k, size):
        return lax.ppermute(v, axis, [(i, i ^ k) for i in range(size)])

    swap_core = lambda v: swap(v, "tp", 1, tp)
    swap_z = lambda v, k: swap(v, "tp", 2 * k, tp)
    swap_sp = lambda v, k: swap(v, "sp", k, sp)

    flags = np.zeros((4 * TOPK, LANES), np.float32)
    flags[np.arange(4 * TOPK), np.arange(4 * TOPK)] = 1.0
    ordinal = np.arange(all_tokens)
    lower = (ordinal[:, None] > ordinal[None, :]) & (
        ordinal[:, None] // tokens == ordinal[None, :] // tokens
    )
    lower = jnp.asarray(lower.astype(np.float32), bf16)
    first_half, second_half = call(
        pack_kernel,
        [routes.T, route_weights.T, residual, jnp.asarray(flags, bf16)],
        (shape((tokens, width // 2 + LANES), bf16), shape((tokens, width // 2), bf16)),
        room=ROOM,
    )
    first_parts = [first_half] + [swap_z(first_half, k) for k in range(1, groups)]
    second_parts = [second_half] + [swap_z(second_half, k) for k in range(1, groups)]

    pack = LANES // (ROPE * heads)
    inner, first = turn_tables(rows, sp)
    selk = jnp.asarray(np.concatenate(rope_select(0, ROPE), axis=1), bf16)
    selq = jnp.asarray(head_select(heads), bf16)
    selg = jnp.asarray(np.abs(head_select(1)), f32)
    bundle, q1, q2 = call(
        functools.partial(prep_kernel, heads),
        [
            latent, rot_key.T, latent_gain[None, :], key_up, value_up, queries.T,
            query_gain[None, :], key_gain[None, :], inner, first, selq, selk, selg,
        ],
        (
            shape((heads * rows + rows // pack, LANES), bf16),
            shape((heads, rows, LANES), bf16),
            shape((heads * pack, rows, LANES), bf16),
        ),
        flops=2 * rows * latent.shape[1] * 256 + 2 * rows * 192 * 768,
        room=ROOM,
    )
    bundles = [bundle] + [swap_sp(bundle, k) for k in range(1, sp)]

    gate_b = swap_core(expert_gate)
    up_b = swap_core(expert_up)
    down_b = swap_core(expert_down)
    table, *first_rows = call(
        functools.partial(residual_first_kernel, groups, sp, cap),
        [lower] + first_parts,
        (shape((sp, all_tokens, slots), bf16),)
        + tuple([shape((slots, width // 2 + LANES), bf16)] * sp),
        [pltpu.VMEM((all_tokens, width // 2 + LANES), bf16)],
        flops=sp * slots * all_tokens * width,
    )
    first_in = [first_rows[0]] + [swap_sp(first_rows[k], k) for k in range(1, sp)]

    half = heads * VH
    split = min(3, sp)
    early, late = list(range(split)), list(range(split, sp))
    state = call(
        functools.partial(attend_first_kernel, heads, early),
        [q1, q2] + [bundles[k] for k in early],
        shape((heads, LANES, rows), f32),
        room=ROOM,
        flops=2 * heads * rows * rows * len(early) * 384,
        trans=heads * rows * rows * len(early),
    )
    keep, send = call(
        functools.partial(attend_last_kernel, heads, tokens, groups, late),
        [q1, q2, state] + [bundles[k] for k in late],
        (shape((all_tokens, half), bf16), shape((all_tokens, half), bf16)),
        [pltpu.VMEM((heads, LANES, rows), f32), pltpu.VMEM((rows, half), f32)],
        room=ROOM,
        flops=2 * heads * rows * rows * len(late) * 384,
        trans=heads * rows * rows * len(late),
    )
    second_rows = call(
        functools.partial(residual_second_kernel, groups),
        [table] + second_parts,
        tuple([shape((slots, width // 2), bf16)] * sp),
        [pltpu.VMEM((all_tokens, width // 2), bf16)],
        flops=sp * slots * all_tokens * width,
    )
    second_in = [second_rows[0]] + [swap_sp(second_rows[k], k) for k in range(1, sp)]
    other = swap_core(send)
    pieces = [keep, other]
    kept_in = [swap_z(keep, k) for k in range(1, groups)]
    other_in = [swap_z(other, k) for k in range(1, groups)]
    for a, b in zip(kept_in, other_in):
        pieces += [a, b]
    *norm_rows, own_rows = call(
        functools.partial(choose_kernel, groups, tokens),
        [out_gain[None, :], table] + pieces,
        tuple([shape((slots, att_width), bf16)] * sp) + (shape((tokens, att_width), bf16),),
        [pltpu.VMEM((all_tokens, att_width), f32), pltpu.VMEM((all_tokens, att_width), bf16)],
        flops=2 * sp * slots * all_tokens * att_width,
    )
    norm_in = [norm_rows[0]] + [swap_sp(norm_rows[k], k) for k in range(1, sp)]

    hidden = 2 * expert_gate.shape[2]
    chunk = width // COL_CHUNKS
    parts = expert_parts(sp)
    served = [None] * sp
    before = []
    for n, part in enumerate(parts):
        extra_in = [residual, own_rows] if n == 0 else []
        extra_out = (shape((tokens, width), f32),) if n == 0 else ()
        outs = call(
            functools.partial(expert_kernel, part, COL_CHUNKS, n == 0),
            [
                out_weight, ffn_gain[None, :], expert_gate, expert_up, expert_down,
                gate_b, up_b, down_b,
            ]
            + [first_in[k] for k in part]
            + [second_in[k] for k in part]
            + [norm_in[k] for k in part]
            + extra_in,
            tuple([shape((slots, chunk), bf16)] * (len(part) * COL_CHUNKS)) + extra_out,
            after=before,
            flops=2 * len(part) * slots * width * (att_width + 3 * hidden),
            inside=(0, 2, 3, 4, 5, 6, 7),
        )
        if n == 0:
            middle = outs[-1]
        before = [outs[0]]
        for i, k in enumerate(part):
            served[k] = outs[i * COL_CHUNKS : (i + 1) * COL_CHUNKS]
    finished = []
    for j in range(COL_CHUNKS):
        back = [served[0][j]] + [swap_sp(served[k][j], k) for k in range(1, sp)]
        own, *rest = call(
            functools.partial(combine_kernel, sp, tokens),
            [table] + back,
            (shape((tokens, chunk), f32),) + tuple([shape((tokens, chunk), bf16)] * (groups - 1)),
            flops=2 * all_tokens * sp * slots * chunk,
        )
        total = middle[:, j * chunk : (j + 1) * chunk] + own
        for k in range(1, groups):
            total = total + swap_z(rest[k - 1], k).astype(f32)
        finished.append(total.astype(bf16))
    return jnp.concatenate(finished, axis=1)


def expert_parts(sp):
    parts, at = [[0], [k for k in (1, 2) if k < sp]], 3
    while at < sp:
        parts.append(list(range(at, min(at + 4, sp))))
        at += 4
    return [p for p in parts if p]


def solution(mesh):
    return jax.shard_map(
        program,
        mesh=mesh,
        in_specs=(
            P("sp", "tp"),
            P("sp", None),
            P("sp", None),
            P(),
            P(None, "tp"),
            P(None, "tp"),
            P(),
            P(),
            P(),
            P(),
            P(("sp", "tp"), None),
            P(),
            P(("sp", "tp"), None),
            P(("sp", "tp"), None),
            P("sp", None, "tp"),
            P("sp", None, "tp"),
            P("sp", "tp", None),
        ),
        out_specs=P(("sp", "tp"), None),
        check_vma=False,
    )
```

profile of v0, /device:TPU:0, one launch (start us, length us, event | category | flops | bytes accessed | tf_op | source)
XLA Modules:
  0.0 144.4 jit_solution(10180203264115754562)
XLA Ops:
  0.0 3.8 %shard_map.229 = (bf16[1280,128]{1,0:T(8,128)(2,1)}, bf16[2,512,128]{2,1,0:T(8,128)(2,1)}, bf16[4,512,128]{2,1,0:T(8,128)(2,1)}) custom-call(bf16[512,512]{1,0:T(8,128)(2,1)} %refs_0_.5, bf16[32,512]{1,0:T(8,128)(2,1)} %bitcast.14, f32[1,512]{1,0:T(1,128)} %bitcast.15, bf16[512,128]{1,0:T(8,128)(2,1)} %refs_3_.5, bf16[512,128]{1,0:T(8,128)(2,1)} %refs_4_.4, ...), custom_call_target="tpu_custom_call" | custom-call | flops 285212672 | bytes 3119872 | tf_op jit(solution)/shard_map/pallas_call | solution.py:383
  3.8 3.9 %collective-permute-start.11 = (bf16[1280,128]{1,0:T(8,128)(2,1)}, bf16[1280,128]{1,0:T(8,128)(2,1)S(1)}, u32[]{:S(2)}, u32[]{:S(2)}) collective-permute-start(bf16[1280,128]{1,0:T(8,128)(2,1)} %get-tuple-element.50.refs_2_), channel_id=1, source_target_pairs={{0,24},{8,16},{16,8},{24,0},{1,25},{9,17},{17,9},{25,1},{2,26},{10... | collective-permute-start | bytes 983048 | tf_op jit(solution)/shard_map/ppermute | solution.py:418
  7.7 1.8 %shard_map.226 = (bf16[64,1152]{1,0:T(8,128)(2,1)}, bf16[64,1024]{1,0:T(8,128)(2,1)}) custom-call(s32[2,64]{1,0:T(2,128)} %bitcast.16, f32[2,64]{1,0:T(2,128)} %bitcast.17, bf16[64,2048]{1,0:T(8,128)(2,1)} %refs_11_.2, bf16[8,128]{1,0:T(8,128)(2,1)} %constant.15.clone.refs_3_), custom_call_target="tpu_custom_call" | custom-call | bytes 543744 | tf_op jit(solution)/shard_map/pallas_call | solution.py:383
  9.5 3.6 %collective-permute-start.8 = (bf16[64,1024]{1,0:T(8,128)(2,1)}, bf16[64,1024]{1,0:T(8,128)(2,1)S(1)}, u32[]{:S(2)}, u32[]{:S(2)}) collective-permute-start(bf16[64,1024]{1,0:T(8,128)(2,1)} %get-tuple-element.46.refs_1_), channel_id=1, source_target_pairs={{0,6},{1,7},{2,4},{3,5},{4,2},{5,3},{6,0},{7,1},{8,14},{9,15},{10,... | collective-permute-start | bytes 393224 | tf_op jit(solution)/shard_map/ppermute | solution.py:418
  13.1 1.9 %collective-permute-start.5 = (bf16[64,1152]{1,0:T(8,128)(2,1)}, bf16[64,1152]{1,0:T(8,128)(2,1)S(1)}, u32[]{:S(2)}, u32[]{:S(2)}) collective-permute-start(bf16[64,1152]{1,0:T(8,128)(2,1)} %get-tuple-element.43.refs_1_), channel_id=1, source_target_pairs={{0,6},{1,7},{2,4},{3,5},{4,2},{5,3},{6,0},{7,1},{8,14},{9,15},{10,... | collective-permute-start | bytes 442376 | tf_op jit(solution)/shard_map/ppermute | solution.py:418
  19.1 9.1 %collective-permute-done.7.refs_3_ = bf16[64,1024]{1,0:T(8,128)(2,1)S(1)} collective-permute-done((bf16[64,1024]{1,0:T(8,128)(2,1)}, bf16[64,1024]{1,0:T(8,128)(2,1)S(1)}, u32[]{:S(2)}, u32[]{:S(2)}) %collective-permute-start.7) | collective-permute-done | bytes 131104 | tf_op jit(solution)/shard_map/ppermute | solution.py:418
  30.7 4.7 %collective-permute-start.4 = (bf16[64,1152]{1,0:T(8,128)(2,1)}, bf16[64,1152]{1,0:T(8,128)(2,1)S(1)}, u32[]{:S(2)}, u32[]{:S(2)}) collective-permute-start(bf16[64,1152]{1,0:T(8,128)(2,1)} %get-tuple-element.43.refs_1_), channel_id=1, source_target_pairs={{0,4},{1,5},{2,6},{3,7},{4,0},{5,1},{6,2},{7,3},{8,12},{9,13},{10,... | collective-permute-start | bytes 442376 | tf_op jit(solution)/shard_map/ppermute | solution.py:418
  37.7 3.6 %shard_map.230.refs_2_ = f32[2,128,512]{2,1,0:T(8,128)} custom-call(bf16[2,512,128]{2,1,0:T(8,128)(2,1)} %get-tuple-element.48.refs_0_, bf16[4,512,128]{2,1,0:T(8,128)(2,1)} %get-tuple-element.49.refs_1_, bf16[1280,128]{1,0:T(8,128)(2,1)} %get-tuple-element.50.refs_2_, bf16[1280,128]{1,0:T(8,128)(2,1)} %copy-done.20, bf16[1280,128]{1,0:T(8,128)(2,1)} %copy-done.19), custom_call_target="tpu_custom_call" | custom-call | flops 1207959552 | bytes 2293760 | tf_op jit(solution)/shard_map/pallas_call | solution.py:383
  41.3 2.4 %shard_map.231 = (bf16[256,128]{1,0:T(8,128)(2,1)}, bf16[256,128]{1,0:T(8,128)(2,1)}) custom-call(bf16[2,512,128]{2,1,0:T(8,128)(2,1)} %get-tuple-element.48.refs_0_, bf16[4,512,128]{2,1,0:T(8,128)(2,1)} %get-tuple-element.49.refs_1_, f32[2,128,512]{2,1,0:T(8,128)} %shard_map.230.refs_2_, bf16[1280,128]{1,0:T(8,128)(2,1)} %copy-done.18), custom_call_target="tpu_custom_call" | custom-call | flops 402653184 | bytes 1769472 | tf_op jit(solution)/shard_map/pallas_call | solution.py:383
  43.7 2.2 %collective-permute-start.17 = (bf16[256,128]{1,0:T(8,128)(2,1)}, bf16[256,128]{1,0:T(8,128)(2,1)S(1)}, u32[]{:S(2)}, u32[]{:S(2)}) collective-permute-start(bf16[256,128]{1,0:T(8,128)(2,1)} %get-tuple-element.51.refs_2_), channel_id=1, source_target_pairs={{0,6},{1,7},{2,4},{3,5},{4,2},{5,3},{6,0},{7,1},{8,14},{9,15},{10,... | collective-permute-start | bytes 196616 | tf_op jit(solution)/shard_map/ppermute | solution.py:418
  50.7 2.1 %collective-permute-start.13 = (bf16[256,128]{1,0:T(8,128)(2,1)}, bf16[256,128]{1,0:T(8,128)(2,1)S(1)}, u32[]{:S(2)}, u32[]{:S(2)}) collective-permute-start(bf16[256,128]{1,0:T(8,128)(2,1)} %get-tuple-element.51.refs_2_), channel_id=1, source_target_pairs={{0,2},{1,3},{2,0},{3,1},{4,6},{5,7},{6,4},{7,5},{8,10},{9,11},{10,... | collective-permute-start | bytes 196616 | tf_op jit(solution)/shard_map/ppermute | solution.py:418
  57.0 1.9 %collective-permute-start.21 = (bf16[144,1024]{1,0:T(8,128)(2,1)S(1)}, bf16[144,1024]{1,0:T(8,128)(2,1)S(1)}, u32[]{:S(2)}, u32[]{:S(2)}) collective-permute-start(bf16[144,1024]{1,0:T(8,128)(2,1)S(1)} %get-tuple-element.59), channel_id=1, source_target_pairs={{0,8},{8,0},{16,24},{24,16},{1,9},{9,1},{17,25},{25,17},{2,10},{10... | collective-permute-start | bytes 884744 | tf_op jit(solution)/shard_map/ppermute | solution.py:418
  58.9 3.1 %collective-permute-start.22 = (bf16[144,1024]{1,0:T(8,128)(2,1)S(1)}, bf16[144,1024]{1,0:T(8,128)(2,1)S(1)}, u32[]{:S(2)}, u32[]{:S(2)}) collective-permute-start(bf16[144,1024]{1,0:T(8,128)(2,1)S(1)} %get-tuple-element.60), channel_id=1, source_target_pairs={{0,16},{8,24},{16,0},{24,8},{1,17},{9,25},{17,1},{25,9},{2,18},{10... | collective-permute-start | bytes 884744 | tf_op jit(solution)/shard_map/ppermute | solution.py:418
  61.9 1.8 %collective-permute-done.21.refs_10_ = bf16[144,1024]{1,0:T(8,128)(2,1)S(1)} collective-permute-done((bf16[144,1024]{1,0:T(8,128)(2,1)S(1)}, bf16[144,1024]{1,0:T(8,128)(2,1)S(1)}, u32[]{:S(2)}, u32[]{:S(2)}) %collective-permute-start.21) | collective-permute-done | bytes 294944 | tf_op jit(solution)/shard_map/ppermute | solution.py:418
  63.8 2.2 %collective-permute-start.18 = (bf16[256,128]{1,0:T(8,128)(2,1)S(1)}, bf16[256,128]{1,0:T(8,128)(2,1)S(1)}, u32[]{:S(2)}, u32[]{:S(2)}) collective-permute-start(bf16[256,128]{1,0:T(8,128)(2,1)S(1)} %collective-permute-done.12.refs_3_), channel_id=1, source_target_pairs={{0,6},{1,7},{2,4},{3,5},{4,2},{5,3},{6,0},{7,1},{8,14},{9,15},{10,... | collective-permute-start | bytes 196616 | tf_op jit(solution)/shard_map/ppermute | solution.py:418
  66.6 1.6 %collective-permute-start.16 = (bf16[256,128]{1,0:T(8,128)(2,1)S(1)}, bf16[256,128]{1,0:T(8,128)(2,1)S(1)}, u32[]{:S(2)}, u32[]{:S(2)}) collective-permute-start(bf16[256,128]{1,0:T(8,128)(2,1)S(1)} %collective-permute-done.12.refs_3_), channel_id=1, source_target_pairs={{0,4},{1,5},{2,6},{3,7},{4,0},{5,1},{6,2},{7,3},{8,12},{9,13},{10,... | collective-permute-start | bytes 196616 | tf_op jit(solution)/shard_map/ppermute | solution.py:418
  68.2 2.2 %collective-permute-done.18.refs_9_ = bf16[256,128]{1,0:T(8,128)(2,1)S(1)} collective-permute-done((bf16[256,128]{1,0:T(8,128)(2,1)S(1)}, bf16[256,128]{1,0:T(8,128)(2,1)S(1)}, u32[]{:S(2)}, u32[]{:S(2)}) %collective-permute-start.18) | collective-permute-done | bytes 65568 | tf_op jit(solution)/shard_map/ppermute | solution.py:418
  70.4 2.1 %collective-permute-done.16.refs_7_ = bf16[256,128]{1,0:T(8,128)(2,1)S(1)} collective-permute-done((bf16[256,128]{1,0:T(8,128)(2,1)S(1)}, bf16[256,128]{1,0:T(8,128)(2,1)S(1)}, u32[]{:S(2)}, u32[]{:S(2)}) %collective-permute-start.16) | collective-permute-done | bytes 65568 | tf_op jit(solution)/shard_map/ppermute | solution.py:418
  74.7 3.1 %collective-permute-start.20 = (bf16[144,1152]{1,0:T(8,128)(2,1)S(1)}, bf16[144,1152]{1,0:T(8,128)(2,1)S(1)}, u32[]{:S(2)}, u32[]{:S(2)}) collective-permute-start(bf16[144,1152]{1,0:T(8,128)(2,1)S(1)} %get-tuple-element.58), channel_id=1, source_target_pairs={{0,16},{8,24},{16,0},{24,8},{1,17},{9,25},{17,1},{25,9},{2,18},{10... | collective-permute-start | bytes 995336 | tf_op jit(solution)/shard_map/ppermute | solution.py:418
  81.0 2.0 %collective-permute-start.27 = (bf16[144,1152]{1,0:T(8,128)(2,1)S(1)}, bf16[144,1152]{1,0:T(8,128)(2,1)S(1)}, u32[]{:S(2)}, u32[]{:S(2)}) collective-permute-start(bf16[144,1152]{1,0:T(8,128)(2,1)S(1)} %get-tuple-element.65), channel_id=1, source_target_pairs={{0,24},{8,16},{16,8},{24,0},{1,25},{9,17},{17,9},{25,1},{2,26},{10... | collective-permute-start | bytes 995336 | tf_op jit(solution)/shard_map/ppermute | solution.py:418
  83.1 2.2 %copy-done = bf16[1024,2048]{1,0:T(8,128)(2,1)S(1)} copy-done((bf16[1024,2048]{1,0:T(8,128)(2,1)S(1)}, bf16[1024,2048]{1,0:T(8,128)(2,1)}, u32[]{:S(2)}) %copy-start) | copy-done | bytes 4194328
  85.3 4.3 %shard_map.233 = (bf16[144,1024]{1,0:T(8,128)(2,1)S(1)}, bf16[144,1024]{1,0:T(8,128)(2,1)S(1)}, f32[64,2048]{1,0:T(8,128)S(1)}) custom-call(bf16[1024,2048]{1,0:T(8,128)(2,1)S(1)} %copy-done, f32[1,2048]{1,0:T(1,128)S(1)} %bitcast.9, bf16[1,2048,256]{2,1,0:T(8,128)(2,1)S(1)} %copy-done.2, bf16[1,2048,256]{2,1,0:T(8,128)(2,1)S(1)} %copy-done.3, ...), custom_call_target="tpu_custom_call" | custom-call | flops 1509949440 | bytes 12922880 | tf_op jit(solution)/shard_map/pallas_call | solution.py:383
  90.7 2.0 %collective-permute-start.29 = (bf16[144,1024]{1,0:T(8,128)(2,1)S(1)}, bf16[144,1024]{1,0:T(8,128)(2,1)S(1)}, u32[]{:S(2)}, u32[]{:S(2)}) collective-permute-start(bf16[144,1024]{1,0:T(8,128)(2,1)S(1)} %get-tuple-element.67), channel_id=1, source_target_pairs={{0,24},{8,16},{16,8},{24,0},{1,25},{9,17},{17,9},{25,1},{2,26},{10... | collective-permute-start | bytes 884744 | tf_op jit(solution)/shard_map/ppermute | solution.py:418
  92.6 15.1 %collective-permute-done.24.refs_13_ = bf16[144,1024]{1,0:T(8,128)(2,1)S(1)} collective-permute-done((bf16[144,1024]{1,0:T(8,128)(2,1)S(1)}, bf16[144,1024]{1,0:T(8,128)(2,1)S(1)}, u32[]{:S(2)}, u32[]{:S(2)}) %collective-permute-start.24) | collective-permute-done | bytes 294944 | tf_op jit(solution)/shard_map/ppermute | solution.py:418
  107.8 5.5 %shard_map.234 = (bf16[144,1024]{1,0:T(8,128)(2,1)S(1)}, bf16[144,1024]{1,0:T(8,128)(2,1)S(1)}, bf16[144,1024]{1,0:T(8,128)(2,1)S(1)}, bf16[144,1024]{1,0:T(8,128)(2,1)S(1)}) custom-call(bf16[1024,2048]{1,0:T(8,128)(2,1)S(1)} %copy-done.1, f32[1,2048]{1,0:T(1,128)S(1)} %bitcast.10, bf16[1,2048,256]{2,1,0:T(8,128)(2,1)S(1)} %copy-done.2, ...), custom_call_target="tpu_custom_call" | custom-call | flops 3019898880 | bytes 13516800 | tf_op jit(solution)/shard_map/pallas_call | solution.py:383
  114.6 3.9 %shard_map.235 = (bf16[144,1024]{1,0:T(8,128)(2,1)S(1)}, bf16[144,1024]{1,0:T(8,128)(2,1)S(1)}) custom-call(bf16[1024,2048]{1,0:T(8,128)(2,1)S(1)} %copy-done.1, f32[1,2048]{1,0:T(1,128)S(1)} %bitcast.11, bf16[1,2048,256]{2,1,0:T(8,128)(2,1)S(1)} %copy-done.2, bf16[1,2048,256]{2,1,0:T(8,128)(2,1)S(1)} %copy-done.3, bf16[1,256,2048]{2,1,0:T(8,128)(2,1)S(1)} %copy-done.4, ...), custom_call_target="tpu_custom_call" | custom-call | flops 1509949440 | bytes 12005376 | tf_op jit(solution)/shard_map/pallas_call | solution.py:383
  118.5 2.3 %collective-permute-start.30 = (bf16[144,1024]{1,0:T(8,128)(2,1)S(1)}, bf16[144,1024]{1,0:T(8,128)(2,1)S(1)}, u32[]{:S(2)}, u32[]{:S(2)}) collective-permute-start(bf16[144,1024]{1,0:T(8,128)(2,1)S(1)} %get-tuple-element.68), channel_id=1, source_target_pairs={{0,24},{8,16},{16,8},{24,0},{1,25},{9,17},{17,9},{25,1},{2,26},{10... | collective-permute-start | bytes 884744 | tf_op jit(solution)/shard_map/ppermute | solution.py:418
  122.1 2.4 %collective-permute-start.36 = (bf16[144,1024]{1,0:T(8,128)(2,1)S(1)}, bf16[144,1024]{1,0:T(8,128)(2,1)S(1)}, u32[]{:S(2)}, u32[]{:S(2)}) collective-permute-start(bf16[144,1024]{1,0:T(8,128)(2,1)S(1)} %get-tuple-element.76), channel_id=1, source_target_pairs={{0,24},{8,16},{16,8},{24,0},{1,25},{9,17},{17,9},{25,1},{2,26},{10... | collective-permute-start | bytes 884744 | tf_op jit(solution)/shard_map/ppermute | solution.py:418
  124.5 1.8 %collective-permute-done.30.refs_4_ = bf16[144,1024]{1,0:T(8,128)(2,1)S(1)} collective-permute-done((bf16[144,1024]{1,0:T(8,128)(2,1)S(1)}, bf16[144,1024]{1,0:T(8,128)(2,1)S(1)}, u32[]{:S(2)}, u32[]{:S(2)}) %collective-permute-start.30) | collective-permute-done | bytes 294944 | tf_op jit(solution)/shard_map/ppermute | solution.py:418
  127.1 2.7 %collective-permute-start.32 = (bf16[64,1024]{1,0:T(8,128)(2,1)S(1)}, bf16[64,1024]{1,0:T(8,128)(2,1)S(1)}, u32[]{:S(2)}, u32[]{:S(2)}) collective-permute-start(bf16[64,1024]{1,0:T(8,128)(2,1)S(1)} %get-tuple-element.71), channel_id=1, source_target_pairs={{0,4},{1,5},{2,6},{3,7},{4,0},{5,1},{6,2},{7,3},{8,12},{9,13},{10,... | collective-permute-start | bytes 393224 | tf_op jit(solution)/shard_map/ppermute | solution.py:418
  129.8 1.6 %collective-permute-start.33 = (bf16[64,1024]{1,0:T(8,128)(2,1)S(1)}, bf16[64,1024]{1,0:T(8,128)(2,1)S(1)}, u32[]{:S(2)}, u32[]{:S(2)}) collective-permute-start(bf16[64,1024]{1,0:T(8,128)(2,1)S(1)} %get-tuple-element.72), channel_id=1, source_target_pairs={{0,6},{1,7},{2,4},{3,5},{4,2},{5,3},{6,0},{7,1},{8,14},{9,15},{10,... | collective-permute-start | bytes 393224 | tf_op jit(solution)/shard_map/ppermute | solution.py:418
  138.5 4.9 %collective-permute-done.38 = bf16[64,1024]{1,0:T(8,128)(2,1)S(1)} collective-permute-done((bf16[64,1024]{1,0:T(8,128)(2,1)S(1)}, bf16[64,1024]{1,0:T(8,128)(2,1)S(1)}, u32[]{:S(2)}, u32[]{:S(2)}) %collective-permute-start.38) | collective-permute-done | bytes 131104 | tf_op jit(solution)/shard_map/ppermute | solution.py:418
  (104 shorter events, 36.3 us)
Async XLA Ops:
  3.8 26.8 %collective-permute-start.11 = (bf16[1280,128]{1,0:T(8,128)(2,1)}, bf16[1280,128]{1,0:T(8,128)(2,1)S(1)}, u32[]{:S(2)}, u32[]{:S(2)}) collective-permute-start(bf16[1280,128]{1,0:T(8,128)(2,1)} %get-tuple-element.50.refs_2_), channel_id=1, source_target_pairs={{0,24},{8,16},{16,8},{24,0},{1,25},{9,17},{17,9},{25,1},{2,26},{10... | collective-permute-start | bytes 983048 | tf_op jit(solution)/shard_map/ppermute | solution.py:418
  9.5 8.4 %collective-permute-start.8 = (bf16[64,1024]{1,0:T(8,128)(2,1)}, bf16[64,1024]{1,0:T(8,128)(2,1)S(1)}, u32[]{:S(2)}, u32[]{:S(2)}) collective-permute-start(bf16[64,1024]{1,0:T(8,128)(2,1)} %get-tuple-element.46.refs_1_), channel_id=1, source_target_pairs={{0,6},{1,7},{2,4},{3,5},{4,2},{5,3},{6,0},{7,1},{8,14},{9,15},{10,... | collective-permute-start | bytes 393224 | tf_op jit(solution)/shard_map/ppermute | solution.py:418
  13.1 15.1 %collective-permute-start.7 = (bf16[64,1024]{1,0:T(8,128)(2,1)}, bf16[64,1024]{1,0:T(8,128)(2,1)S(1)}, u32[]{:S(2)}, u32[]{:S(2)}) collective-permute-start(bf16[64,1024]{1,0:T(8,128)(2,1)} %get-tuple-element.46.refs_1_), channel_id=1, source_target_pairs={{0,4},{1,5},{2,6},{3,7},{4,0},{5,1},{6,2},{7,3},{8,12},{9,13},{10,... | collective-permute-start | bytes 393224 | tf_op jit(solution)/shard_map/ppermute | solution.py:418
  13.1 17.0 %collective-permute-start.5 = (bf16[64,1152]{1,0:T(8,128)(2,1)}, bf16[64,1152]{1,0:T(8,128)(2,1)S(1)}, u32[]{:S(2)}, u32[]{:S(2)}) collective-permute-start(bf16[64,1152]{1,0:T(8,128)(2,1)} %get-tuple-element.43.refs_1_), channel_id=1, source_target_pairs={{0,6},{1,7},{2,4},{3,5},{4,2},{5,3},{6,0},{7,1},{8,14},{9,15},{10,... | collective-permute-start | bytes 442376 | tf_op jit(solution)/shard_map/ppermute | solution.py:418
  15.0 14.4 %collective-permute-start.6 = (bf16[64,1024]{1,0:T(8,128)(2,1)}, bf16[64,1024]{1,0:T(8,128)(2,1)S(1)}, u32[]{:S(2)}, u32[]{:S(2)}) collective-permute-start(bf16[64,1024]{1,0:T(8,128)(2,1)} %get-tuple-element.46.refs_1_), channel_id=1, source_target_pairs={{0,2},{1,3},{2,0},{3,1},{4,6},{5,7},{6,4},{7,5},{8,10},{9,11},{10,... | collective-permute-start | bytes 393224 | tf_op jit(solution)/shard_map/ppermute | solution.py:418
  18.6 12.1 %collective-permute-start.10 = (bf16[1280,128]{1,0:T(8,128)(2,1)}, bf16[1280,128]{1,0:T(8,128)(2,1)S(1)}, u32[]{:S(2)}, u32[]{:S(2)}) collective-permute-start(bf16[1280,128]{1,0:T(8,128)(2,1)} %get-tuple-element.50.refs_2_), channel_id=1, source_target_pairs={{0,16},{8,24},{16,0},{24,8},{1,17},{9,25},{17,1},{25,9},{2,18},{10... | collective-permute-start | bytes 983048 | tf_op jit(solution)/shard_map/ppermute | solution.py:418
  28.9 8.0 %collective-permute-start.9 = (bf16[1280,128]{1,0:T(8,128)(2,1)}, bf16[1280,128]{1,0:T(8,128)(2,1)S(1)}, u32[]{:S(2)}, u32[]{:S(2)}) collective-permute-start(bf16[1280,128]{1,0:T(8,128)(2,1)} %get-tuple-element.50.refs_2_), channel_id=1, source_target_pairs={{0,8},{8,0},{16,24},{24,16},{1,9},{9,1},{17,25},{25,17},{2,10},{10... | collective-permute-start | bytes 983048 | tf_op jit(solution)/shard_map/ppermute | solution.py:418
  30.1 49.4 %collective-permute-start = (bf16[1,2048,256]{2,1,0:T(8,128)(2,1)}, bf16[1,2048,256]{2,1,0:T(8,128)(2,1)}, u32[]{:S(2)}, u32[]{:S(2)}) collective-permute-start(bf16[1,2048,256]{2,1,0:T(8,128)(2,1)} %refs_2_.7), channel_id=1, source_target_pairs={{0,1},{1,0},{2,3},{3,2},{4,5},{5,4},{6,7},{7,6},{8,9},{9,8},{10,11... | collective-permute-start | bytes 3145736 | tf_op jit(solution)/shard_map/ppermute | solution.py:418
  30.1 51.0 %collective-permute-start.1 = (bf16[1,2048,256]{2,1,0:T(8,128)(2,1)}, bf16[1,2048,256]{2,1,0:T(8,128)(2,1)}, u32[]{:S(2)}, u32[]{:S(2)}) collective-permute-start(bf16[1,2048,256]{2,1,0:T(8,128)(2,1)} %refs_3_.8), channel_id=1, source_target_pairs={{0,1},{1,0},{2,3},{3,2},{4,5},{5,4},{6,7},{7,6},{8,9},{9,8},{10,11... | collective-permute-start | bytes 3145736 | tf_op jit(solution)/shard_map/ppermute | solution.py:418
  30.6 50.5 %collective-permute-start.2 = (bf16[1,256,2048]{2,1,0:T(8,128)(2,1)}, bf16[1,256,2048]{2,1,0:T(8,128)(2,1)}, u32[]{:S(2)}, u32[]{:S(2)}) collective-permute-start(bf16[1,256,2048]{2,1,0:T(8,128)(2,1)} %refs_4_.7), channel_id=1, source_target_pairs={{0,1},{1,0},{2,3},{3,2},{4,5},{5,4},{6,7},{7,6},{8,9},{9,8},{10,11... | collective-permute-start | bytes 3145736 | tf_op jit(solution)/shard_map/ppermute | solution.py:418
  30.7 13.0 %collective-permute-start.4 = (bf16[64,1152]{1,0:T(8,128)(2,1)}, bf16[64,1152]{1,0:T(8,128)(2,1)S(1)}, u32[]{:S(2)}, u32[]{:S(2)}) collective-permute-start(bf16[64,1152]{1,0:T(8,128)(2,1)} %get-tuple-element.43.refs_1_), channel_id=1, source_target_pairs={{0,4},{1,5},{2,6},{3,7},{4,0},{5,1},{6,2},{7,3},{8,12},{9,13},{10,... | collective-permute-start | bytes 442376 | tf_op jit(solution)/shard_map/ppermute | solution.py:418
  46.0 11.0 %collective-permute-start.15 = (bf16[256,128]{1,0:T(8,128)(2,1)}, bf16[256,128]{1,0:T(8,128)(2,1)S(1)}, u32[]{:S(2)}, u32[]{:S(2)}) collective-permute-start(bf16[256,128]{1,0:T(8,128)(2,1)} %get-tuple-element.51.refs_2_), channel_id=1, source_target_pairs={{0,4},{1,5},{2,6},{3,7},{4,0},{5,1},{6,2},{7,3},{8,12},{9,13},{10,... | collective-permute-start | bytes 196616 | tf_op jit(solution)/shard_map/ppermute | solution.py:418
  50.7 8.1 %collective-permute-start.13 = (bf16[256,128]{1,0:T(8,128)(2,1)}, bf16[256,128]{1,0:T(8,128)(2,1)S(1)}, u32[]{:S(2)}, u32[]{:S(2)}) collective-permute-start(bf16[256,128]{1,0:T(8,128)(2,1)} %get-tuple-element.51.refs_2_), channel_id=1, source_target_pairs={{0,2},{1,3},{2,0},{3,1},{4,6},{5,7},{6,4},{7,5},{8,10},{9,11},{10,... | collective-permute-start | bytes 196616 | tf_op jit(solution)/shard_map/ppermute | solution.py:418
  58.9 7.8 %collective-permute-start.22 = (bf16[144,1024]{1,0:T(8,128)(2,1)S(1)}, bf16[144,1024]{1,0:T(8,128)(2,1)S(1)}, u32[]{:S(2)}, u32[]{:S(2)}) collective-permute-start(bf16[144,1024]{1,0:T(8,128)(2,1)S(1)} %get-tuple-element.60), channel_id=1, source_target_pairs={{0,16},{8,24},{16,0},{24,8},{1,17},{9,25},{17,1},{25,9},{2,18},{10... | collective-permute-start | bytes 884744 | tf_op jit(solution)/shard_map/ppermute | solution.py:418
  72.5 17.1 %collective-permute-start.19 = (bf16[144,1152]{1,0:T(8,128)(2,1)S(1)}, bf16[144,1152]{1,0:T(8,128)(2,1)S(1)}, u32[]{:S(2)}, u32[]{:S(2)}) collective-permute-start(bf16[144,1152]{1,0:T(8,128)(2,1)S(1)} %get-tuple-element.57), channel_id=1, source_target_pairs={{0,8},{8,0},{16,24},{24,16},{1,9},{9,1},{17,25},{25,17},{2,10},{10... | collective-permute-start | bytes 995336 | tf_op jit(solution)/shard_map/ppermute | solution.py:418
  74.7 16.0 %collective-permute-start.20 = (bf16[144,1152]{1,0:T(8,128)(2,1)S(1)}, bf16[144,1152]{1,0:T(8,128)(2,1)S(1)}, u32[]{:S(2)}, u32[]{:S(2)}) collective-permute-start(bf16[144,1152]{1,0:T(8,128)(2,1)S(1)} %get-tuple-element.58), channel_id=1, source_target_pairs={{0,16},{8,24},{16,0},{24,8},{1,17},{9,25},{17,1},{25,9},{2,18},{10... | collective-permute-start | bytes 995336 | tf_op jit(solution)/shard_map/ppermute | solution.py:418
  79.5 13.1 %collective-permute-start.23 = (bf16[144,1024]{1,0:T(8,128)(2,1)S(1)}, bf16[144,1024]{1,0:T(8,128)(2,1)S(1)}, u32[]{:S(2)}, u32[]{:S(2)}) collective-permute-start(bf16[144,1024]{1,0:T(8,128)(2,1)S(1)} %get-tuple-element.61), channel_id=1, source_target_pairs={{0,8},{8,0},{16,24},{24,16},{1,9},{9,1},{17,25},{25,17},{2,10},{10... | collective-permute-start | bytes 884744 | tf_op jit(solution)/shard_map/ppermute | solution.py:418
  81.0 26.7 %collective-permute-start.24 = (bf16[144,1024]{1,0:T(8,128)(2,1)S(1)}, bf16[144,1024]{1,0:T(8,128)(2,1)S(1)}, u32[]{:S(2)}, u32[]{:S(2)}) collective-permute-start(bf16[144,1024]{1,0:T(8,128)(2,1)S(1)} %get-tuple-element.62), channel_id=1, source_target_pairs={{0,16},{8,24},{16,0},{24,8},{1,17},{9,25},{17,1},{25,9},{2,18},{10... | collective-permute-start | bytes 884744 | tf_op jit(solution)/shard_map/ppermute | solution.py:418
  81.0 33.5 %collective-permute-start.27 = (bf16[144,1152]{1,0:T(8,128)(2,1)S(1)}, bf16[144,1152]{1,0:T(8,128)(2,1)S(1)}, u32[]{:S(2)}, u32[]{:S(2)}) collective-permute-start(bf16[144,1152]{1,0:T(8,128)(2,1)S(1)} %get-tuple-element.65), channel_id=1, source_target_pairs={{0,24},{8,16},{16,8},{24,0},{1,25},{9,17},{17,9},{25,1},{2,26},{10... | collective-permute-start | bytes 995336 | tf_op jit(solution)/shard_map/ppermute | solution.py:418
  89.7 24.9 %collective-permute-start.28 = (bf16[144,1024]{1,0:T(8,128)(2,1)S(1)}, bf16[144,1024]{1,0:T(8,128)(2,1)S(1)}, u32[]{:S(2)}, u32[]{:S(2)}) collective-permute-start(bf16[144,1024]{1,0:T(8,128)(2,1)S(1)} %get-tuple-element.66), channel_id=1, source_target_pairs={{0,24},{8,16},{16,8},{24,0},{1,25},{9,17},{17,9},{25,1},{2,26},{10... | collective-permute-start | bytes 884744 | tf_op jit(solution)/shard_map/ppermute | solution.py:418
  90.7 23.9 %collective-permute-start.29 = (bf16[144,1024]{1,0:T(8,128)(2,1)S(1)}, bf16[144,1024]{1,0:T(8,128)(2,1)S(1)}, u32[]{:S(2)}, u32[]{:S(2)}) collective-permute-start(bf16[144,1024]{1,0:T(8,128)(2,1)S(1)} %get-tuple-element.67), channel_id=1, source_target_pairs={{0,24},{8,16},{16,8},{24,0},{1,25},{9,17},{17,9},{25,1},{2,26},{10... | collective-permute-start | bytes 884744 | tf_op jit(solution)/shard_map/ppermute | solution.py:418
  113.3 8.8 %collective-permute-start.26 = (bf16[144,1024]{1,0:T(8,128)(2,1)S(1)}, bf16[144,1024]{1,0:T(8,128)(2,1)S(1)}, u32[]{:S(2)}, u32[]{:S(2)}) collective-permute-start(bf16[144,1024]{1,0:T(8,128)(2,1)S(1)} %get-tuple-element.64), channel_id=1, source_target_pairs={{0,16},{8,24},{16,0},{24,8},{1,17},{9,25},{17,1},{25,9},{2,18},{10... | collective-permute-start | bytes 884744 | tf_op jit(solution)/shard_map/ppermute | solution.py:418
  113.5 11.0 %collective-permute-start.25 = (bf16[144,1024]{1,0:T(8,128)(2,1)S(1)}, bf16[144,1024]{1,0:T(8,128)(2,1)S(1)}, u32[]{:S(2)}, u32[]{:S(2)}) collective-permute-start(bf16[144,1024]{1,0:T(8,128)(2,1)S(1)} %get-tuple-element.63.refs_11_), channel_id=1, source_target_pairs={{0,8},{8,0},{16,24},{24,16},{1,9},{9,1},{17,25},{25,17},{2,10},{10... | collective-permute-start | bytes 884744 | tf_op jit(solution)/shard_map/ppermute | solution.py:418
  118.5 7.8 %collective-permute-start.30 = (bf16[144,1024]{1,0:T(8,128)(2,1)S(1)}, bf16[144,1024]{1,0:T(8,128)(2,1)S(1)}, u32[]{:S(2)}, u32[]{:S(2)}) collective-permute-start(bf16[144,1024]{1,0:T(8,128)(2,1)S(1)} %get-tuple-element.68), channel_id=1, source_target_pairs={{0,24},{8,16},{16,8},{24,0},{1,25},{9,17},{17,9},{25,1},{2,26},{10... | collective-permute-start | bytes 884744 | tf_op jit(solution)/shard_map/ppermute | solution.py:418
  120.8 9.1 %collective-permute-start.34 = (bf16[144,1024]{1,0:T(8,128)(2,1)S(1)}, bf16[144,1024]{1,0:T(8,128)(2,1)S(1)}, u32[]{:S(2)}, u32[]{:S(2)}) collective-permute-start(bf16[144,1024]{1,0:T(8,128)(2,1)S(1)} %get-tuple-element.74), channel_id=1, source_target_pairs={{0,8},{8,0},{16,24},{24,16},{1,9},{9,1},{17,25},{25,17},{2,10},{10... | collective-permute-start | bytes 884744 | tf_op jit(solution)/shard_map/ppermute | solution.py:418
  120.8 10.6 %collective-permute-start.35 = (bf16[144,1024]{1,0:T(8,128)(2,1)S(1)}, bf16[144,1024]{1,0:T(8,128)(2,1)S(1)}, u32[]{:S(2)}, u32[]{:S(2)}) collective-permute-start(bf16[144,1024]{1,0:T(8,128)(2,1)S(1)} %get-tuple-element.75), channel_id=1, source_target_pairs={{0,16},{8,24},{16,0},{24,8},{1,17},{9,25},{17,1},{25,9},{2,18},{10... | collective-permute-start | bytes 884744 | tf_op jit(solution)/shard_map/ppermute | solution.py:418
  122.1 10.4 %collective-permute-start.36 = (bf16[144,1024]{1,0:T(8,128)(2,1)S(1)}, bf16[144,1024]{1,0:T(8,128)(2,1)S(1)}, u32[]{:S(2)}, u32[]{:S(2)}) collective-permute-start(bf16[144,1024]{1,0:T(8,128)(2,1)S(1)} %get-tuple-element.76), channel_id=1, source_target_pairs={{0,24},{8,16},{16,8},{24,0},{1,25},{9,17},{17,9},{25,1},{2,26},{10... | collective-permute-start | bytes 884744 | tf_op jit(solution)/shard_map/ppermute | solution.py:418
  127.0 9.1 %collective-permute-start.31 = (bf16[64,1024]{1,0:T(8,128)(2,1)S(1)}, bf16[64,1024]{1,0:T(8,128)(2,1)S(1)}, u32[]{:S(2)}, u32[]{:S(2)}) collective-permute-start(bf16[64,1024]{1,0:T(8,128)(2,1)S(1)} %get-tuple-element.70), channel_id=1, source_target_pairs={{0,2},{1,3},{2,0},{3,1},{4,6},{5,7},{6,4},{7,5},{8,10},{9,11},{10,... | collective-permute-start | bytes 393224 | tf_op jit(solution)/shard_map/ppermute | solution.py:418
  127.1 10.6 %collective-permute-start.32 = (bf16[64,1024]{1,0:T(8,128)(2,1)S(1)}, bf16[64,1024]{1,0:T(8,128)(2,1)S(1)}, u32[]{:S(2)}, u32[]{:S(2)}) collective-permute-start(bf16[64,1024]{1,0:T(8,128)(2,1)S(1)} %get-tuple-element.71), channel_id=1, source_target_pairs={{0,4},{1,5},{2,6},{3,7},{4,0},{5,1},{6,2},{7,3},{8,12},{9,13},{10,... | collective-permute-start | bytes 393224 | tf_op jit(solution)/shard_map/ppermute | solution.py:418
  129.8 7.9 %collective-permute-start.33 = (bf16[64,1024]{1,0:T(8,128)(2,1)S(1)}, bf16[64,1024]{1,0:T(8,128)(2,1)S(1)}, u32[]{:S(2)}, u32[]{:S(2)}) collective-permute-start(bf16[64,1024]{1,0:T(8,128)(2,1)S(1)} %get-tuple-element.72), channel_id=1, source_target_pairs={{0,6},{1,7},{2,4},{3,5},{4,2},{5,3},{6,0},{7,1},{8,14},{9,15},{10,... | collective-permute-start | bytes 393224 | tf_op jit(solution)/shard_map/ppermute | solution.py:418
  134.8 8.7 %collective-permute-start.38 = (bf16[64,1024]{1,0:T(8,128)(2,1)S(1)}, bf16[64,1024]{1,0:T(8,128)(2,1)S(1)}, u32[]{:S(2)}, u32[]{:S(2)}) collective-permute-start(bf16[64,1024]{1,0:T(8,128)(2,1)S(1)} %get-tuple-element.79), channel_id=1, source_target_pairs={{0,4},{1,5},{2,6},{3,7},{4,0},{5,1},{6,2},{7,3},{8,12},{9,13},{10,... | collective-permute-start | bytes 393224 | tf_op jit(solution)/shard_map/ppermute | solution.py:418
  136.1 7.3 %collective-permute-start.39 = (bf16[64,1024]{1,0:T(8,128)(2,1)S(1)}, bf16[64,1024]{1,0:T(8,128)(2,1)S(1)}, u32[]{:S(2)}, u32[]{:S(2)}) collective-permute-start(bf16[64,1024]{1,0:T(8,128)(2,1)S(1)} %get-tuple-element.80), channel_id=1, source_target_pairs={{0,6},{1,7},{2,4},{3,5},{4,2},{5,3},{6,0},{7,1},{8,14},{9,15},{10,... | collective-permute-start | bytes 393224 | tf_op jit(solution)/shard_map/ppermute | solution.py:418
  (29 other events, 423.3 us)
where the time goes:
time: 145 us; the launch traced here: 144 us
  starting transfers between devices  58.5 us (40%)
  waiting for transfers between devices  45.2 us (31%)
  Pallas kernels  29.3 us (20%)
  local copies, waits for them, and re-layouts  10.2 us (7%)
    ppermute x40, starting transfers between devices, swap(): return lax.ppermute(v, axis, [(i, i ^ k) for i in range(size)])  58.5 us
    ppermute x40, waiting for transfers between devices, swap(): return lax.ppermute(v, axis, [(i, i ^ k) for i in range(size)])  45.2 us
    pallas_call x12, Pallas kernels, call(): pl.pallas_call(kernel, out_shape=outs, in_specs=[VM] * count + [ANY] * le...  29.3 us
    unnamed x42, local copies, waits for them, and re-layouts  10.2 us
  transfers between devices with their start and end apart: 40, of which 14 were waited for; matrix products, arithmetic and copies ran while one was open for 0% of the time, Pallas kernels for 18%

commit v1 on v0

--- a/solution.py
+++ b/solution.py
@@ -16,7 +16,9 @@
 QK = 96
 LANES = 128
 COL_CHUNKS = 2
+APART = 4
 ROOM = 60
+ATTEND_ROOM = 44
 
 
 epsilon = 1e-06
@@ -66,8 +68,9 @@
 
 def prep_kernel(
     heads, lat, rot, lat_gain, key_up, value_up, queries, q_gain, k_gain, inner, first,
-    selq, selk, selg, bundle, q1, q2,
+    selq, selk, selg, routes, route_weights, residual, flags, bundle, q1, q2, head, rest,
 ):
+    pack_rows(routes, route_weights, residual, flags, head, rest)
     rows = lat.shape[0]
     pack = LANES // (ROPE * heads)
     sub = rows // pack
@@ -190,29 +193,17 @@
         state[h] = jnp.where(row == 0, peak, jnp.where(row == 1, total, part))
 
 
-def attend_first_kernel(heads, sources, q1, q2, *refs):
-    bundles, state = refs[: len(sources)], refs[-1]
-    me = lax.axis_index("sp")
-    attend_own(heads, q1, q2, bundles[0], state)
-    for i, k in enumerate(sources):
-        if k:
-
-            @pl.when((me ^ k) < me)
-            def _():
-                attend_other(heads, q1, q2, bundles[i], state)
-
-
-def attend_last_kernel(heads, tokens, groups, sources, q1, q2, before, *refs):
-    bundles = refs[: len(sources)]
-    keep, send, state, result = refs[len(sources) :]
+def attend_kernel(heads, tokens, groups, q1, q2, *refs):
+    bundles = refs[:-4]
+    keep, send, state, result = refs[-4:]
     me = lax.axis_index("sp")
     core = lax.axis_index("tp") % 2
-    state[...] = before[...]
-    for i, k in enumerate(sources):
+    attend_own(heads, q1, q2, bundles[0], state)
+    for k in range(1, len(bundles)):
 
         @pl.when((me ^ k) < me)
         def _():
-            attend_other(heads, q1, q2, bundles[i], state)
+            attend_other(heads, q1, q2, bundles[k], state)
 
     outs = [state[h, NOPE:, :] / state[h, 1:2, :] for h in range(heads)]
     result[...] = (outs[0] if heads == 1 else jnp.concatenate(outs, axis=0)).T
@@ -226,7 +217,7 @@
         ].astype(bf16)
 
 
-def pack_kernel(routes, weights, residual, flags, first, second):
+def pack_rows(routes, weights, residual, flags, first, second):
     half = second.shape[1]
     rows = [routes[...].astype(f32)]
     for j in range(TOPK):
@@ -248,7 +239,6 @@
     half = width - LANES
     slots = outs[0].shape[0]
     me = lax.axis_index("sp")
-    z = lax.axis_index("tp") // 2
     for g in range(groups):
         everything[g * tokens : (g + 1) * tokens, :] = parts[g][...]
     ticket = everything[:, half:].astype(f32)
@@ -258,7 +248,7 @@
     named = me ^ lane
     hit = ((route[0] == named) | (route[1] == named)) & (lane < sp)
     rank = dot(lower[...], hit.astype(f32).astype(bf16)).astype(jnp.int32)
-    slot = jnp.where(hit, rank + (z ^ (row // tokens)) * cap, -1)
+    slot = jnp.where(hit, rank + (row // tokens) * cap, -1)
     named = me ^ (lane // 3)
     tail = jnp.zeros(ticket.shape, f32)
     for j in range(TOPK):
@@ -314,12 +304,15 @@
 
 
 def expert_kernel(
-    part, chunks, own, out_weight, ffn_gain, gate_a, up_a, down_a, gate_b, up_b, down_b, *refs
+    part, chunks, own, cap, carried, out_weight, ffn_gain, gate_a, up_a, down_a, gate_b, up_b, down_b, *refs
 ):
     count = len(part)
     resids, seconds, norms = refs[:count], refs[count : 2 * count], refs[2 * count : 3 * count]
-    outs = refs[-count * chunks - (1 if own else 0) :]
     slots = resids[0].shape[0]
+    groups = slots // cap
+    results = count * chunks + groups + (1 if own else 0)
+    outs, apart = refs[-results:], refs[-results:][count * chunks :][:groups]
+    brought = refs[-results - groups : -results] if carried else ()
     total = count * slots
     half = seconds[0].shape[1]
     resid_rows = [jnp.concatenate([r[:, :half], t[...]], axis=1) for r, t in zip(resids, seconds)]
@@ -352,13 +345,39 @@
         out = (out * weight).astype(bf16)
         for i in range(count):
             outs[i * chunks + j][...] = out[i * slots : (i + 1) * slots]
-
-
-def combine_kernel(sources, tokens, table, *refs):
+    out = dot(hiddens[0], down_a[0, :, chunks * chunk :])
+    out = (out + dot(hiddens[1], down_b[0, :, chunks * chunk :])) * weight
+    for g in range(groups):
+        pieces = [out[i * slots + g * cap : i * slots + (g + 1) * cap] for i in range(count)]
+        if carried:
+            pieces = [brought[g][...].astype(f32)] + pieces
+        apart[g][...] = join(pieces).astype(bf16)
+
+
+def sum_kernel(groups, cap, *refs):
+    parts, outs = refs[:groups], refs[groups:]
+    total = parts[0][...].astype(f32)
+    for part in parts[1:]:
+        total = total + part[...].astype(f32)
+    for i, out in enumerate(outs):
+        out[...] = total[i * cap : (i + 1) * cap].astype(bf16)
+
+
+def finish_kernel(sp, tokens, cap, table, middle, *refs):
+    rows, out = refs[:sp], refs[sp]
+    width = out.shape[1]
+    total = middle[:, middle.shape[1] - width :]
+    for k in range(sp):
+        total = total + dot(table[k, :tokens, :cap], rows[k][...])
+    out[...] = total.astype(bf16)
+
+
+def combine_kernel(sources, tokens, place, chunk, table, *refs):
     rows, outs = refs[:sources], refs[sources:]
     total = None
     for k in range(sources):
-        part = dot(table[k], rows[k][...])
+        at = 0 if rows[k].shape[1] == chunk else place * chunk
+        part = dot(table[k], rows[k][:, at : at + chunk])
         total = part if total is None else total + part
     for g, out in enumerate(outs):
         out[...] = total[g * tokens : (g + 1) * tokens].astype(out.dtype)
@@ -368,7 +387,7 @@
 ANY = pl.BlockSpec(memory_space=pl.ANY)
 
 
-def call(body, args, outs, scratch=(), after=(), flops=0, trans=0, inside=(), room=32):
+def call(body, args, outs, scratch=(), after=(), flops=0, trans=0, room=32):
     size = lambda a: int(np.prod(a.shape)) * a.dtype.itemsize
     count = len(args)
     after = list(after)
@@ -376,10 +395,6 @@
     def kernel(*refs):
         body(*refs[:count], *refs[count + len(after) :])
 
-    held = [
-        pltpu.with_memory_space_constraint(a, pltpu.VMEM) if i in inside else a
-        for i, a in enumerate(args)
-    ]
     return pl.pallas_call(
         kernel,
         out_shape=outs,
@@ -392,7 +407,7 @@
             bytes_accessed=sum(map(size, args)) + sum(map(size, jax.tree.leaves(outs))),
         ),
         compiler_params=pltpu.CompilerParams(vmem_limit_bytes=room * 1024 * 1024),
-    )(*held, *after)
+    )(*args, *after)
 
 
 def shape(dims, dtype):
@@ -417,6 +432,9 @@
     def swap(v, axis, k, size):
         return lax.ppermute(v, axis, [(i, i ^ k) for i in range(size)])
 
+    def gather_z(v):
+        return [v] + [swap_z(v, k) for k in range(1, groups)]
+
     swap_core = lambda v: swap(v, "tp", 1, tp)
     swap_z = lambda v, k: swap(v, "tp", 2 * k, tp)
     swap_sp = lambda v, k: swap(v, "sp", k, sp)
@@ -428,34 +446,30 @@
         ordinal[:, None] // tokens == ordinal[None, :] // tokens
     )
     lower = jnp.asarray(lower.astype(np.float32), bf16)
-    first_half, second_half = call(
-        pack_kernel,
-        [routes.T, route_weights.T, residual, jnp.asarray(flags, bf16)],
-        (shape((tokens, width // 2 + LANES), bf16), shape((tokens, width // 2), bf16)),
-        room=ROOM,
-    )
-    first_parts = [first_half] + [swap_z(first_half, k) for k in range(1, groups)]
-    second_parts = [second_half] + [swap_z(second_half, k) for k in range(1, groups)]
-
     pack = LANES // (ROPE * heads)
     inner, first = turn_tables(rows, sp)
     selk = jnp.asarray(np.concatenate(rope_select(0, ROPE), axis=1), bf16)
     selq = jnp.asarray(head_select(heads), bf16)
     selg = jnp.asarray(np.abs(head_select(1)), f32)
-    bundle, q1, q2 = call(
+    bundle, q1, q2, first_half, second_half = call(
         functools.partial(prep_kernel, heads),
         [
             latent, rot_key.T, latent_gain[None, :], key_up, value_up, queries.T,
             query_gain[None, :], key_gain[None, :], inner, first, selq, selk, selg,
+            routes.T, route_weights.T, residual, jnp.asarray(flags, bf16),
         ],
         (
             shape((heads * rows + rows // pack, LANES), bf16),
             shape((heads, rows, LANES), bf16),
             shape((heads * pack, rows, LANES), bf16),
+            shape((tokens, width // 2 + LANES), bf16),
+            shape((tokens, width // 2), bf16),
         ),
         flops=2 * rows * latent.shape[1] * 256 + 2 * rows * 192 * 768,
         room=ROOM,
     )
+    first_parts = gather_z(first_half)
+    second_parts = gather_z(second_half)
     bundles = [bundle] + [swap_sp(bundle, k) for k in range(1, sp)]
 
     gate_b = swap_core(expert_gate)
@@ -472,24 +486,14 @@
     first_in = [first_rows[0]] + [swap_sp(first_rows[k], k) for k in range(1, sp)]
 
     half = heads * VH
-    split = min(3, sp)
-    early, late = list(range(split)), list(range(split, sp))
-    state = call(
-        functools.partial(attend_first_kernel, heads, early),
-        [q1, q2] + [bundles[k] for k in early],
-        shape((heads, LANES, rows), f32),
-        room=ROOM,
-        flops=2 * heads * rows * rows * len(early) * 384,
-        trans=heads * rows * rows * len(early),
-    )
     keep, send = call(
-        functools.partial(attend_last_kernel, heads, tokens, groups, late),
-        [q1, q2, state] + [bundles[k] for k in late],
+        functools.partial(attend_kernel, heads, tokens, groups),
+        [q1, q2] + bundles,
         (shape((all_tokens, half), bf16), shape((all_tokens, half), bf16)),
         [pltpu.VMEM((heads, LANES, rows), f32), pltpu.VMEM((rows, half), f32)],
-        room=ROOM,
-        flops=2 * heads * rows * rows * len(late) * 384,
-        trans=heads * rows * rows * len(late),
+        room=ATTEND_ROOM,
+        flops=2 * heads * rows * rows * sp * 384,
+        trans=heads * rows * rows * sp,
     )
     second_rows = call(
         functools.partial(residual_second_kernel, groups),
@@ -500,11 +504,9 @@
     )
     second_in = [second_rows[0]] + [swap_sp(second_rows[k], k) for k in range(1, sp)]
     other = swap_core(send)
-    pieces = [keep, other]
-    kept_in = [swap_z(keep, k) for k in range(1, groups)]
-    other_in = [swap_z(other, k) for k in range(1, groups)]
-    for a, b in zip(kept_in, other_in):
-        pieces += [a, b]
+    pieces = []
+    for pair in zip(gather_z(keep), gather_z(other)):
+        pieces += pair
     *norm_rows, own_rows = call(
         functools.partial(choose_kernel, groups, tokens),
         [out_gain[None, :], table] + pieces,
@@ -515,15 +517,19 @@
     norm_in = [norm_rows[0]] + [swap_sp(norm_rows[k], k) for k in range(1, sp)]
 
     hidden = 2 * expert_gate.shape[2]
-    chunk = width // COL_CHUNKS
+    apart = width // APART
+    chunk = (width - apart) // COL_CHUNKS
     parts = expert_parts(sp)
-    served = [None] * sp
-    before = []
+    served, summed = [None] * sp, [None] * sp
+    before, carried = [], []
     for n, part in enumerate(parts):
-        extra_in = [residual, own_rows] if n == 0 else []
-        extra_out = (shape((tokens, width), f32),) if n == 0 else ()
+        own, last = n == 0, n == len(parts) - 1
+        extra_in = ([residual, own_rows] if own else []) + (carried if last and n else [])
+        extra_out = (shape((tokens, width), f32),) if own else ()
+        members = ([0] if last and n else []) + part
+        cuts = COL_CHUNKS if last else 1
         outs = call(
-            functools.partial(expert_kernel, part, COL_CHUNKS, n == 0),
+            functools.partial(expert_kernel, part, cuts, own, cap, bool(last and n)),
             [
                 out_weight, ffn_gain[None, :], expert_gate, expert_up, expert_down,
                 gate_b, up_b, down_b,
@@ -532,21 +538,32 @@
             + [second_in[k] for k in part]
             + [norm_in[k] for k in part]
             + extra_in,
-            tuple([shape((slots, chunk), bf16)] * (len(part) * COL_CHUNKS)) + extra_out,
+            tuple([shape((slots, chunk * COL_CHUNKS // cuts), bf16)] * (len(part) * cuts))
+            + tuple([shape((len(members) * cap, apart), bf16)] * groups)
+            + extra_out,
             after=before,
             flops=2 * len(part) * slots * width * (att_width + 3 * hidden),
-            inside=(0, 2, 3, 4, 5, 6, 7),
-        )
-        if n == 0:
-            middle = outs[-1]
+        )
         before = [outs[0]]
         for i, k in enumerate(part):
-            served[k] = outs[i * COL_CHUNKS : (i + 1) * COL_CHUNKS]
+            served[k] = [swap_sp(v, k) if k else v for v in outs[i * cuts : (i + 1) * cuts]]
+        split = outs[len(part) * cuts :][:groups]
+        if own:
+            middle = outs[-1]
+            carried = list(split)
+        if not own or last:
+            sums = call(
+                functools.partial(sum_kernel, groups, cap),
+                [split[0]] + [swap_z(split[k], k) for k in range(1, groups)],
+                tuple([shape((cap, apart), bf16)] * len(members)),
+            )
+            for k, v in zip(members, sums):
+                summed[k] = swap_sp(v, k) if k else v
     finished = []
     for j in range(COL_CHUNKS):
-        back = [served[0][j]] + [swap_sp(served[k][j], k) for k in range(1, sp)]
+        back = [v[min(j, len(v) - 1)] for v in served]
         own, *rest = call(
-            functools.partial(combine_kernel, sp, tokens),
+            functools.partial(combine_kernel, sp, tokens, j, chunk),
             [table] + back,
             (shape((tokens, chunk), f32),) + tuple([shape((tokens, chunk), bf16)] * (groups - 1)),
             flops=2 * all_tokens * sp * slots * chunk,
@@ -555,6 +572,13 @@
         for k in range(1, groups):
             total = total + swap_z(rest[k - 1], k).astype(f32)
         finished.append(total.astype(bf16))
+    finished.append(
+        call(
+            functools.partial(finish_kernel, sp, tokens, cap),
+            [table, middle] + summed,
+            shape((tokens, apart), bf16),
+        )
+    )
     return jnp.concatenate(finished, axis=1)
 
 

time: 145 us -> 173 us (1.19)
  waiting for transfers between devices: 45.2 us -> 88 us
  Pallas kernels: 29.3 us -> 17.6 us
  local copies, waits for them, and re-layouts: 10.2 us -> 4.96 us
  starting transfers between devices: 58.5 us -> 60.8 us
    ppermute x40 -> x47, waiting for transfers between devices: 45.2 us -> 88 us  [swap(): return lax.ppermute(v, axis, [(i, i ^ k) for i in range(size)])]
    pallas_call x12 -> x13, Pallas kernels: 29.3 us -> 17.6 us  [call(): pl.pallas_call(kernel, out_shape=outs, in_specs=[VM] * count + [ANY] * le...]
    unnamed x42 -> x26, local copies, waits for them, and re-layouts: 10.2 us -> 4.96 us
    ppermute x40 -> x47, starting transfers between devices: 58.5 us -> 60.8 us  [swap(): return lax.ppermute(v, axis, [(i, i ^ k) for i in range(size)])]
  transfers between devices with their start and end apart: 40 -> 47, of which waited for: 14 -> 20; matrix products, arithmetic and copies ran while one was open for 0% -> 0% of each run, Pallas kernels for 18% -> 8%
where the time goes in v1:
time: 173 us; the launch traced here: 172 us
  waiting for transfers between devices  88 us (51%)
  starting transfers between devices  60.8 us (35%)
  Pallas kernels  17.6 us (10%)
  local copies, waits for them, and re-layouts  4.96 us (3%)
    ppermute x47, waiting for transfers between devices, swap(): return lax.ppermute(v, axis, [(i, i ^ k) for i in range(size)])  88 us
    ppermute x47, starting transfers between devices, swap(): return lax.ppermute(v, axis, [(i, i ^ k) for i in range(size)])  60.8 us
    pallas_call x13, Pallas kernels, call(): pl.pallas_call(kernel, out_shape=outs, in_specs=[VM] * count + [ANY] * le...  17.6 us
    unnamed x26, local copies, waits for them, and re-layouts  4.96 us
  transfers between devices with their start and end apart: 47, of which 20 were waited for; matrix products, arithmetic and copies ran while one was open for 0% of the time, Pallas kernels for 8%

profile of v1, /device:TPU:0, one launch (start us, length us, event | category | flops | bytes accessed | tf_op | source)
XLA Modules:
  0.0 172.4 jit_solution(13981550142689190040)
XLA Ops:
  0.0 4.0 %shard_map.226 = (bf16[1280,128]{1,0:T(8,128)(2,1)}, bf16[2,512,128]{2,1,0:T(8,128)(2,1)}, bf16[4,512,128]{2,1,0:T(8,128)(2,1)}, bf16[64,1152]{1,0:T(8,128)(2,1)}, bf16[64,1024]{1,0:T(8,128)(2,1)}) custom-call(bf16[512,512]{1,0:T(8,128)(2,1)} %refs_0_.5, bf16[32,512]{1,0:T(8,128)(2,1)} %bitcast.14, f32[1,512]{1,0:T(1,128)} %bitcast.15, ...), custom_call_target="tpu_custom_call" | custom-call | flops 285212672 | bytes 3663616 | tf_op jit(solution)/shard_map/pallas_call | solution.py:398
  4.0 4.0 %collective-permute-start.11 = (bf16[1280,128]{1,0:T(8,128)(2,1)}, bf16[1280,128]{1,0:T(8,128)(2,1)S(1)}, u32[]{:S(2)}, u32[]{:S(2)}) collective-permute-start(bf16[1280,128]{1,0:T(8,128)(2,1)} %get-tuple-element.63.refs_2_), channel_id=1, source_target_pairs={{0,24},{8,16},{16,8},{24,0},{1,25},{9,17},{17,9},{25,1},{2,26},{10... | collective-permute-start | bytes 983048 | tf_op jit(solution)/shard_map/ppermute | solution.py:433
  8.0 3.6 %collective-permute-start.8 = (bf16[64,1024]{1,0:T(8,128)(2,1)}, bf16[64,1024]{1,0:T(8,128)(2,1)S(1)}, u32[]{:S(2)}, u32[]{:S(2)}) collective-permute-start(bf16[64,1024]{1,0:T(8,128)(2,1)} %get-tuple-element.59.refs_1_), channel_id=1, source_target_pairs={{0,6},{1,7},{2,4},{3,5},{4,2},{5,3},{6,0},{7,1},{8,14},{9,15},{10,... | collective-permute-start | bytes 393224 | tf_op jit(solution)/shard_map/ppermute | solution.py:433
  12.6 2.1 %collective-permute-start.4 = (bf16[64,1152]{1,0:T(8,128)(2,1)}, bf16[64,1152]{1,0:T(8,128)(2,1)S(1)}, u32[]{:S(2)}, u32[]{:S(2)}) collective-permute-start(bf16[64,1152]{1,0:T(8,128)(2,1)} %get-tuple-element.56.refs_1_), channel_id=1, source_target_pairs={{0,4},{1,5},{2,6},{3,7},{4,0},{5,1},{6,2},{7,3},{8,12},{9,13},{10,... | collective-permute-start | bytes 442376 | tf_op jit(solution)/shard_map/ppermute | solution.py:433
  15.8 17.2 %collective-permute-done.7.refs_3_ = bf16[64,1024]{1,0:T(8,128)(2,1)S(1)} collective-permute-done((bf16[64,1024]{1,0:T(8,128)(2,1)}, bf16[64,1024]{1,0:T(8,128)(2,1)S(1)}, u32[]{:S(2)}, u32[]{:S(2)}) %collective-permute-start.7) | collective-permute-done | bytes 131104 | tf_op jit(solution)/shard_map/ppermute | solution.py:433
  36.2 8.0 %collective-permute-done.10.refs_4_ = bf16[1280,128]{1,0:T(8,128)(2,1)S(1)} collective-permute-done((bf16[1280,128]{1,0:T(8,128)(2,1)}, bf16[1280,128]{1,0:T(8,128)(2,1)S(1)}, u32[]{:S(2)}, u32[]{:S(2)}) %collective-permute-start.10) | collective-permute-done | bytes 327712 | tf_op jit(solution)/shard_map/ppermute | solution.py:433
  56.3 2.2 %collective-permute-start.17 = (bf16[256,128]{1,0:T(8,128)(2,1)S(1)}, bf16[256,128]{1,0:T(8,128)(2,1)S(1)}, u32[]{:S(2)}, u32[]{:S(2)}) collective-permute-start(bf16[256,128]{1,0:T(8,128)(2,1)S(1)} %get-tuple-element.64.refs_2_), channel_id=1, source_target_pairs={{0,6},{1,7},{2,4},{3,5},{4,2},{5,3},{6,0},{7,1},{8,14},{9,15},{10,... | collective-permute-start | bytes 196616 | tf_op jit(solution)/shard_map/ppermute | solution.py:433
  58.5 3.9 %collective-permute-done.17.refs_8_ = bf16[256,128]{1,0:T(8,128)(2,1)S(1)} collective-permute-done((bf16[256,128]{1,0:T(8,128)(2,1)S(1)}, bf16[256,128]{1,0:T(8,128)(2,1)S(1)}, u32[]{:S(2)}, u32[]{:S(2)}) %collective-permute-start.17) | collective-permute-done | bytes 65568 | tf_op jit(solution)/shard_map/ppermute | solution.py:433
  62.4 5.2 %collective-permute-done.15.refs_6_ = bf16[256,128]{1,0:T(8,128)(2,1)S(1)} collective-permute-done((bf16[256,128]{1,0:T(8,128)(2,1)S(1)}, bf16[256,128]{1,0:T(8,128)(2,1)S(1)}, u32[]{:S(2)}, u32[]{:S(2)}) %collective-permute-start.15) | collective-permute-done | bytes 65568 | tf_op jit(solution)/shard_map/ppermute | solution.py:433
  67.6 4.3 %collective-permute-done.13.refs_4_ = bf16[256,128]{1,0:T(8,128)(2,1)S(1)} collective-permute-done((bf16[256,128]{1,0:T(8,128)(2,1)S(1)}, bf16[256,128]{1,0:T(8,128)(2,1)S(1)}, u32[]{:S(2)}, u32[]{:S(2)}) %collective-permute-start.13) | collective-permute-done | bytes 65568 | tf_op jit(solution)/shard_map/ppermute | solution.py:433
  71.8 2.2 %collective-permute-start.18 = (bf16[256,128]{1,0:T(8,128)(2,1)S(1)}, bf16[256,128]{1,0:T(8,128)(2,1)S(1)}, u32[]{:S(2)}, u32[]{:S(2)}) collective-permute-start(bf16[256,128]{1,0:T(8,128)(2,1)S(1)} %collective-permute-done.12.refs_3_), channel_id=1, source_target_pairs={{0,6},{1,7},{2,4},{3,5},{4,2},{5,3},{6,0},{7,1},{8,14},{9,15},{10,... | collective-permute-start | bytes 196616 | tf_op jit(solution)/shard_map/ppermute | solution.py:433
  74.0 3.9 %collective-permute-done.18.refs_9_ = bf16[256,128]{1,0:T(8,128)(2,1)S(1)} collective-permute-done((bf16[256,128]{1,0:T(8,128)(2,1)S(1)}, bf16[256,128]{1,0:T(8,128)(2,1)S(1)}, u32[]{:S(2)}, u32[]{:S(2)}) %collective-permute-start.18) | collective-permute-done | bytes 65568 | tf_op jit(solution)/shard_map/ppermute | solution.py:433
  80.1 2.1 %collective-permute-done.14.refs_5_ = bf16[256,128]{1,0:T(8,128)(2,1)S(1)} collective-permute-done((bf16[256,128]{1,0:T(8,128)(2,1)S(1)}, bf16[256,128]{1,0:T(8,128)(2,1)S(1)}, u32[]{:S(2)}, u32[]{:S(2)}) %collective-permute-start.14) | collective-permute-done | bytes 65568 | tf_op jit(solution)/shard_map/ppermute | solution.py:433
  82.2 3.8 %collective-permute-start.20 = (bf16[144,1152]{1,0:T(8,128)(2,1)S(1)}, bf16[144,1152]{1,0:T(8,128)(2,1)S(1)}, u32[]{:S(2)}, u32[]{:S(2)}) collective-permute-start(bf16[144,1152]{1,0:T(8,128)(2,1)S(1)} %get-tuple-element.71), channel_id=1, source_target_pairs={{0,16},{8,24},{16,0},{24,8},{1,17},{9,25},{17,1},{25,9},{2,18},{10... | collective-permute-start | bytes 995336 | tf_op jit(solution)/shard_map/ppermute | solution.py:433
  87.4 2.0 %collective-permute-start.24 = (bf16[144,1024]{1,0:T(8,128)(2,1)S(1)}, bf16[144,1024]{1,0:T(8,128)(2,1)S(1)}, u32[]{:S(2)}, u32[]{:S(2)}) collective-permute-start(bf16[144,1024]{1,0:T(8,128)(2,1)S(1)} %get-tuple-element.75), channel_id=1, source_target_pairs={{0,16},{8,24},{16,0},{24,8},{1,17},{9,25},{17,1},{25,9},{2,18},{10... | collective-permute-start | bytes 884744 | tf_op jit(solution)/shard_map/ppermute | solution.py:433
  89.4 2.3 %shard_map.231 = (bf16[144,1536]{1,0:T(8,128)(2,1)S(1)}, bf16[36,512]{1,0:T(8,128)(2,1)S(1)}, bf16[36,512]{1,0:T(8,128)(2,1)S(1)}, bf16[36,512]{1,0:T(8,128)(2,1...) custom-call(bf16[1024,2048]{1,0:T(8,128)(2,1)S(1)} %copy-done, f32[1,2048]{1,0:T(1,128)S(1)} %bitcast.9, ...), custom_call_target="tpu_custom_call" | custom-call | flops 1509949440 | bytes 12922880 | tf_op jit(solution)/shard_map/pallas_call | solution.py:398
  91.7 15.6 %collective-permute-done.22.refs_11_ = bf16[144,1024]{1,0:T(8,128)(2,1)S(1)} collective-permute-done((bf16[144,1024]{1,0:T(8,128)(2,1)S(1)}, bf16[144,1024]{1,0:T(8,128)(2,1)S(1)}, u32[]{:S(2)}, u32[]{:S(2)}) %collective-permute-start.22) | collective-permute-done | bytes 294944 | tf_op jit(solution)/shard_map/ppermute | solution.py:433
  112.1 3.6 %shard_map.232 = (bf16[144,1536]{1,0:T(8,128)(2,1)S(1)}, bf16[144,1536]{1,0:T(8,128)(2,1)S(1)}, bf16[72,512]{1,0:T(8,128)(2,1)S(1)}, bf16[72,512]{1,0:T(8,128)(2...) custom-call(bf16[1024,2048]{1,0:T(8,128)(2,1)S(1)} %copy-done, f32[1,2048]{1,0:T(1,128)S(1)} %bitcast.10, ...), custom_call_target="tpu_custom_call" | custom-call | flops 3019898880 | bytes 13516800 | tf_op jit(solution)/shard_map/pallas_call | solution.py:398
  117.5 7.9 %collective-permute-done.28.refs_9_ = bf16[144,1024]{1,0:T(8,128)(2,1)S(1)} collective-permute-done((bf16[144,1024]{1,0:T(8,128)(2,1)S(1)}, bf16[144,1024]{1,0:T(8,128)(2,1)S(1)}, u32[]{:S(2)}, u32[]{:S(2)}) %collective-permute-start.28) | collective-permute-done | bytes 294944 | tf_op jit(solution)/shard_map/ppermute | solution.py:433
  125.3 5.3 %collective-permute-done.29.refs_10_ = bf16[144,1024]{1,0:T(8,128)(2,1)S(1)} collective-permute-done((bf16[144,1024]{1,0:T(8,128)(2,1)S(1)}, bf16[144,1024]{1,0:T(8,128)(2,1)S(1)}, u32[]{:S(2)}, u32[]{:S(2)}) %collective-permute-start.29) | collective-permute-done | bytes 294944 | tf_op jit(solution)/shard_map/ppermute | solution.py:433
  130.7 2.1 %shard_map.233 = (bf16[144,768]{1,0:T(8,128)(2,1)S(1)}, bf16[144,768]{1,0:T(8,128)(2,1)S(1)}, bf16[72,512]{1,0:T(8,128)(2,1)S(1)}, bf16[72,512]{1,0:T(8,128)(2,1...) custom-call(bf16[1024,2048]{1,0:T(8,128)(2,1)S(1)} %copy-done, f32[1,2048]{1,0:T(1,128)S(1)} %bitcast.11, ...), custom_call_target="tpu_custom_call" | custom-call | flops 1509949440 | bytes 12300288 | tf_op jit(solution)/shard_map/pallas_call | solution.py:398
  132.7 2.1 %collective-permute-start.34 = (bf16[144,768]{1,0:T(8,128)(2,1)S(1)}, bf16[144,768]{1,0:T(8,128)(2,1)S(1)}, u32[]{:S(2)}, u32[]{:S(2)}) collective-permute-start(bf16[144,768]{1,0:T(8,128)(2,1)S(1)} %get-tuple-element.90), channel_id=1, source_target_pairs={{0,24},{8,16},{16,8},{24,0},{1,25},{9,17},{17,9},{25,1},{2,26},{10... | collective-permute-start | bytes 663560 | tf_op jit(solution)/shard_map/ppermute | solution.py:433
  135.4 6.5 %collective-permute-start.42 = (bf16[72,512]{1,0:T(8,128)(2,1)S(1)}, bf16[72,512]{1,0:T(8,128)(2,1)S(1)}, u32[]{:S(2)}, u32[]{:S(2)}) collective-permute-start(bf16[72,512]{1,0:T(8,128)(2,1)S(1)} %get-tuple-element.102), channel_id=1, source_target_pairs={{0,4},{1,5},{2,6},{3,7},{4,0},{5,1},{6,2},{7,3},{8,12},{9,13},{10,... | collective-permute-start | bytes 221192 | tf_op jit(solution)/shard_map/ppermute | solution.py:433
  143.0 3.8 %collective-permute-done.42.refs_2_ = bf16[72,512]{1,0:T(8,128)(2,1)S(1)} collective-permute-done((bf16[72,512]{1,0:T(8,128)(2,1)S(1)}, bf16[72,512]{1,0:T(8,128)(2,1)S(1)}, u32[]{:S(2)}, u32[]{:S(2)}) %collective-permute-start.42) | collective-permute-done | bytes 73760 | tf_op jit(solution)/shard_map/ppermute | solution.py:433
  146.8 2.1 %collective-permute-start.43 = (bf16[72,512]{1,0:T(8,128)(2,1)S(1)}, bf16[72,512]{1,0:T(8,128)(2,1)S(1)}, u32[]{:S(2)}, u32[]{:S(2)}) collective-permute-start(bf16[72,512]{1,0:T(8,128)(2,1)S(1)} %get-tuple-element.103), channel_id=1, source_target_pairs={{0,6},{1,7},{2,4},{3,5},{4,2},{5,3},{6,0},{7,1},{8,14},{9,15},{10,... | collective-permute-start | bytes 221192 | tf_op jit(solution)/shard_map/ppermute | solution.py:433
  148.9 2.3 %collective-permute-start.39 = (bf16[72,512]{1,0:T(8,128)(2,1)S(1)}, bf16[72,512]{1,0:T(8,128)(2,1)S(1)}, u32[]{:S(2)}, u32[]{:S(2)}) collective-permute-start(bf16[72,512]{1,0:T(8,128)(2,1)S(1)} %get-tuple-element.97), channel_id=1, source_target_pairs={{0,4},{1,5},{2,6},{3,7},{4,0},{5,1},{6,2},{7,3},{8,12},{9,13},{10,... | collective-permute-start | bytes 221192 | tf_op jit(solution)/shard_map/ppermute | solution.py:433
  151.2 2.1 %collective-permute-start.40 = (bf16[72,512]{1,0:T(8,128)(2,1)S(1)}, bf16[72,512]{1,0:T(8,128)(2,1)S(1)}, u32[]{:S(2)}, u32[]{:S(2)}) collective-permute-start(bf16[72,512]{1,0:T(8,128)(2,1)S(1)} %get-tuple-element.98), channel_id=1, source_target_pairs={{0,6},{1,7},{2,4},{3,5},{4,2},{5,3},{6,0},{7,1},{8,14},{9,15},{10,... | collective-permute-start | bytes 221192 | tf_op jit(solution)/shard_map/ppermute | solution.py:433
  160.6 2.1 %collective-permute-start.37 = (bf16[64,768]{1,0:T(8,128)(2,1)S(1)}, bf16[64,768]{1,0:T(8,128)(2,1)S(1)}, u32[]{:S(2)}, u32[]{:S(2)}) collective-permute-start(bf16[64,768]{1,0:T(8,128)(2,1)S(1)} %get-tuple-element.94), channel_id=1, source_target_pairs={{0,6},{1,7},{2,4},{3,5},{4,2},{5,3},{6,0},{7,1},{8,14},{9,15},{10,... | collective-permute-start | bytes 294920 | tf_op jit(solution)/shard_map/ppermute | solution.py:433
  162.7 2.3 %collective-permute-start.32 = (bf16[64,768]{1,0:T(8,128)(2,1)S(1)}, bf16[64,768]{1,0:T(8,128)(2,1)S(1)}, u32[]{:S(2)}, u32[]{:S(2)}) collective-permute-start(bf16[64,768]{1,0:T(8,128)(2,1)S(1)} %get-tuple-element.88), channel_id=1, source_target_pairs={{0,4},{1,5},{2,6},{3,7},{4,0},{5,1},{6,2},{7,3},{8,12},{9,13},{10,... | collective-permute-start | bytes 294920 | tf_op jit(solution)/shard_map/ppermute | solution.py:433
  165.0 2.1 %collective-permute-start.33 = (bf16[64,768]{1,0:T(8,128)(2,1)S(1)}, bf16[64,768]{1,0:T(8,128)(2,1)S(1)}, u32[]{:S(2)}, u32[]{:S(2)}) collective-permute-start(bf16[64,768]{1,0:T(8,128)(2,1)S(1)} %get-tuple-element.89), channel_id=1, source_target_pairs={{0,6},{1,7},{2,4},{3,5},{4,2},{5,3},{6,0},{7,1},{8,14},{9,15},{10,... | collective-permute-start | bytes 294920 | tf_op jit(solution)/shard_map/ppermute | solution.py:433
  167.3 1.9 %collective-permute-done.31 = bf16[64,768]{1,0:T(8,128)(2,1)S(1)} collective-permute-done((bf16[64,768]{1,0:T(8,128)(2,1)S(1)}, bf16[64,768]{1,0:T(8,128)(2,1)S(1)}, u32[]{:S(2)}, u32[]{:S(2)}) %collective-permute-start.31) | collective-permute-done | bytes 98336 | tf_op jit(solution)/shard_map/ppermute | solution.py:433
  169.3 2.3 %collective-permute-done.33 = bf16[64,768]{1,0:T(8,128)(2,1)S(1)} collective-permute-done((bf16[64,768]{1,0:T(8,128)(2,1)S(1)}, bf16[64,768]{1,0:T(8,128)(2,1)S(1)}, u32[]{:S(2)}, u32[]{:S(2)}) %collective-permute-start.33) | collective-permute-done | bytes 98336 | tf_op jit(solution)/shard_map/ppermute | solution.py:433
  (103 shorter events, 37.5 us)
Async XLA Ops:
  4.0 31.7 %collective-permute-start.11 = (bf16[1280,128]{1,0:T(8,128)(2,1)}, bf16[1280,128]{1,0:T(8,128)(2,1)S(1)}, u32[]{:S(2)}, u32[]{:S(2)}) collective-permute-start(bf16[1280,128]{1,0:T(8,128)(2,1)} %get-tuple-element.63.refs_2_), channel_id=1, source_target_pairs={{0,24},{8,16},{16,8},{24,0},{1,25},{9,17},{17,9},{25,1},{2,26},{10... | collective-permute-start | bytes 983048 | tf_op jit(solution)/shard_map/ppermute | solution.py:433
  8.0 7.8 %collective-permute-start.8 = (bf16[64,1024]{1,0:T(8,128)(2,1)}, bf16[64,1024]{1,0:T(8,128)(2,1)S(1)}, u32[]{:S(2)}, u32[]{:S(2)}) collective-permute-start(bf16[64,1024]{1,0:T(8,128)(2,1)} %get-tuple-element.59.refs_1_), channel_id=1, source_target_pairs={{0,6},{1,7},{2,4},{3,5},{4,2},{5,3},{6,0},{7,1},{8,14},{9,15},{10,... | collective-permute-start | bytes 393224 | tf_op jit(solution)/shard_map/ppermute | solution.py:433
  11.6 21.4 %collective-permute-start.5 = (bf16[64,1152]{1,0:T(8,128)(2,1)}, bf16[64,1152]{1,0:T(8,128)(2,1)S(1)}, u32[]{:S(2)}, u32[]{:S(2)}) collective-permute-start(bf16[64,1152]{1,0:T(8,128)(2,1)} %get-tuple-element.56.refs_1_), channel_id=1, source_target_pairs={{0,6},{1,7},{2,4},{3,5},{4,2},{5,3},{6,0},{7,1},{8,14},{9,15},{10,... | collective-permute-start | bytes 442376 | tf_op jit(solution)/shard_map/ppermute | solution.py:433
  11.8 21.2 %collective-permute-start.7 = (bf16[64,1024]{1,0:T(8,128)(2,1)}, bf16[64,1024]{1,0:T(8,128)(2,1)S(1)}, u32[]{:S(2)}, u32[]{:S(2)}) collective-permute-start(bf16[64,1024]{1,0:T(8,128)(2,1)} %get-tuple-element.59.refs_1_), channel_id=1, source_target_pairs={{0,4},{1,5},{2,6},{3,7},{4,0},{5,1},{6,2},{7,3},{8,12},{9,13},{10,... | collective-permute-start | bytes 393224 | tf_op jit(solution)/shard_map/ppermute | solution.py:433
  12.6 22.6 %collective-permute-start.4 = (bf16[64,1152]{1,0:T(8,128)(2,1)}, bf16[64,1152]{1,0:T(8,128)(2,1)S(1)}, u32[]{:S(2)}, u32[]{:S(2)}) collective-permute-start(bf16[64,1152]{1,0:T(8,128)(2,1)} %get-tuple-element.56.refs_1_), channel_id=1, source_target_pairs={{0,4},{1,5},{2,6},{3,7},{4,0},{5,1},{6,2},{7,3},{8,12},{9,13},{10,... | collective-permute-start | bytes 442376 | tf_op jit(solution)/shard_map/ppermute | solution.py:433
  15.8 70.2 %collective-permute-start = (bf16[1,2048,256]{2,1,0:T(8,128)(2,1)}, bf16[1,2048,256]{2,1,0:T(8,128)(2,1)S(1)}, u32[]{:S(2)}, u32[]{:S(2)}) collective-permute-start(bf16[1,2048,256]{2,1,0:T(8,128)(2,1)} %refs_2_.5), channel_id=1, source_target_pairs={{0,1},{1,0},{2,3},{3,2},{4,5},{5,4},{6,7},{7,6},{8,9},{9,8},{10,11... | collective-permute-start | bytes 3145736 | tf_op jit(solution)/shard_map/ppermute | solution.py:433
  33.0 53.9 %collective-permute-start.1 = (bf16[1,2048,256]{2,1,0:T(8,128)(2,1)}, bf16[1,2048,256]{2,1,0:T(8,128)(2,1)S(1)}, u32[]{:S(2)}, u32[]{:S(2)}) collective-permute-start(bf16[1,2048,256]{2,1,0:T(8,128)(2,1)} %refs_3_.7), channel_id=1, source_target_pairs={{0,1},{1,0},{2,3},{3,2},{4,5},{5,4},{6,7},{7,6},{8,9},{9,8},{10,11... | collective-permute-start | bytes 3145736 | tf_op jit(solution)/shard_map/ppermute | solution.py:433
  33.0 54.4 %collective-permute-start.2 = (bf16[1,256,2048]{2,1,0:T(8,128)(2,1)}, bf16[1,256,2048]{2,1,0:T(8,128)(2,1)S(1)}, u32[]{:S(2)}, u32[]{:S(2)}) collective-permute-start(bf16[1,256,2048]{2,1,0:T(8,128)(2,1)} %refs_4_.7), channel_id=1, source_target_pairs={{0,1},{1,0},{2,3},{3,2},{4,5},{5,4},{6,7},{7,6},{8,9},{9,8},{10,11... | collective-permute-start | bytes 3145736 | tf_op jit(solution)/shard_map/ppermute | solution.py:433
  35.2 9.0 %collective-permute-start.10 = (bf16[1280,128]{1,0:T(8,128)(2,1)}, bf16[1280,128]{1,0:T(8,128)(2,1)S(1)}, u32[]{:S(2)}, u32[]{:S(2)}) collective-permute-start(bf16[1280,128]{1,0:T(8,128)(2,1)} %get-tuple-element.63.refs_2_), channel_id=1, source_target_pairs={{0,16},{8,24},{16,0},{24,8},{1,17},{9,25},{17,1},{25,9},{2,18},{10... | collective-permute-start | bytes 983048 | tf_op jit(solution)/shard_map/ppermute | solution.py:433
  35.7 8.7 %collective-permute-start.9 = (bf16[1280,128]{1,0:T(8,128)(2,1)}, bf16[1280,128]{1,0:T(8,128)(2,1)S(1)}, u32[]{:S(2)}, u32[]{:S(2)}) collective-permute-start(bf16[1280,128]{1,0:T(8,128)(2,1)} %get-tuple-element.63.refs_2_), channel_id=1, source_target_pairs={{0,8},{8,0},{16,24},{24,16},{1,9},{9,1},{17,25},{25,17},{2,10},{10... | collective-permute-start | bytes 983048 | tf_op jit(solution)/shard_map/ppermute | solution.py:433
  44.2 9.4 %collective-permute-start.6 = (bf16[64,1024]{1,0:T(8,128)(2,1)}, bf16[64,1024]{1,0:T(8,128)(2,1)S(1)}, u32[]{:S(2)}, u32[]{:S(2)}) collective-permute-start(bf16[64,1024]{1,0:T(8,128)(2,1)} %get-tuple-element.59.refs_1_), channel_id=1, source_target_pairs={{0,2},{1,3},{2,0},{3,1},{4,6},{5,7},{6,4},{7,5},{8,10},{9,11},{10,... | collective-permute-start | bytes 393224 | tf_op jit(solution)/shard_map/ppermute | solution.py:433
  44.4 6.9 %collective-permute-start.3 = (bf16[64,1152]{1,0:T(8,128)(2,1)}, bf16[64,1152]{1,0:T(8,128)(2,1)S(1)}, u32[]{:S(2)}, u32[]{:S(2)}) collective-permute-start(bf16[64,1152]{1,0:T(8,128)(2,1)} %get-tuple-element.56.refs_1_), channel_id=1, source_target_pairs={{0,2},{1,3},{2,0},{3,1},{4,6},{5,7},{6,4},{7,5},{8,10},{9,11},{10,... | collective-permute-start | bytes 442376 | tf_op jit(solution)/shard_map/ppermute | solution.py:433
  55.0 19.0 %collective-permute-start.21 = (bf16[144,1024]{1,0:T(8,128)(2,1)S(1)}, bf16[144,1024]{1,0:T(8,128)(2,1)S(1)}, u32[]{:S(2)}, u32[]{:S(2)}) collective-permute-start(bf16[144,1024]{1,0:T(8,128)(2,1)S(1)} %get-tuple-element.72), channel_id=1, source_target_pairs={{0,8},{8,0},{16,24},{24,16},{1,9},{9,1},{17,25},{25,17},{2,10},{10... | collective-permute-start | bytes 884744 | tf_op jit(solution)/shard_map/ppermute | solution.py:433
  79.3 29.8 %collective-permute-start.19 = (bf16[144,1152]{1,0:T(8,128)(2,1)S(1)}, bf16[144,1152]{1,0:T(8,128)(2,1)S(1)}, u32[]{:S(2)}, u32[]{:S(2)}) collective-permute-start(bf16[144,1152]{1,0:T(8,128)(2,1)S(1)} %get-tuple-element.70), channel_id=1, source_target_pairs={{0,8},{8,0},{16,24},{24,16},{1,9},{9,1},{17,25},{25,17},{2,10},{10... | collective-permute-start | bytes 995336 | tf_op jit(solution)/shard_map/ppermute | solution.py:433
  82.2 28.1 %collective-permute-start.20 = (bf16[144,1152]{1,0:T(8,128)(2,1)S(1)}, bf16[144,1152]{1,0:T(8,128)(2,1)S(1)}, u32[]{:S(2)}, u32[]{:S(2)}) collective-permute-start(bf16[144,1152]{1,0:T(8,128)(2,1)S(1)} %get-tuple-element.71), channel_id=1, source_target_pairs={{0,16},{8,24},{16,0},{24,8},{1,17},{9,25},{17,1},{25,9},{2,18},{10... | collective-permute-start | bytes 995336 | tf_op jit(solution)/shard_map/ppermute | solution.py:433
  86.0 21.3 %collective-permute-start.22 = (bf16[144,1024]{1,0:T(8,128)(2,1)S(1)}, bf16[144,1024]{1,0:T(8,128)(2,1)S(1)}, u32[]{:S(2)}, u32[]{:S(2)}) collective-permute-start(bf16[144,1024]{1,0:T(8,128)(2,1)S(1)} %get-tuple-element.73), channel_id=1, source_target_pairs={{0,16},{8,24},{16,0},{24,8},{1,17},{9,25},{17,1},{25,9},{2,18},{10... | collective-permute-start | bytes 884744 | tf_op jit(solution)/shard_map/ppermute | solution.py:433
  86.9 25.2 %collective-permute-start.23 = (bf16[144,1024]{1,0:T(8,128)(2,1)S(1)}, bf16[144,1024]{1,0:T(8,128)(2,1)S(1)}, u32[]{:S(2)}, u32[]{:S(2)}) collective-permute-start(bf16[144,1024]{1,0:T(8,128)(2,1)S(1)} %get-tuple-element.74), channel_id=1, source_target_pairs={{0,8},{8,0},{16,24},{24,16},{1,9},{9,1},{17,25},{25,17},{2,10},{10... | collective-permute-start | bytes 884744 | tf_op jit(solution)/shard_map/ppermute | solution.py:433
  87.4 24.7 %collective-permute-start.24 = (bf16[144,1024]{1,0:T(8,128)(2,1)S(1)}, bf16[144,1024]{1,0:T(8,128)(2,1)S(1)}, u32[]{:S(2)}, u32[]{:S(2)}) collective-permute-start(bf16[144,1024]{1,0:T(8,128)(2,1)S(1)} %get-tuple-element.75), channel_id=1, source_target_pairs={{0,16},{8,24},{16,0},{24,8},{1,17},{9,25},{17,1},{25,9},{2,18},{10... | collective-permute-start | bytes 884744 | tf_op jit(solution)/shard_map/ppermute | solution.py:433
  107.3 18.0 %collective-permute-start.27 = (bf16[144,1152]{1,0:T(8,128)(2,1)S(1)}, bf16[144,1152]{1,0:T(8,128)(2,1)S(1)}, u32[]{:S(2)}, u32[]{:S(2)}) collective-permute-start(bf16[144,1152]{1,0:T(8,128)(2,1)S(1)} %get-tuple-element.78), channel_id=1, source_target_pairs={{0,24},{8,16},{16,8},{24,0},{1,25},{9,17},{17,9},{25,1},{2,26},{10... | collective-permute-start | bytes 995336 | tf_op jit(solution)/shard_map/ppermute | solution.py:433
  109.2 16.2 %collective-permute-start.28 = (bf16[144,1024]{1,0:T(8,128)(2,1)S(1)}, bf16[144,1024]{1,0:T(8,128)(2,1)S(1)}, u32[]{:S(2)}, u32[]{:S(2)}) collective-permute-start(bf16[144,1024]{1,0:T(8,128)(2,1)S(1)} %get-tuple-element.79), channel_id=1, source_target_pairs={{0,24},{8,16},{16,8},{24,0},{1,25},{9,17},{17,9},{25,1},{2,26},{10... | collective-permute-start | bytes 884744 | tf_op jit(solution)/shard_map/ppermute | solution.py:433
  110.3 20.4 %collective-permute-start.29 = (bf16[144,1024]{1,0:T(8,128)(2,1)S(1)}, bf16[144,1024]{1,0:T(8,128)(2,1)S(1)}, u32[]{:S(2)}, u32[]{:S(2)}) collective-permute-start(bf16[144,1024]{1,0:T(8,128)(2,1)S(1)} %get-tuple-element.80), channel_id=1, source_target_pairs={{0,24},{8,16},{16,8},{24,0},{1,25},{9,17},{17,9},{25,1},{2,26},{10... | collective-permute-start | bytes 884744 | tf_op jit(solution)/shard_map/ppermute | solution.py:433
  115.7 33.2 %collective-permute-start.26 = (bf16[144,1536]{1,0:T(8,128)(2,1)S(1)}, bf16[144,1536]{1,0:T(8,128)(2,1)S(1)}, u32[]{:S(2)}, u32[]{:S(2)}) collective-permute-start(bf16[144,1536]{1,0:T(8,128)(2,1)S(1)} %get-tuple-element.77), channel_id=1, source_target_pairs={{0,16},{8,24},{16,0},{24,8},{1,17},{9,25},{17,1},{25,9},{2,18},{10... | collective-permute-start | bytes 1327112 | tf_op jit(solution)/shard_map/ppermute | solution.py:433
  116.5 34.7 %collective-permute-start.25 = (bf16[144,1536]{1,0:T(8,128)(2,1)S(1)}, bf16[144,1536]{1,0:T(8,128)(2,1)S(1)}, u32[]{:S(2)}, u32[]{:S(2)}) collective-permute-start(bf16[144,1536]{1,0:T(8,128)(2,1)S(1)} %get-tuple-element.76.refs_15_), channel_id=1, source_target_pairs={{0,8},{8,0},{16,24},{24,16},{1,9},{9,1},{17,25},{25,17},{2,10},{10... | collective-permute-start | bytes 1327112 | tf_op jit(solution)/shard_map/ppermute | solution.py:433
  132.7 16.2 %collective-permute-start.34 = (bf16[144,768]{1,0:T(8,128)(2,1)S(1)}, bf16[144,768]{1,0:T(8,128)(2,1)S(1)}, u32[]{:S(2)}, u32[]{:S(2)}) collective-permute-start(bf16[144,768]{1,0:T(8,128)(2,1)S(1)} %get-tuple-element.90), channel_id=1, source_target_pairs={{0,24},{8,16},{16,8},{24,0},{1,25},{9,17},{17,9},{25,1},{2,26},{10... | collective-permute-start | bytes 663560 | tf_op jit(solution)/shard_map/ppermute | solution.py:433
  134.8 7.0 %collective-permute-start.41 = (bf16[72,512]{1,0:T(8,128)(2,1)S(1)}, bf16[72,512]{1,0:T(8,128)(2,1)S(1)}, u32[]{:S(2)}, u32[]{:S(2)}) collective-permute-start(bf16[72,512]{1,0:T(8,128)(2,1)S(1)} %get-tuple-element.101), channel_id=1, source_target_pairs={{0,2},{1,3},{2,0},{3,1},{4,6},{5,7},{6,4},{7,5},{8,10},{9,11},{10,... | collective-permute-start | bytes 221192 | tf_op jit(solution)/shard_map/ppermute | solution.py:433
  135.4 11.4 %collective-permute-start.42 = (bf16[72,512]{1,0:T(8,128)(2,1)S(1)}, bf16[72,512]{1,0:T(8,128)(2,1)S(1)}, u32[]{:S(2)}, u32[]{:S(2)}) collective-permute-start(bf16[72,512]{1,0:T(8,128)(2,1)S(1)} %get-tuple-element.102), channel_id=1, source_target_pairs={{0,4},{1,5},{2,6},{3,7},{4,0},{5,1},{6,2},{7,3},{8,12},{9,13},{10,... | collective-permute-start | bytes 221192 | tf_op jit(solution)/shard_map/ppermute | solution.py:433
  141.9 16.7 %collective-permute-start.30 = (bf16[144,768]{1,0:T(8,128)(2,1)S(1)}, bf16[144,768]{1,0:T(8,128)(2,1)S(1)}, u32[]{:S(2)}, u32[]{:S(2)}) collective-permute-start(bf16[144,768]{1,0:T(8,128)(2,1)S(1)} %get-tuple-element.85), channel_id=1, source_target_pairs={{0,24},{8,16},{16,8},{24,0},{1,25},{9,17},{17,9},{25,1},{2,26},{10... | collective-permute-start | bytes 663560 | tf_op jit(solution)/shard_map/ppermute | solution.py:433
  146.8 7.0 %collective-permute-start.43 = (bf16[72,512]{1,0:T(8,128)(2,1)S(1)}, bf16[72,512]{1,0:T(8,128)(2,1)S(1)}, u32[]{:S(2)}, u32[]{:S(2)}) collective-permute-start(bf16[72,512]{1,0:T(8,128)(2,1)S(1)} %get-tuple-element.103), channel_id=1, source_target_pairs={{0,6},{1,7},{2,4},{3,5},{4,2},{5,3},{6,0},{7,1},{8,14},{9,15},{10,... | collective-permute-start | bytes 221192 | tf_op jit(solution)/shard_map/ppermute | solution.py:433
  153.9 11.2 %collective-permute-start.35 = (bf16[64,768]{1,0:T(8,128)(2,1)S(1)}, bf16[64,768]{1,0:T(8,128)(2,1)S(1)}, u32[]{:S(2)}, u32[]{:S(2)}) collective-permute-start(bf16[64,768]{1,0:T(8,128)(2,1)S(1)} %get-tuple-element.92), channel_id=1, source_target_pairs={{0,2},{1,3},{2,0},{3,1},{4,6},{5,7},{6,4},{7,5},{8,10},{9,11},{10,... | collective-permute-start | bytes 294920 | tf_op jit(solution)/shard_map/ppermute | solution.py:433
  155.6 7.1 %collective-permute-start.45 = (bf16[36,512]{1,0:T(8,128)(2,1)S(1)}, bf16[36,512]{1,0:T(8,128)(2,1)S(1)}, u32[]{:S(2)}, u32[]{:S(2)}) collective-permute-start(bf16[36,512]{1,0:T(8,128)(2,1)S(1)} %get-tuple-element.105), channel_id=1, source_target_pairs={{0,16},{8,24},{16,0},{24,8},{1,17},{9,25},{17,1},{25,9},{2,18},{10... | collective-permute-start | bytes 110600 | tf_op jit(solution)/shard_map/ppermute | solution.py:433
  158.6 8.7 %collective-permute-start.36 = (bf16[64,768]{1,0:T(8,128)(2,1)S(1)}, bf16[64,768]{1,0:T(8,128)(2,1)S(1)}, u32[]{:S(2)}, u32[]{:S(2)}) collective-permute-start(bf16[64,768]{1,0:T(8,128)(2,1)S(1)} %get-tuple-element.93), channel_id=1, source_target_pairs={{0,4},{1,5},{2,6},{3,7},{4,0},{5,1},{6,2},{7,3},{8,12},{9,13},{10,... | collective-permute-start | bytes 294920 | tf_op jit(solution)/shard_map/ppermute | solution.py:433
  160.6 6.8 %collective-permute-start.37 = (bf16[64,768]{1,0:T(8,128)(2,1)S(1)}, bf16[64,768]{1,0:T(8,128)(2,1)S(1)}, u32[]{:S(2)}, u32[]{:S(2)}) collective-permute-start(bf16[64,768]{1,0:T(8,128)(2,1)S(1)} %get-tuple-element.94), channel_id=1, source_target_pairs={{0,6},{1,7},{2,4},{3,5},{4,2},{5,3},{6,0},{7,1},{8,14},{9,15},{10,... | collective-permute-start | bytes 294920 | tf_op jit(solution)/shard_map/ppermute | solution.py:433
  (28 other events, 465.0 us)

commit v2 on v1

--- a/solution.py
+++ b/solution.py
@@ -68,7 +68,7 @@
 
 def prep_kernel(
     heads, lat, rot, lat_gain, key_up, value_up, queries, q_gain, k_gain, inner, first,
-    selq, selk, selg, routes, route_weights, residual, flags, bundle, q1, q2, head, rest,
+    selq, selk, selg, routes, route_weights, residual, flags, bundle, q, head, rest,
 ):
     pack_rows(routes, route_weights, residual, flags, head, rest)
     rows = lat.shape[0]
@@ -126,20 +126,22 @@
         qb = picked[:, base + 2 * LANES : base + 3 * LANES]
         sq = jnp.sum(nope * nope + qa * qa * (ROPE / LANES), axis=-1, keepdims=True)
         r = lax.rsqrt(sq * (1.0 / QK) + epsilon)
-        q1[h] = (nope * r * cut(gq, 0)).astype(bf16)
+        q[h] = (nope * r * cut(gq, 0)).astype(bf16)
         turned = (qa * cut(gq, 1) * cos + qb * cut(gq, 2) * sin) * r
         for p in range(pack):
-            q2[h * pack + p] = jnp.where(lane // ROPE == p * heads + h, turned, 0.0).astype(bf16)
-
-
-def scores_of(heads, q1, q2, ref, h, top, count, parts):
-    rows = q1.shape[1]
+            q[heads + h * pack + p] = jnp.where(
+                lane // ROPE == p * heads + h, turned, 0.0
+            ).astype(bf16)
+
+
+def scores_of(heads, q, ref, h, top, count, parts):
+    rows = q.shape[1]
     pack = LANES // (ROPE * heads)
     sub = rows // pack
     out = []
     for p in range(parts):
         query = jnp.concatenate(
-            [q1[h, top : top + count], q2[h * pack + p, top : top + count]], axis=1
+            [q[h, top : top + count], q[heads + h * pack + p, top : top + count]], axis=1
         )
         key = jnp.concatenate(
             [
@@ -157,13 +159,13 @@
 FACTOR = float(QK ** (-0.5) * np.log2(np.e))
 
 
-def attend_own(heads, q1, q2, ref, state):
-    rows = q1.shape[1]
+def attend_own(heads, q, ref, state):
+    rows = q.shape[1]
     pack = LANES // (ROPE * heads)
     sub = rows // pack
     for h in range(heads):
         for b in range(pack):
-            scores = scores_of(heads, q1, q2, ref, h, b * sub, sub, b + 1)
+            scores = scores_of(heads, q, ref, h, b * sub, sub, b + 1)
             key = lax.broadcasted_iota(jnp.int32, scores.shape, 0)
             query = lax.broadcasted_iota(jnp.int32, scores.shape, 1) + b * sub
             scores = jnp.where(key <= query, scores, -1e30)
@@ -177,11 +179,11 @@
             )
 
 
-def attend_other(heads, q1, q2, ref, state):
-    rows = q1.shape[1]
+def attend_other(heads, q, ref, state):
+    rows = q.shape[1]
     pack = LANES // (ROPE * heads)
     for h in range(heads):
-        scores = scores_of(heads, q1, q2, ref, h, 0, rows, pack)
+        scores = scores_of(heads, q, ref, h, 0, rows, pack)
         old = state[h, 0:1, :]
         peak = jnp.maximum(old, jnp.max(scores, axis=0, keepdims=True))
         fade = jnp.exp2((old - peak) * FACTOR)
@@ -193,17 +195,17 @@
         state[h] = jnp.where(row == 0, peak, jnp.where(row == 1, total, part))
 
 
-def attend_kernel(heads, tokens, groups, q1, q2, *refs):
+def attend_kernel(heads, tokens, groups, q, *refs):
     bundles = refs[:-4]
     keep, send, state, result = refs[-4:]
     me = lax.axis_index("sp")
     core = lax.axis_index("tp") % 2
-    attend_own(heads, q1, q2, bundles[0], state)
+    attend_own(heads, q, bundles[0], state)
     for k in range(1, len(bundles)):
 
         @pl.when((me ^ k) < me)
         def _():
-            attend_other(heads, q1, q2, bundles[k], state)
+            attend_other(heads, q, bundles[k], state)
 
     outs = [state[h, NOPE:, :] / state[h, 1:2, :] for h in range(heads)]
     result[...] = (outs[0] if heads == 1 else jnp.concatenate(outs, axis=0)).T
@@ -232,7 +234,7 @@
     second[...] = residual[:, half:]
 
 
-def residual_first_kernel(groups, sp, cap, lower, *refs):
+def residual_first_kernel(groups, sp, cap, *refs):
     parts = refs[:groups]
     table, outs, everything = refs[groups], refs[groups + 1 : -1], refs[-1]
     tokens, width = parts[0].shape
@@ -247,7 +249,12 @@
     route = [ticket[:, j : j + 1].astype(jnp.int32) for j in range(TOPK)]
     named = me ^ lane
     hit = ((route[0] == named) | (route[1] == named)) & (lane < sp)
-    rank = dot(lower[...], hit.astype(f32).astype(bf16)).astype(jnp.int32)
+    total = groups * tokens
+    later = lax.broadcasted_iota(jnp.int32, (total, total), 0)
+    earlier = lax.broadcasted_iota(jnp.int32, (total, total), 1)
+    lower = (later > earlier) & (later // tokens == earlier // tokens)
+    lower = jnp.where(lower, 1.0, 0.0).astype(bf16)
+    rank = dot(lower, hit.astype(f32).astype(bf16)).astype(jnp.int32)
     slot = jnp.where(hit, rank + (row // tokens) * cap, -1)
     named = me ^ (lane // 3)
     tail = jnp.zeros(ticket.shape, f32)
@@ -441,17 +448,13 @@
 
     flags = np.zeros((4 * TOPK, LANES), np.float32)
     flags[np.arange(4 * TOPK), np.arange(4 * TOPK)] = 1.0
-    ordinal = np.arange(all_tokens)
-    lower = (ordinal[:, None] > ordinal[None, :]) & (
-        ordinal[:, None] // tokens == ordinal[None, :] // tokens
-    )
-    lower = jnp.asarray(lower.astype(np.float32), bf16)
+
     pack = LANES // (ROPE * heads)
     inner, first = turn_tables(rows, sp)
     selk = jnp.asarray(np.concatenate(rope_select(0, ROPE), axis=1), bf16)
     selq = jnp.asarray(head_select(heads), bf16)
     selg = jnp.asarray(np.abs(head_select(1)), f32)
-    bundle, q1, q2, first_half, second_half = call(
+    bundle, q, first_half, second_half = call(
         functools.partial(prep_kernel, heads),
         [
             latent, rot_key.T, latent_gain[None, :], key_up, value_up, queries.T,
@@ -460,8 +463,7 @@
         ],
         (
             shape((heads * rows + rows // pack, LANES), bf16),
-            shape((heads, rows, LANES), bf16),
-            shape((heads * pack, rows, LANES), bf16),
+            shape((heads * (1 + pack), rows, LANES), bf16),
             shape((tokens, width // 2 + LANES), bf16),
             shape((tokens, width // 2), bf16),
         ),
@@ -477,7 +479,7 @@
     down_b = swap_core(expert_down)
     table, *first_rows = call(
         functools.partial(residual_first_kernel, groups, sp, cap),
-        [lower] + first_parts,
+        first_parts,
         (shape((sp, all_tokens, slots), bf16),)
         + tuple([shape((slots, width // 2 + LANES), bf16)] * sp),
         [pltpu.VMEM((all_tokens, width // 2 + LANES), bf16)],
@@ -488,7 +490,7 @@
     half = heads * VH
     keep, send = call(
         functools.partial(attend_kernel, heads, tokens, groups),
-        [q1, q2] + bundles,
+        [q] + bundles,
         (shape((all_tokens, half), bf16), shape((all_tokens, half), bf16)),
         [pltpu.VMEM((heads, LANES, rows), f32), pltpu.VMEM((rows, half), f32)],
         room=ATTEND_ROOM,
@@ -527,7 +529,7 @@
         extra_in = ([residual, own_rows] if own else []) + (carried if last and n else [])
         extra_out = (shape((tokens, width), f32),) if own else ()
         members = ([0] if last and n else []) + part
-        cuts = COL_CHUNKS if last else 1
+        cuts = COL_CHUNKS
         outs = call(
             functools.partial(expert_kernel, part, cuts, own, cap, bool(last and n)),
             [

time: 173 us -> 156 us (0.902)
  waiting for transfers between devices: 88 us -> 62.9 us
  starting transfers between devices: 60.8 us -> 69.9 us
    ppermute x47 -> x49, waiting for transfers between devices: 88 us -> 62.9 us  [swap(): return lax.ppermute(v, axis, [(i, i ^ k) for i in range(size)])]
    ppermute x47 -> x49, starting transfers between devices: 60.8 us -> 69.9 us  [swap(): return lax.ppermute(v, axis, [(i, i ^ k) for i in range(size)])]
    unnamed x26 -> x22, local copies, waits for them, and re-layouts: 4.96 us -> 3.95 us
  transfers between devices with their start and end apart: 47 -> 49, of which waited for: 20 -> 18; matrix products, arithmetic and copies ran while one was open for 0% -> 0% of each run, Pallas kernels for 8% -> 9%
where the time goes in v2:
time: 156 us; the launch traced here: 155 us
  starting transfers between devices  69.9 us (45%)
  waiting for transfers between devices  62.9 us (40%)
  Pallas kernels  17.6 us (11%)
  local copies, waits for them, and re-layouts  3.95 us (3%)
    ppermute x49, starting transfers between devices, swap(): return lax.ppermute(v, axis, [(i, i ^ k) for i in range(size)])  69.9 us
    ppermute x49, waiting for transfers between devices, swap(): return lax.ppermute(v, axis, [(i, i ^ k) for i in range(size)])  62.9 us
    pallas_call x13, Pallas kernels, call(): pl.pallas_call(kernel, out_shape=outs, in_specs=[VM] * count + [ANY] * le...  17.6 us
    unnamed x22, local copies, waits for them, and re-layouts  3.95 us
  transfers between devices with their start and end apart: 49, of which 18 were waited for; matrix products, arithmetic and copies ran while one was open for 0% of the time, Pallas kernels for 9%

profile of v2, /device:TPU:0, one launch (start us, length us, event | category | flops | bytes accessed | tf_op | source)
XLA Modules:
  0.0 155.5 jit_solution(9595841321476095095)
XLA Ops:
  0.0 3.9 %shard_map.217 = (bf16[1280,128]{1,0:T(8,128)(2,1)}, bf16[6,512,128]{2,1,0:T(8,128)(2,1)}, bf16[64,1152]{1,0:T(8,128)(2,1)}, bf16[64,1024]{1,0:T(8,128)(2,1)}) custom-call(bf16[512,512]{1,0:T(8,128)(2,1)} %refs_0_.4, bf16[32,512]{1,0:T(8,128)(2,1)} %bitcast.14, f32[1,512]{1,0:T(1,128)} %bitcast.15, bf16[512,128]{1,0:T(8,128)(2,1)} %refs_3_.4, ...), custom_call_target="tpu_custom_call" | custom-call | flops 285212672 | bytes 3663616 | tf_op jit(solution)/shard_map/pallas_call | solution.py:405
  3.9 4.0 %collective-permute-start.11 = (bf16[1280,128]{1,0:T(8,128)(2,1)}, bf16[1280,128]{1,0:T(8,128)(2,1)S(1)}, u32[]{:S(2)}, u32[]{:S(2)}) collective-permute-start(bf16[1280,128]{1,0:T(8,128)(2,1)} %get-tuple-element.64.refs_1_), channel_id=1, source_target_pairs={{0,24},{8,16},{16,8},{24,0},{1,25},{9,17},{17,9},{25,1},{2,26},{10... | collective-permute-start | bytes 983048 | tf_op jit(solution)/shard_map/ppermute | solution.py:440
  8.6 4.0 %collective-permute-start.8 = (bf16[64,1024]{1,0:T(8,128)(2,1)}, bf16[64,1024]{1,0:T(8,128)(2,1)S(1)}, u32[]{:S(2)}, u32[]{:S(2)}) collective-permute-start(bf16[64,1024]{1,0:T(8,128)(2,1)} %get-tuple-element.61.refs_1_), channel_id=1, source_target_pairs={{0,6},{1,7},{2,4},{3,5},{4,2},{5,3},{6,0},{7,1},{8,14},{9,15},{10,... | collective-permute-start | bytes 393224 | tf_op jit(solution)/shard_map/ppermute | solution.py:440
  12.6 4.4 %collective-permute-done.8.refs_4_ = bf16[64,1024]{1,0:T(8,128)(2,1)S(1)} collective-permute-done((bf16[64,1024]{1,0:T(8,128)(2,1)}, bf16[64,1024]{1,0:T(8,128)(2,1)S(1)}, u32[]{:S(2)}, u32[]{:S(2)}) %collective-permute-start.8) | collective-permute-done | bytes 131104 | tf_op jit(solution)/shard_map/ppermute | solution.py:440
  16.9 3.5 %collective-permute-start.5 = (bf16[64,1152]{1,0:T(8,128)(2,1)}, bf16[64,1152]{1,0:T(8,128)(2,1)S(1)}, u32[]{:S(2)}, u32[]{:S(2)}) collective-permute-start(bf16[64,1152]{1,0:T(8,128)(2,1)} %get-tuple-element.58.refs_0_), channel_id=1, source_target_pairs={{0,6},{1,7},{2,4},{3,5},{4,2},{5,3},{6,0},{7,1},{8,14},{9,15},{10,... | collective-permute-start | bytes 442376 | tf_op jit(solution)/shard_map/ppermute | solution.py:440
  20.5 6.6 %collective-permute-done.7.refs_3_ = bf16[64,1024]{1,0:T(8,128)(2,1)S(1)} collective-permute-done((bf16[64,1024]{1,0:T(8,128)(2,1)}, bf16[64,1024]{1,0:T(8,128)(2,1)S(1)}, u32[]{:S(2)}, u32[]{:S(2)}) %collective-permute-start.7) | collective-permute-done | bytes 131104 | tf_op jit(solution)/shard_map/ppermute | solution.py:440
  27.5 4.9 %collective-permute-done.6.refs_2_ = bf16[64,1024]{1,0:T(8,128)(2,1)S(1)} collective-permute-done((bf16[64,1024]{1,0:T(8,128)(2,1)}, bf16[64,1024]{1,0:T(8,128)(2,1)S(1)}, u32[]{:S(2)}, u32[]{:S(2)}) %collective-permute-start.6) | collective-permute-done | bytes 131104 | tf_op jit(solution)/shard_map/ppermute | solution.py:440
  32.4 3.7 %collective-permute-start.4 = (bf16[64,1152]{1,0:T(8,128)(2,1)}, bf16[64,1152]{1,0:T(8,128)(2,1)S(1)}, u32[]{:S(2)}, u32[]{:S(2)}) collective-permute-start(bf16[64,1152]{1,0:T(8,128)(2,1)} %get-tuple-element.58.refs_0_), channel_id=1, source_target_pairs={{0,4},{1,5},{2,6},{3,7},{4,0},{5,1},{6,2},{7,3},{8,12},{9,13},{10,... | collective-permute-start | bytes 442376 | tf_op jit(solution)/shard_map/ppermute | solution.py:440
  36.1 2.5 %collective-permute-start.3 = (bf16[64,1152]{1,0:T(8,128)(2,1)}, bf16[64,1152]{1,0:T(8,128)(2,1)S(1)}, u32[]{:S(2)}, u32[]{:S(2)}) collective-permute-start(bf16[64,1152]{1,0:T(8,128)(2,1)} %get-tuple-element.58.refs_0_), channel_id=1, source_target_pairs={{0,2},{1,3},{2,0},{3,1},{4,6},{5,7},{6,4},{7,5},{8,10},{9,11},{10,... | collective-permute-start | bytes 442376 | tf_op jit(solution)/shard_map/ppermute | solution.py:440
  47.6 2.6 %collective-permute-done.17.refs_8_ = bf16[256,128]{1,0:T(8,128)(2,1)S(1)} collective-permute-done((bf16[256,128]{1,0:T(8,128)(2,1)S(1)}, bf16[256,128]{1,0:T(8,128)(2,1)S(1)}, u32[]{:S(2)}, u32[]{:S(2)}) %collective-permute-start.17) | collective-permute-done | bytes 65568 | tf_op jit(solution)/shard_map/ppermute | solution.py:440
  52.3 2.9 %collective-permute-start.21 = (bf16[144,1024]{1,0:T(8,128)(2,1)S(1)}, bf16[144,1024]{1,0:T(8,128)(2,1)S(1)}, u32[]{:S(2)}, u32[]{:S(2)}) collective-permute-start(bf16[144,1024]{1,0:T(8,128)(2,1)S(1)} %get-tuple-element.73), channel_id=1, source_target_pairs={{0,8},{8,0},{16,24},{24,16},{1,9},{9,1},{17,25},{25,17},{2,10},{10... | collective-permute-start | bytes 884744 | tf_op jit(solution)/shard_map/ppermute | solution.py:440
  55.2 4.0 %collective-permute-start.22 = (bf16[144,1024]{1,0:T(8,128)(2,1)S(1)}, bf16[144,1024]{1,0:T(8,128)(2,1)S(1)}, u32[]{:S(2)}, u32[]{:S(2)}) collective-permute-start(bf16[144,1024]{1,0:T(8,128)(2,1)S(1)} %get-tuple-element.74), channel_id=1, source_target_pairs={{0,16},{8,24},{16,0},{24,8},{1,17},{9,25},{17,1},{25,9},{2,18},{10... | collective-permute-start | bytes 884744 | tf_op jit(solution)/shard_map/ppermute | solution.py:440
  59.1 3.2 %collective-permute-done.21.refs_10_ = bf16[144,1024]{1,0:T(8,128)(2,1)S(1)} collective-permute-done((bf16[144,1024]{1,0:T(8,128)(2,1)S(1)}, bf16[144,1024]{1,0:T(8,128)(2,1)S(1)}, u32[]{:S(2)}, u32[]{:S(2)}) %collective-permute-start.21) | collective-permute-done | bytes 294944 | tf_op jit(solution)/shard_map/ppermute | solution.py:440
  63.0 3.0 %collective-permute-done.22.refs_11_ = bf16[144,1024]{1,0:T(8,128)(2,1)S(1)} collective-permute-done((bf16[144,1024]{1,0:T(8,128)(2,1)S(1)}, bf16[144,1024]{1,0:T(8,128)(2,1)S(1)}, u32[]{:S(2)}, u32[]{:S(2)}) %collective-permute-start.22) | collective-permute-done | bytes 294944 | tf_op jit(solution)/shard_map/ppermute | solution.py:440
  66.0 2.4 %collective-permute-done.18.refs_9_ = bf16[256,128]{1,0:T(8,128)(2,1)S(1)} collective-permute-done((bf16[256,128]{1,0:T(8,128)(2,1)S(1)}, bf16[256,128]{1,0:T(8,128)(2,1)S(1)}, u32[]{:S(2)}, u32[]{:S(2)}) %collective-permute-start.18) | collective-permute-done | bytes 65568 | tf_op jit(solution)/shard_map/ppermute | solution.py:440
  68.4 2.8 %collective-permute-done.16.refs_7_ = bf16[256,128]{1,0:T(8,128)(2,1)S(1)} collective-permute-done((bf16[256,128]{1,0:T(8,128)(2,1)S(1)}, bf16[256,128]{1,0:T(8,128)(2,1)S(1)}, u32[]{:S(2)}, u32[]{:S(2)}) %collective-permute-start.16) | collective-permute-done | bytes 65568 | tf_op jit(solution)/shard_map/ppermute | solution.py:440
  72.6 4.5 %collective-permute-start.20 = (bf16[144,1152]{1,0:T(8,128)(2,1)S(1)}, bf16[144,1152]{1,0:T(8,128)(2,1)S(1)}, u32[]{:S(2)}, u32[]{:S(2)}) collective-permute-start(bf16[144,1152]{1,0:T(8,128)(2,1)S(1)} %get-tuple-element.72), channel_id=1, source_target_pairs={{0,16},{8,24},{16,0},{24,8},{1,17},{9,25},{17,1},{25,9},{2,18},{10... | collective-permute-start | bytes 995336 | tf_op jit(solution)/shard_map/ppermute | solution.py:440
  80.1 2.3 %collective-permute-done.20.refs_9_ = bf16[144,1152]{1,0:T(8,128)(2,1)S(1)} collective-permute-done((bf16[144,1152]{1,0:T(8,128)(2,1)S(1)}, bf16[144,1152]{1,0:T(8,128)(2,1)S(1)}, u32[]{:S(2)}, u32[]{:S(2)}) %collective-permute-start.20) | collective-permute-done | bytes 331808 | tf_op jit(solution)/shard_map/ppermute | solution.py:440
  82.3 1.9 %collective-permute-start.24 = (bf16[144,1024]{1,0:T(8,128)(2,1)S(1)}, bf16[144,1024]{1,0:T(8,128)(2,1)S(1)}, u32[]{:S(2)}, u32[]{:S(2)}) collective-permute-start(bf16[144,1024]{1,0:T(8,128)(2,1)S(1)} %get-tuple-element.76), channel_id=1, source_target_pairs={{0,16},{8,24},{16,0},{24,8},{1,17},{9,25},{17,1},{25,9},{2,18},{10... | collective-permute-start | bytes 884744 | tf_op jit(solution)/shard_map/ppermute | solution.py:440
  88.4 2.3 %shard_map.222 = (bf16[144,768]{1,0:T(8,128)(2,1)S(1)}, bf16[144,768]{1,0:T(8,128)(2,1)S(1)}, bf16[36,512]{1,0:T(8,128)(2,1)S(1)}, bf16[36,512]{1,0:T(8,128)(2,1...) custom-call(bf16[1024,2048]{1,0:T(8,128)(2,1)S(1)} %copy-done, ...), custom_call_target="tpu_custom_call" | custom-call | flops 1509949440 | bytes 12922880 | tf_op jit(solution)/shard_map/pallas_call | solution.py:405
  90.8 17.9 %collective-permute-done.24.refs_13_ = bf16[144,1024]{1,0:T(8,128)(2,1)S(1)} collective-permute-done((bf16[144,1024]{1,0:T(8,128)(2,1)S(1)}, bf16[144,1024]{1,0:T(8,128)(2,1)S(1)}, u32[]{:S(2)}, u32[]{:S(2)}) %collective-permute-start.24) | collective-permute-done | bytes 294944 | tf_op jit(solution)/shard_map/ppermute | solution.py:440
  108.6 3.6 %shard_map.223 = (bf16[144,768]{1,0:T(8,128)(2,1)S(1)}, bf16[144,768]{1,0:T(8,128)(2,1)S(1)}, bf16[144,768]{1,0:T(8,128)(2,1)S(1)}, bf16[144,768]{1,0:T(8,128)(2...) custom-call(bf16[1024,2048]{1,0:T(8,128)(2,1)S(1)} %copy-done, ...), custom_call_target="tpu_custom_call" | custom-call | flops 3019898880 | bytes 13516800 | tf_op jit(solution)/shard_map/pallas_call | solution.py:405
  112.3 2.6 %collective-permute-start.44 = (bf16[72,512]{1,0:T(8,128)(2,1)S(1)}, bf16[72,512]{1,0:T(8,128)(2,1)S(1)}, u32[]{:S(2)}, u32[]{:S(2)}) collective-permute-start(bf16[72,512]{1,0:T(8,128)(2,1)S(1)} %get-tuple-element.106), channel_id=1, source_target_pairs={{0,4},{1,5},{2,6},{3,7},{4,0},{5,1},{6,2},{7,3},{8,12},{9,13},{10,... | collective-permute-start | bytes 221192 | tf_op jit(solution)/shard_map/ppermute | solution.py:440
  117.1 2.1 %shard_map.224 = (bf16[144,768]{1,0:T(8,128)(2,1)S(1)}, bf16[144,768]{1,0:T(8,128)(2,1)S(1)}, bf16[72,512]{1,0:T(8,128)(2,1)S(1)}, bf16[72,512]{1,0:T(8,128)(2,1...) custom-call(bf16[1024,2048]{1,0:T(8,128)(2,1)S(1)} %copy-done, f32[1,2048]{1,0:T(1,128)S(1)} %bitcast.11, ...), custom_call_target="tpu_custom_call" | custom-call | flops 1509949440 | bytes 12300288 | tf_op jit(solution)/shard_map/pallas_call | solution.py:405
  120.6 2.6 %collective-permute-start.45 = (bf16[72,512]{1,0:T(8,128)(2,1)S(1)}, bf16[72,512]{1,0:T(8,128)(2,1)S(1)}, u32[]{:S(2)}, u32[]{:S(2)}) collective-permute-start(bf16[72,512]{1,0:T(8,128)(2,1)S(1)} %get-tuple-element.107), channel_id=1, source_target_pairs={{0,6},{1,7},{2,4},{3,5},{4,2},{5,3},{6,0},{7,1},{8,14},{9,15},{10,... | collective-permute-start | bytes 221192 | tf_op jit(solution)/shard_map/ppermute | solution.py:440
  123.2 3.6 %collective-permute-done.45.refs_3_ = bf16[72,512]{1,0:T(8,128)(2,1)S(1)} collective-permute-done((bf16[72,512]{1,0:T(8,128)(2,1)S(1)}, bf16[72,512]{1,0:T(8,128)(2,1)S(1)}, u32[]{:S(2)}, u32[]{:S(2)}) %collective-permute-start.45) | collective-permute-done | bytes 73760 | tf_op jit(solution)/shard_map/ppermute | solution.py:440
  130.7 3.4 %collective-permute-start.42 = (bf16[72,512]{1,0:T(8,128)(2,1)S(1)}, bf16[72,512]{1,0:T(8,128)(2,1)S(1)}, u32[]{:S(2)}, u32[]{:S(2)}) collective-permute-start(bf16[72,512]{1,0:T(8,128)(2,1)S(1)} %get-tuple-element.102), channel_id=1, source_target_pairs={{0,6},{1,7},{2,4},{3,5},{4,2},{5,3},{6,0},{7,1},{8,14},{9,15},{10,... | collective-permute-start | bytes 221192 | tf_op jit(solution)/shard_map/ppermute | solution.py:440
  134.7 2.9 %collective-permute-done.41.refs_2_ = bf16[72,512]{1,0:T(8,128)(2,1)S(1)} collective-permute-done((bf16[72,512]{1,0:T(8,128)(2,1)S(1)}, bf16[72,512]{1,0:T(8,128)(2,1)S(1)}, u32[]{:S(2)}, u32[]{:S(2)}) %collective-permute-start.41) | collective-permute-done | bytes 73760 | tf_op jit(solution)/shard_map/ppermute | solution.py:440
  138.1 1.7 %collective-permute-start.47 = (bf16[36,512]{1,0:T(8,128)(2,1)S(1)}, bf16[36,512]{1,0:T(8,128)(2,1)S(1)}, u32[]{:S(2)}, u32[]{:S(2)}) collective-permute-start(bf16[36,512]{1,0:T(8,128)(2,1)S(1)} %get-tuple-element.109), channel_id=1, source_target_pairs={{0,16},{8,24},{16,0},{24,8},{1,17},{9,25},{17,1},{25,9},{2,18},{10... | collective-permute-start | bytes 110600 | tf_op jit(solution)/shard_map/ppermute | solution.py:440
  143.2 3.1 %collective-permute-start.33 = (bf16[64,768]{1,0:T(8,128)(2,1)S(1)}, bf16[64,768]{1,0:T(8,128)(2,1)S(1)}, u32[]{:S(2)}, u32[]{:S(2)}) collective-permute-start(bf16[64,768]{1,0:T(8,128)(2,1)S(1)} %get-tuple-element.90), channel_id=1, source_target_pairs={{0,6},{1,7},{2,4},{3,5},{4,2},{5,3},{6,0},{7,1},{8,14},{9,15},{10,... | collective-permute-start | bytes 294920 | tf_op jit(solution)/shard_map/ppermute | solution.py:440
  147.7 3.0 %collective-permute-start.39 = (bf16[64,768]{1,0:T(8,128)(2,1)S(1)}, bf16[64,768]{1,0:T(8,128)(2,1)S(1)}, u32[]{:S(2)}, u32[]{:S(2)}) collective-permute-start(bf16[64,768]{1,0:T(8,128)(2,1)S(1)} %get-tuple-element.98), channel_id=1, source_target_pairs={{0,6},{1,7},{2,4},{3,5},{4,2},{5,3},{6,0},{7,1},{8,14},{9,15},{10,... | collective-permute-start | bytes 294920 | tf_op jit(solution)/shard_map/ppermute | solution.py:440
  151.1 3.5 %collective-permute-done.38 = bf16[64,768]{1,0:T(8,128)(2,1)S(1)} collective-permute-done((bf16[64,768]{1,0:T(8,128)(2,1)S(1)}, bf16[64,768]{1,0:T(8,128)(2,1)S(1)}, u32[]{:S(2)}, u32[]{:S(2)}) %collective-permute-start.38) | collective-permute-done | bytes 98336 | tf_op jit(solution)/shard_map/ppermute | solution.py:440
  (103 shorter events, 35.8 us)
Async XLA Ops:
  3.9 34.7 %collective-permute-start.11 = (bf16[1280,128]{1,0:T(8,128)(2,1)}, bf16[1280,128]{1,0:T(8,128)(2,1)S(1)}, u32[]{:S(2)}, u32[]{:S(2)}) collective-permute-start(bf16[1280,128]{1,0:T(8,128)(2,1)} %get-tuple-element.64.refs_1_), channel_id=1, source_target_pairs={{0,24},{8,16},{16,8},{24,0},{1,25},{9,17},{17,9},{25,1},{2,26},{10... | collective-permute-start | bytes 983048 | tf_op jit(solution)/shard_map/ppermute | solution.py:440
  7.9 30.7 %collective-permute-start.10 = (bf16[1280,128]{1,0:T(8,128)(2,1)}, bf16[1280,128]{1,0:T(8,128)(2,1)S(1)}, u32[]{:S(2)}, u32[]{:S(2)}) collective-permute-start(bf16[1280,128]{1,0:T(8,128)(2,1)} %get-tuple-element.64.refs_1_), channel_id=1, source_target_pairs={{0,16},{8,24},{16,0},{24,8},{1,17},{9,25},{17,1},{25,9},{2,18},{10... | collective-permute-start | bytes 983048 | tf_op jit(solution)/shard_map/ppermute | solution.py:440
  8.4 30.7 %collective-permute-start.9 = (bf16[1280,128]{1,0:T(8,128)(2,1)}, bf16[1280,128]{1,0:T(8,128)(2,1)S(1)}, u32[]{:S(2)}, u32[]{:S(2)}) collective-permute-start(bf16[1280,128]{1,0:T(8,128)(2,1)} %get-tuple-element.64.refs_1_), channel_id=1, source_target_pairs={{0,8},{8,0},{16,24},{24,16},{1,9},{9,1},{17,25},{25,17},{2,10},{10... | collective-permute-start | bytes 983048 | tf_op jit(solution)/shard_map/ppermute | solution.py:440
  8.6 8.4 %collective-permute-start.8 = (bf16[64,1024]{1,0:T(8,128)(2,1)}, bf16[64,1024]{1,0:T(8,128)(2,1)S(1)}, u32[]{:S(2)}, u32[]{:S(2)}) collective-permute-start(bf16[64,1024]{1,0:T(8,128)(2,1)} %get-tuple-element.61.refs_1_), channel_id=1, source_target_pairs={{0,6},{1,7},{2,4},{3,5},{4,2},{5,3},{6,0},{7,1},{8,14},{9,15},{10,... | collective-permute-start | bytes 393224 | tf_op jit(solution)/shard_map/ppermute | solution.py:440
  12.6 14.5 %collective-permute-start.7 = (bf16[64,1024]{1,0:T(8,128)(2,1)}, bf16[64,1024]{1,0:T(8,128)(2,1)S(1)}, u32[]{:S(2)}, u32[]{:S(2)}) collective-permute-start(bf16[64,1024]{1,0:T(8,128)(2,1)} %get-tuple-element.61.refs_1_), channel_id=1, source_target_pairs={{0,4},{1,5},{2,6},{3,7},{4,0},{5,1},{6,2},{7,3},{8,12},{9,13},{10,... | collective-permute-start | bytes 393224 | tf_op jit(solution)/shard_map/ppermute | solution.py:440
  16.9 19.2 %collective-permute-start.5 = (bf16[64,1152]{1,0:T(8,128)(2,1)}, bf16[64,1152]{1,0:T(8,128)(2,1)S(1)}, u32[]{:S(2)}, u32[]{:S(2)}) collective-permute-start(bf16[64,1152]{1,0:T(8,128)(2,1)} %get-tuple-element.58.refs_0_), channel_id=1, source_target_pairs={{0,6},{1,7},{2,4},{3,5},{4,2},{5,3},{6,0},{7,1},{8,14},{9,15},{10,... | collective-permute-start | bytes 442376 | tf_op jit(solution)/shard_map/ppermute | solution.py:440
  32.4 10.6 %collective-permute-start.4 = (bf16[64,1152]{1,0:T(8,128)(2,1)}, bf16[64,1152]{1,0:T(8,128)(2,1)S(1)}, u32[]{:S(2)}, u32[]{:S(2)}) collective-permute-start(bf16[64,1152]{1,0:T(8,128)(2,1)} %get-tuple-element.58.refs_0_), channel_id=1, source_target_pairs={{0,4},{1,5},{2,6},{3,7},{4,0},{5,1},{6,2},{7,3},{8,12},{9,13},{10,... | collective-permute-start | bytes 442376 | tf_op jit(solution)/shard_map/ppermute | solution.py:440
  38.6 45.6 %collective-permute-start = (bf16[1,2048,256]{2,1,0:T(8,128)(2,1)}, bf16[1,2048,256]{2,1,0:T(8,128)(2,1)S(1)}, u32[]{:S(2)}, u32[]{:S(2)}) collective-permute-start(bf16[1,2048,256]{2,1,0:T(8,128)(2,1)} %refs_2_.5), channel_id=1, source_target_pairs={{0,1},{1,0},{2,3},{3,2},{4,5},{5,4},{6,7},{7,6},{8,9},{9,8},{10,11... | collective-permute-start | bytes 3145736 | tf_op jit(solution)/shard_map/ppermute | solution.py:440
  38.7 46.8 %collective-permute-start.1 = (bf16[1,2048,256]{2,1,0:T(8,128)(2,1)}, bf16[1,2048,256]{2,1,0:T(8,128)(2,1)S(1)}, u32[]{:S(2)}, u32[]{:S(2)}) collective-permute-start(bf16[1,2048,256]{2,1,0:T(8,128)(2,1)} %refs_3_.7), channel_id=1, source_target_pairs={{0,1},{1,0},{2,3},{3,2},{4,5},{5,4},{6,7},{7,6},{8,9},{9,8},{10,11... | collective-permute-start | bytes 3145736 | tf_op jit(solution)/shard_map/ppermute | solution.py:440
  39.2 48.0 %collective-permute-start.2 = (bf16[1,256,2048]{2,1,0:T(8,128)(2,1)}, bf16[1,256,2048]{2,1,0:T(8,128)(2,1)S(1)}, u32[]{:S(2)}, u32[]{:S(2)}) collective-permute-start(bf16[1,256,2048]{2,1,0:T(8,128)(2,1)} %refs_4_.7), channel_id=1, source_target_pairs={{0,1},{1,0},{2,3},{3,2},{4,5},{5,4},{6,7},{7,6},{8,9},{9,8},{10,11... | collective-permute-start | bytes 3145736 | tf_op jit(solution)/shard_map/ppermute | solution.py:440
  52.3 10.0 %collective-permute-start.21 = (bf16[144,1024]{1,0:T(8,128)(2,1)S(1)}, bf16[144,1024]{1,0:T(8,128)(2,1)S(1)}, u32[]{:S(2)}, u32[]{:S(2)}) collective-permute-start(bf16[144,1024]{1,0:T(8,128)(2,1)S(1)} %get-tuple-element.73), channel_id=1, source_target_pairs={{0,8},{8,0},{16,24},{24,16},{1,9},{9,1},{17,25},{25,17},{2,10},{10... | collective-permute-start | bytes 884744 | tf_op jit(solution)/shard_map/ppermute | solution.py:440
  55.2 10.8 %collective-permute-start.22 = (bf16[144,1024]{1,0:T(8,128)(2,1)S(1)}, bf16[144,1024]{1,0:T(8,128)(2,1)S(1)}, u32[]{:S(2)}, u32[]{:S(2)}) collective-permute-start(bf16[144,1024]{1,0:T(8,128)(2,1)S(1)} %get-tuple-element.74), channel_id=1, source_target_pairs={{0,16},{8,24},{16,0},{24,8},{1,17},{9,25},{17,1},{25,9},{2,18},{10... | collective-permute-start | bytes 884744 | tf_op jit(solution)/shard_map/ppermute | solution.py:440
  71.2 8.0 %collective-permute-start.19 = (bf16[144,1152]{1,0:T(8,128)(2,1)S(1)}, bf16[144,1152]{1,0:T(8,128)(2,1)S(1)}, u32[]{:S(2)}, u32[]{:S(2)}) collective-permute-start(bf16[144,1152]{1,0:T(8,128)(2,1)S(1)} %get-tuple-element.71), channel_id=1, source_target_pairs={{0,8},{8,0},{16,24},{24,16},{1,9},{9,1},{17,25},{25,17},{2,10},{10... | collective-permute-start | bytes 995336 | tf_op jit(solution)/shard_map/ppermute | solution.py:440
  72.6 9.7 %collective-permute-start.20 = (bf16[144,1152]{1,0:T(8,128)(2,1)S(1)}, bf16[144,1152]{1,0:T(8,128)(2,1)S(1)}, u32[]{:S(2)}, u32[]{:S(2)}) collective-permute-start(bf16[144,1152]{1,0:T(8,128)(2,1)S(1)} %get-tuple-element.72), channel_id=1, source_target_pairs={{0,16},{8,24},{16,0},{24,8},{1,17},{9,25},{17,1},{25,9},{2,18},{10... | collective-permute-start | bytes 995336 | tf_op jit(solution)/shard_map/ppermute | solution.py:440
  79.1 11.6 %collective-permute-start.23 = (bf16[144,1024]{1,0:T(8,128)(2,1)S(1)}, bf16[144,1024]{1,0:T(8,128)(2,1)S(1)}, u32[]{:S(2)}, u32[]{:S(2)}) collective-permute-start(bf16[144,1024]{1,0:T(8,128)(2,1)S(1)} %get-tuple-element.75), channel_id=1, source_target_pairs={{0,8},{8,0},{16,24},{24,16},{1,9},{9,1},{17,25},{25,17},{2,10},{10... | collective-permute-start | bytes 884744 | tf_op jit(solution)/shard_map/ppermute | solution.py:440
  82.3 26.3 %collective-permute-start.24 = (bf16[144,1024]{1,0:T(8,128)(2,1)S(1)}, bf16[144,1024]{1,0:T(8,128)(2,1)S(1)}, u32[]{:S(2)}, u32[]{:S(2)}) collective-permute-start(bf16[144,1024]{1,0:T(8,128)(2,1)S(1)} %get-tuple-element.76), channel_id=1, source_target_pairs={{0,16},{8,24},{16,0},{24,8},{1,17},{9,25},{17,1},{25,9},{2,18},{10... | collective-permute-start | bytes 884744 | tf_op jit(solution)/shard_map/ppermute | solution.py:440
  84.3 32.1 %collective-permute-start.27 = (bf16[144,1152]{1,0:T(8,128)(2,1)S(1)}, bf16[144,1152]{1,0:T(8,128)(2,1)S(1)}, u32[]{:S(2)}, u32[]{:S(2)}) collective-permute-start(bf16[144,1152]{1,0:T(8,128)(2,1)S(1)} %get-tuple-element.79), channel_id=1, source_target_pairs={{0,24},{8,16},{16,8},{24,0},{1,25},{9,17},{17,9},{25,1},{2,26},{10... | collective-permute-start | bytes 995336 | tf_op jit(solution)/shard_map/ppermute | solution.py:440
  85.5 29.5 %collective-permute-start.28 = (bf16[144,1024]{1,0:T(8,128)(2,1)S(1)}, bf16[144,1024]{1,0:T(8,128)(2,1)S(1)}, u32[]{:S(2)}, u32[]{:S(2)}) collective-permute-start(bf16[144,1024]{1,0:T(8,128)(2,1)S(1)} %get-tuple-element.80), channel_id=1, source_target_pairs={{0,24},{8,16},{16,8},{24,0},{1,25},{9,17},{17,9},{25,1},{2,26},{10... | collective-permute-start | bytes 884744 | tf_op jit(solution)/shard_map/ppermute | solution.py:440
  87.2 30.0 %collective-permute-start.29 = (bf16[144,1024]{1,0:T(8,128)(2,1)S(1)}, bf16[144,1024]{1,0:T(8,128)(2,1)S(1)}, u32[]{:S(2)}, u32[]{:S(2)}) collective-permute-start(bf16[144,1024]{1,0:T(8,128)(2,1)S(1)} %get-tuple-element.81), channel_id=1, source_target_pairs={{0,24},{8,16},{16,8},{24,0},{1,25},{9,17},{17,9},{25,1},{2,26},{10... | collective-permute-start | bytes 884744 | tf_op jit(solution)/shard_map/ppermute | solution.py:440
  112.3 8.3 %collective-permute-start.43 = (bf16[72,512]{1,0:T(8,128)(2,1)S(1)}, bf16[72,512]{1,0:T(8,128)(2,1)S(1)}, u32[]{:S(2)}, u32[]{:S(2)}) collective-permute-start(bf16[72,512]{1,0:T(8,128)(2,1)S(1)} %get-tuple-element.105), channel_id=1, source_target_pairs={{0,2},{1,3},{2,0},{3,1},{4,6},{5,7},{6,4},{7,5},{8,10},{9,11},{10,... | collective-permute-start | bytes 221192 | tf_op jit(solution)/shard_map/ppermute | solution.py:440
  112.3 10.9 %collective-permute-start.44 = (bf16[72,512]{1,0:T(8,128)(2,1)S(1)}, bf16[72,512]{1,0:T(8,128)(2,1)S(1)}, u32[]{:S(2)}, u32[]{:S(2)}) collective-permute-start(bf16[72,512]{1,0:T(8,128)(2,1)S(1)} %get-tuple-element.106), channel_id=1, source_target_pairs={{0,4},{1,5},{2,6},{3,7},{4,0},{5,1},{6,2},{7,3},{8,12},{9,13},{10,... | collective-permute-start | bytes 221192 | tf_op jit(solution)/shard_map/ppermute | solution.py:440
  114.9 14.3 %collective-permute-start.26 = (bf16[144,768]{1,0:T(8,128)(2,1)S(1)}, bf16[144,768]{1,0:T(8,128)(2,1)S(1)}, u32[]{:S(2)}, u32[]{:S(2)}) collective-permute-start(bf16[144,768]{1,0:T(8,128)(2,1)S(1)} %get-tuple-element.78), channel_id=1, source_target_pairs={{0,16},{8,24},{16,0},{24,8},{1,17},{9,25},{17,1},{25,9},{2,18},{10... | collective-permute-start | bytes 663560 | tf_op jit(solution)/shard_map/ppermute | solution.py:440
  116.3 14.4 %collective-permute-start.25 = (bf16[144,768]{1,0:T(8,128)(2,1)S(1)}, bf16[144,768]{1,0:T(8,128)(2,1)S(1)}, u32[]{:S(2)}, u32[]{:S(2)}) collective-permute-start(bf16[144,768]{1,0:T(8,128)(2,1)S(1)} %get-tuple-element.77.refs_15_), channel_id=1, source_target_pairs={{0,8},{8,0},{16,24},{24,16},{1,9},{9,1},{17,25},{25,17},{2,10},{10... | collective-permute-start | bytes 663560 | tf_op jit(solution)/shard_map/ppermute | solution.py:440
  119.2 11.5 %collective-permute-start.30 = (bf16[144,768]{1,0:T(8,128)(2,1)S(1)}, bf16[144,768]{1,0:T(8,128)(2,1)S(1)}, u32[]{:S(2)}, u32[]{:S(2)}) collective-permute-start(bf16[144,768]{1,0:T(8,128)(2,1)S(1)} %get-tuple-element.86), channel_id=1, source_target_pairs={{0,24},{8,16},{16,8},{24,0},{1,25},{9,17},{17,9},{25,1},{2,26},{10... | collective-permute-start | bytes 663560 | tf_op jit(solution)/shard_map/ppermute | solution.py:440
  126.8 11.2 %collective-permute-start.34 = (bf16[144,768]{1,0:T(8,128)(2,1)S(1)}, bf16[144,768]{1,0:T(8,128)(2,1)S(1)}, u32[]{:S(2)}, u32[]{:S(2)}) collective-permute-start(bf16[144,768]{1,0:T(8,128)(2,1)S(1)} %get-tuple-element.92), channel_id=1, source_target_pairs={{0,8},{8,0},{16,24},{24,16},{1,9},{9,1},{17,25},{25,17},{2,10},{10... | collective-permute-start | bytes 663560 | tf_op jit(solution)/shard_map/ppermute | solution.py:440
  127.6 12.2 %collective-permute-start.35 = (bf16[144,768]{1,0:T(8,128)(2,1)S(1)}, bf16[144,768]{1,0:T(8,128)(2,1)S(1)}, u32[]{:S(2)}, u32[]{:S(2)}) collective-permute-start(bf16[144,768]{1,0:T(8,128)(2,1)S(1)} %get-tuple-element.93), channel_id=1, source_target_pairs={{0,16},{8,24},{16,0},{24,8},{1,17},{9,25},{17,1},{25,9},{2,18},{10... | collective-permute-start | bytes 663560 | tf_op jit(solution)/shard_map/ppermute | solution.py:440
  129.2 12.0 %collective-permute-start.36 = (bf16[144,768]{1,0:T(8,128)(2,1)S(1)}, bf16[144,768]{1,0:T(8,128)(2,1)S(1)}, u32[]{:S(2)}, u32[]{:S(2)}) collective-permute-start(bf16[144,768]{1,0:T(8,128)(2,1)S(1)} %get-tuple-element.94), channel_id=1, source_target_pairs={{0,24},{8,16},{16,8},{24,0},{1,25},{9,17},{17,9},{25,1},{2,26},{10... | collective-permute-start | bytes 663560 | tf_op jit(solution)/shard_map/ppermute | solution.py:440
  137.5 10.1 %collective-permute-start.31 = (bf16[64,768]{1,0:T(8,128)(2,1)S(1)}, bf16[64,768]{1,0:T(8,128)(2,1)S(1)}, u32[]{:S(2)}, u32[]{:S(2)}) collective-permute-start(bf16[64,768]{1,0:T(8,128)(2,1)S(1)} %get-tuple-element.88), channel_id=1, source_target_pairs={{0,2},{1,3},{2,0},{3,1},{4,6},{5,7},{6,4},{7,5},{8,10},{9,11},{10,... | collective-permute-start | bytes 294920 | tf_op jit(solution)/shard_map/ppermute | solution.py:440
  138.1 8.2 %collective-permute-start.47 = (bf16[36,512]{1,0:T(8,128)(2,1)S(1)}, bf16[36,512]{1,0:T(8,128)(2,1)S(1)}, u32[]{:S(2)}, u32[]{:S(2)}) collective-permute-start(bf16[36,512]{1,0:T(8,128)(2,1)S(1)} %get-tuple-element.109), channel_id=1, source_target_pairs={{0,16},{8,24},{16,0},{24,8},{1,17},{9,25},{17,1},{25,9},{2,18},{10... | collective-permute-start | bytes 110600 | tf_op jit(solution)/shard_map/ppermute | solution.py:440
  141.3 9.6 %collective-permute-start.32 = (bf16[64,768]{1,0:T(8,128)(2,1)S(1)}, bf16[64,768]{1,0:T(8,128)(2,1)S(1)}, u32[]{:S(2)}, u32[]{:S(2)}) collective-permute-start(bf16[64,768]{1,0:T(8,128)(2,1)S(1)} %get-tuple-element.89), channel_id=1, source_target_pairs={{0,4},{1,5},{2,6},{3,7},{4,0},{5,1},{6,2},{7,3},{8,12},{9,13},{10,... | collective-permute-start | bytes 294920 | tf_op jit(solution)/shard_map/ppermute | solution.py:440
  143.2 7.7 %collective-permute-start.33 = (bf16[64,768]{1,0:T(8,128)(2,1)S(1)}, bf16[64,768]{1,0:T(8,128)(2,1)S(1)}, u32[]{:S(2)}, u32[]{:S(2)}) collective-permute-start(bf16[64,768]{1,0:T(8,128)(2,1)S(1)} %get-tuple-element.90), channel_id=1, source_target_pairs={{0,6},{1,7},{2,4},{3,5},{4,2},{5,3},{6,0},{7,1},{8,14},{9,15},{10,... | collective-permute-start | bytes 294920 | tf_op jit(solution)/shard_map/ppermute | solution.py:440
  146.3 8.3 %collective-permute-start.38 = (bf16[64,768]{1,0:T(8,128)(2,1)S(1)}, bf16[64,768]{1,0:T(8,128)(2,1)S(1)}, u32[]{:S(2)}, u32[]{:S(2)}) collective-permute-start(bf16[64,768]{1,0:T(8,128)(2,1)S(1)} %get-tuple-element.97), channel_id=1, source_target_pairs={{0,4},{1,5},{2,6},{3,7},{4,0},{5,1},{6,2},{7,3},{8,12},{9,13},{10,... | collective-permute-start | bytes 294920 | tf_op jit(solution)/shard_map/ppermute | solution.py:440
  (28 other events, 456.8 us)

commit v3 on v2

--- a/solution.py
+++ b/solution.py
@@ -370,13 +370,20 @@
         out[...] = total[i * cap : (i + 1) * cap].astype(bf16)
 
 
-def finish_kernel(sp, tokens, cap, table, middle, *refs):
-    rows, out = refs[:sp], refs[sp]
-    width = out.shape[1]
-    total = middle[:, middle.shape[1] - width :]
+def finish_kernel(sp, tokens, cap, chunks, table, middle, *refs):
+    rows, owns, far, out = refs[:sp], refs[sp : sp + chunks], refs[sp + chunks : -1], refs[-1]
+    each = len(far) // chunks
+    chunk = owns[0].shape[1]
+    for j in range(chunks):
+        cols = slice(j * chunk, (j + 1) * chunk)
+        total = middle[:, cols] + owns[j][...]
+        for part in far[j * each : (j + 1) * each]:
+            total = total + part[...].astype(f32)
+        out[:, cols] = total.astype(bf16)
+    total = middle[:, chunks * chunk :]
     for k in range(sp):
         total = total + dot(table[k, :tokens, :cap], rows[k][...])
-    out[...] = total.astype(bf16)
+    out[:, chunks * chunk :] = total.astype(bf16)
 
 
 def combine_kernel(sources, tokens, place, chunk, table, *refs):
@@ -561,7 +568,7 @@
             )
             for k, v in zip(members, sums):
                 summed[k] = swap_sp(v, k) if k else v
-    finished = []
+    owns, far = [], []
     for j in range(COL_CHUNKS):
         back = [v[min(j, len(v) - 1)] for v in served]
         own, *rest = call(
@@ -570,18 +577,13 @@
             (shape((tokens, chunk), f32),) + tuple([shape((tokens, chunk), bf16)] * (groups - 1)),
             flops=2 * all_tokens * sp * slots * chunk,
         )
-        total = middle[:, j * chunk : (j + 1) * chunk] + own
-        for k in range(1, groups):
-            total = total + swap_z(rest[k - 1], k).astype(f32)
-        finished.append(total.astype(bf16))
-    finished.append(
-        call(
-            functools.partial(finish_kernel, sp, tokens, cap),
-            [table, middle] + summed,
-            shape((tokens, apart), bf16),
-        )
-    )
-    return jnp.concatenate(finished, axis=1)
+        owns.append(own)
+        far += [swap_z(rest[k - 1], k) for k in range(1, groups)]
+    return call(
+        functools.partial(finish_kernel, sp, tokens, cap, COL_CHUNKS),
+        [table, middle] + summed + owns + far,
+        shape((tokens, width), bf16),
+    )
 
 
 def expert_parts(sp):

time: 156 us -> 159 us (1.019)
  waiting for transfers between devices: 62.9 us -> 65.7 us
    ppermute x49, waiting for transfers between devices: 62.9 us -> 65.7 us  [swap(): return lax.ppermute(v, axis, [(i, i ^ k) for i in range(size)])]
  transfers between devices with their start and end apart: 49 -> 49, of which waited for: 18 -> 18; matrix products, arithmetic and copies ran while one was open for 0% -> 0% of each run, Pallas kernels for 9% -> 8%
where the time goes in v3:
time: 159 us
  starting transfers between devices  70.3 us (44%)
  waiting for transfers between devices  65.7 us (41%)
  Pallas kernels  18.3 us (12%)
  local copies, waits for them, and re-layouts  3.95 us (2%)
    ppermute x49, starting transfers between devices, swap(): return lax.ppermute(v, axis, [(i, i ^ k) for i in range(size)])  70.3 us
    ppermute x49, waiting for transfers between devices, swap(): return lax.ppermute(v, axis, [(i, i ^ k) for i in range(size)])  65.7 us
    pallas_call x13, Pallas kernels, call(): pl.pallas_call(kernel, out_shape=outs, in_specs=[VM] * count + [ANY] * le...  18.3 us
    unnamed x22, local copies, waits for them, and re-layouts  3.95 us
  transfers between devices with their start and end apart: 49, of which 18 were waited for; matrix products, arithmetic and copies ran while one was open for 0% of the time, Pallas kernels for 8%

profile of v3, /device:TPU:0, one launch (start us, length us, event | category | flops | bytes accessed | tf_op | source)
XLA Modules:
  0.0 158.5 jit_solution(145749910186978931)
XLA Ops:
  0.0 3.9 %shard_map.217 = (bf16[1280,128]{1,0:T(8,128)(2,1)}, bf16[6,512,128]{2,1,0:T(8,128)(2,1)}, bf16[64,1152]{1,0:T(8,128)(2,1)}, bf16[64,1024]{1,0:T(8,128)(2,1)}) custom-call(bf16[512,512]{1,0:T(8,128)(2,1)} %refs_0_.4, bf16[32,512]{1,0:T(8,128)(2,1)} %bitcast.14, f32[1,512]{1,0:T(1,128)} %bitcast.15, bf16[512,128]{1,0:T(8,128)(2,1)} %refs_3_.4, ...), custom_call_target="tpu_custom_call" | custom-call | flops 285212672 | bytes 3663616 | tf_op jit(solution)/shard_map/pallas_call | solution.py:412
  3.9 4.0 %collective-permute-start.11 = (bf16[1280,128]{1,0:T(8,128)(2,1)}, bf16[1280,128]{1,0:T(8,128)(2,1)S(1)}, u32[]{:S(2)}, u32[]{:S(2)}) collective-permute-start(bf16[1280,128]{1,0:T(8,128)(2,1)} %get-tuple-element.64.refs_1_), channel_id=1, source_target_pairs={{0,24},{8,16},{16,8},{24,0},{1,25},{9,17},{17,9},{25,1},{2,26},{10... | collective-permute-start | bytes 983048 | tf_op jit(solution)/shard_map/ppermute | solution.py:447
  8.6 4.0 %collective-permute-start.8 = (bf16[64,1024]{1,0:T(8,128)(2,1)}, bf16[64,1024]{1,0:T(8,128)(2,1)S(1)}, u32[]{:S(2)}, u32[]{:S(2)}) collective-permute-start(bf16[64,1024]{1,0:T(8,128)(2,1)} %get-tuple-element.61.refs_1_), channel_id=1, source_target_pairs={{0,6},{1,7},{2,4},{3,5},{4,2},{5,3},{6,0},{7,1},{8,14},{9,15},{10,... | collective-permute-start | bytes 393224 | tf_op jit(solution)/shard_map/ppermute | solution.py:447
  12.6 4.4 %collective-permute-done.8.refs_4_ = bf16[64,1024]{1,0:T(8,128)(2,1)S(1)} collective-permute-done((bf16[64,1024]{1,0:T(8,128)(2,1)}, bf16[64,1024]{1,0:T(8,128)(2,1)S(1)}, u32[]{:S(2)}, u32[]{:S(2)}) %collective-permute-start.8) | collective-permute-done | bytes 131104 | tf_op jit(solution)/shard_map/ppermute | solution.py:447
  16.9 3.5 %collective-permute-start.2 = (bf16[64,1152]{1,0:T(8,128)(2,1)}, bf16[64,1152]{1,0:T(8,128)(2,1)S(1)}, u32[]{:S(2)}, u32[]{:S(2)}) collective-permute-start(bf16[64,1152]{1,0:T(8,128)(2,1)} %get-tuple-element.58.refs_0_), channel_id=1, source_target_pairs={{0,6},{1,7},{2,4},{3,5},{4,2},{5,3},{6,0},{7,1},{8,14},{9,15},{10,... | collective-permute-start | bytes 442376 | tf_op jit(solution)/shard_map/ppermute | solution.py:447
  20.5 6.6 %collective-permute-done.7.refs_3_ = bf16[64,1024]{1,0:T(8,128)(2,1)S(1)} collective-permute-done((bf16[64,1024]{1,0:T(8,128)(2,1)}, bf16[64,1024]{1,0:T(8,128)(2,1)S(1)}, u32[]{:S(2)}, u32[]{:S(2)}) %collective-permute-start.7) | collective-permute-done | bytes 131104 | tf_op jit(solution)/shard_map/ppermute | solution.py:447
  27.5 4.9 %collective-permute-done.6.refs_2_ = bf16[64,1024]{1,0:T(8,128)(2,1)S(1)} collective-permute-done((bf16[64,1024]{1,0:T(8,128)(2,1)}, bf16[64,1024]{1,0:T(8,128)(2,1)S(1)}, u32[]{:S(2)}, u32[]{:S(2)}) %collective-permute-start.6) | collective-permute-done | bytes 131104 | tf_op jit(solution)/shard_map/ppermute | solution.py:447
  32.4 3.7 %collective-permute-start.1 = (bf16[64,1152]{1,0:T(8,128)(2,1)}, bf16[64,1152]{1,0:T(8,128)(2,1)S(1)}, u32[]{:S(2)}, u32[]{:S(2)}) collective-permute-start(bf16[64,1152]{1,0:T(8,128)(2,1)} %get-tuple-element.58.refs_0_), channel_id=1, source_target_pairs={{0,4},{1,5},{2,6},{3,7},{4,0},{5,1},{6,2},{7,3},{8,12},{9,13},{10,... | collective-permute-start | bytes 442376 | tf_op jit(solution)/shard_map/ppermute | solution.py:447
  36.1 2.5 %collective-permute-start = (bf16[64,1152]{1,0:T(8,128)(2,1)}, bf16[64,1152]{1,0:T(8,128)(2,1)S(1)}, u32[]{:S(2)}, u32[]{:S(2)}) collective-permute-start(bf16[64,1152]{1,0:T(8,128)(2,1)} %get-tuple-element.58.refs_0_), channel_id=1, source_target_pairs={{0,2},{1,3},{2,0},{3,1},{4,6},{5,7},{6,4},{7,5},{8,10},{9,11},{10,... | collective-permute-start | bytes 442376 | tf_op jit(solution)/shard_map/ppermute | solution.py:447
  47.6 2.6 %collective-permute-done.17.refs_8_ = bf16[256,128]{1,0:T(8,128)(2,1)S(1)} collective-permute-done((bf16[256,128]{1,0:T(8,128)(2,1)S(1)}, bf16[256,128]{1,0:T(8,128)(2,1)S(1)}, u32[]{:S(2)}, u32[]{:S(2)}) %collective-permute-start.17) | collective-permute-done | bytes 65568 | tf_op jit(solution)/shard_map/ppermute | solution.py:447
  52.3 2.9 %collective-permute-start.24 = (bf16[144,1024]{1,0:T(8,128)(2,1)S(1)}, bf16[144,1024]{1,0:T(8,128)(2,1)S(1)}, u32[]{:S(2)}, u32[]{:S(2)}) collective-permute-start(bf16[144,1024]{1,0:T(8,128)(2,1)S(1)} %get-tuple-element.79), channel_id=1, source_target_pairs={{0,8},{8,0},{16,24},{24,16},{1,9},{9,1},{17,25},{25,17},{2,10},{10... | collective-permute-start | bytes 884744 | tf_op jit(solution)/shard_map/ppermute | solution.py:447
  55.2 4.0 %collective-permute-start.25 = (bf16[144,1024]{1,0:T(8,128)(2,1)S(1)}, bf16[144,1024]{1,0:T(8,128)(2,1)S(1)}, u32[]{:S(2)}, u32[]{:S(2)}) collective-permute-start(bf16[144,1024]{1,0:T(8,128)(2,1)S(1)} %get-tuple-element.80), channel_id=1, source_target_pairs={{0,16},{8,24},{16,0},{24,8},{1,17},{9,25},{17,1},{25,9},{2,18},{10... | collective-permute-start | bytes 884744 | tf_op jit(solution)/shard_map/ppermute | solution.py:447
  59.1 3.2 %collective-permute-done.24.refs_10_ = bf16[144,1024]{1,0:T(8,128)(2,1)S(1)} collective-permute-done((bf16[144,1024]{1,0:T(8,128)(2,1)S(1)}, bf16[144,1024]{1,0:T(8,128)(2,1)S(1)}, u32[]{:S(2)}, u32[]{:S(2)}) %collective-permute-start.24) | collective-permute-done | bytes 294944 | tf_op jit(solution)/shard_map/ppermute | solution.py:447
  63.0 3.0 %collective-permute-done.25.refs_11_ = bf16[144,1024]{1,0:T(8,128)(2,1)S(1)} collective-permute-done((bf16[144,1024]{1,0:T(8,128)(2,1)S(1)}, bf16[144,1024]{1,0:T(8,128)(2,1)S(1)}, u32[]{:S(2)}, u32[]{:S(2)}) %collective-permute-start.25) | collective-permute-done | bytes 294944 | tf_op jit(solution)/shard_map/ppermute | solution.py:447
  66.0 2.4 %collective-permute-done.18.refs_9_ = bf16[256,128]{1,0:T(8,128)(2,1)S(1)} collective-permute-done((bf16[256,128]{1,0:T(8,128)(2,1)S(1)}, bf16[256,128]{1,0:T(8,128)(2,1)S(1)}, u32[]{:S(2)}, u32[]{:S(2)}) %collective-permute-start.18) | collective-permute-done | bytes 65568 | tf_op jit(solution)/shard_map/ppermute | solution.py:447
  68.4 2.8 %collective-permute-done.16.refs_7_ = bf16[256,128]{1,0:T(8,128)(2,1)S(1)} collective-permute-done((bf16[256,128]{1,0:T(8,128)(2,1)S(1)}, bf16[256,128]{1,0:T(8,128)(2,1)S(1)}, u32[]{:S(2)}, u32[]{:S(2)}) %collective-permute-start.16) | collective-permute-done | bytes 65568 | tf_op jit(solution)/shard_map/ppermute | solution.py:447
  72.6 4.5 %collective-permute-start.23 = (bf16[144,1152]{1,0:T(8,128)(2,1)S(1)}, bf16[144,1152]{1,0:T(8,128)(2,1)S(1)}, u32[]{:S(2)}, u32[]{:S(2)}) collective-permute-start(bf16[144,1152]{1,0:T(8,128)(2,1)S(1)} %get-tuple-element.78), channel_id=1, source_target_pairs={{0,16},{8,24},{16,0},{24,8},{1,17},{9,25},{17,1},{25,9},{2,18},{10... | collective-permute-start | bytes 995336 | tf_op jit(solution)/shard_map/ppermute | solution.py:447
  80.1 2.3 %collective-permute-done.23.refs_9_ = bf16[144,1152]{1,0:T(8,128)(2,1)S(1)} collective-permute-done((bf16[144,1152]{1,0:T(8,128)(2,1)S(1)}, bf16[144,1152]{1,0:T(8,128)(2,1)S(1)}, u32[]{:S(2)}, u32[]{:S(2)}) %collective-permute-start.23) | collective-permute-done | bytes 331808 | tf_op jit(solution)/shard_map/ppermute | solution.py:447
  88.4 2.4 %shard_map.222 = (bf16[144,768]{1,0:T(8,128)(2,1)S(1)}, bf16[144,768]{1,0:T(8,128)(2,1)S(1)}, bf16[36,512]{1,0:T(8,128)(2,1)S(1)}, bf16[36,512]{1,0:T(8,128)(2,1...) custom-call(bf16[1024,2048]{1,0:T(8,128)(2,1)S(1)} %copy-done, ...), custom_call_target="tpu_custom_call" | custom-call | flops 1509949440 | bytes 12922880 | tf_op jit(solution)/shard_map/pallas_call | solution.py:412
  90.8 17.9 %collective-permute-done.27.refs_13_ = bf16[144,1024]{1,0:T(8,128)(2,1)S(1)} collective-permute-done((bf16[144,1024]{1,0:T(8,128)(2,1)S(1)}, bf16[144,1024]{1,0:T(8,128)(2,1)S(1)}, u32[]{:S(2)}, u32[]{:S(2)}) %collective-permute-start.27) | collective-permute-done | bytes 294944 | tf_op jit(solution)/shard_map/ppermute | solution.py:447
  108.6 3.6 %shard_map.223 = (bf16[144,768]{1,0:T(8,128)(2,1)S(1)}, bf16[144,768]{1,0:T(8,128)(2,1)S(1)}, bf16[144,768]{1,0:T(8,128)(2,1)S(1)}, bf16[144,768]{1,0:T(8,128)(2...) custom-call(bf16[1024,2048]{1,0:T(8,128)(2,1)S(1)} %copy-done, ...), custom_call_target="tpu_custom_call" | custom-call | flops 3019898880 | bytes 13516800 | tf_op jit(solution)/shard_map/pallas_call | solution.py:412
  112.3 2.6 %collective-permute-start.32 = (bf16[72,512]{1,0:T(8,128)(2,1)S(1)}, bf16[72,512]{1,0:T(8,128)(2,1)S(1)}, u32[]{:S(2)}, u32[]{:S(2)}) collective-permute-start(bf16[72,512]{1,0:T(8,128)(2,1)S(1)} %get-tuple-element.92), channel_id=1, source_target_pairs={{0,4},{1,5},{2,6},{3,7},{4,0},{5,1},{6,2},{7,3},{8,12},{9,13},{10,... | collective-permute-start | bytes 221192 | tf_op jit(solution)/shard_map/ppermute | solution.py:447
  115.0 2.2 %collective-permute-start.41 = (bf16[144,768]{1,0:T(8,128)(2,1)S(1)}, bf16[144,768]{1,0:T(8,128)(2,1)S(1)}, u32[]{:S(2)}, u32[]{:S(2)}) collective-permute-start(bf16[144,768]{1,0:T(8,128)(2,1)S(1)} %get-tuple-element.102), channel_id=1, source_target_pairs={{0,16},{8,24},{16,0},{24,8},{1,17},{9,25},{17,1},{25,9},{2,18},{10... | collective-permute-start | bytes 663560 | tf_op jit(solution)/shard_map/ppermute | solution.py:447
  120.6 2.6 %collective-permute-start.33 = (bf16[72,512]{1,0:T(8,128)(2,1)S(1)}, bf16[72,512]{1,0:T(8,128)(2,1)S(1)}, u32[]{:S(2)}, u32[]{:S(2)}) collective-permute-start(bf16[72,512]{1,0:T(8,128)(2,1)S(1)} %get-tuple-element.93), channel_id=1, source_target_pairs={{0,6},{1,7},{2,4},{3,5},{4,2},{5,3},{6,0},{7,1},{8,14},{9,15},{10,... | collective-permute-start | bytes 221192 | tf_op jit(solution)/shard_map/ppermute | solution.py:447
  123.2 3.6 %collective-permute-done.33.refs_3_ = bf16[72,512]{1,0:T(8,128)(2,1)S(1)} collective-permute-done((bf16[72,512]{1,0:T(8,128)(2,1)S(1)}, bf16[72,512]{1,0:T(8,128)(2,1)S(1)}, u32[]{:S(2)}, u32[]{:S(2)}) %collective-permute-start.33) | collective-permute-done | bytes 73760 | tf_op jit(solution)/shard_map/ppermute | solution.py:447
  128.1 2.3 %collective-permute-start.39 = (bf16[144,768]{1,0:T(8,128)(2,1)S(1)}, bf16[144,768]{1,0:T(8,128)(2,1)S(1)}, u32[]{:S(2)}, u32[]{:S(2)}) collective-permute-start(bf16[144,768]{1,0:T(8,128)(2,1)S(1)} %get-tuple-element.98), channel_id=1, source_target_pairs={{0,24},{8,16},{16,8},{24,0},{1,25},{9,17},{17,9},{25,1},{2,26},{10... | collective-permute-start | bytes 663560 | tf_op jit(solution)/shard_map/ppermute | solution.py:447
  131.4 2.6 %collective-permute-start.30 = (bf16[72,512]{1,0:T(8,128)(2,1)S(1)}, bf16[72,512]{1,0:T(8,128)(2,1)S(1)}, u32[]{:S(2)}, u32[]{:S(2)}) collective-permute-start(bf16[72,512]{1,0:T(8,128)(2,1)S(1)} %get-tuple-element.88), channel_id=1, source_target_pairs={{0,6},{1,7},{2,4},{3,5},{4,2},{5,3},{6,0},{7,1},{8,14},{9,15},{10,... | collective-permute-start | bytes 221192 | tf_op jit(solution)/shard_map/ppermute | solution.py:447
  134.6 2.1 %collective-permute-done.29.refs_2_ = bf16[72,512]{1,0:T(8,128)(2,1)S(1)} collective-permute-done((bf16[72,512]{1,0:T(8,128)(2,1)S(1)}, bf16[72,512]{1,0:T(8,128)(2,1)S(1)}, u32[]{:S(2)}, u32[]{:S(2)}) %collective-permute-start.29) | collective-permute-done | bytes 73760 | tf_op jit(solution)/shard_map/ppermute | solution.py:447
  141.9 2.2 %collective-permute-start.47 = (bf16[64,768]{1,0:T(8,128)(2,1)S(1)}, bf16[64,768]{1,0:T(8,128)(2,1)S(1)}, u32[]{:S(2)}, u32[]{:S(2)}) collective-permute-start(bf16[64,768]{1,0:T(8,128)(2,1)S(1)} %get-tuple-element.109), channel_id=1, source_target_pairs={{0,4},{1,5},{2,6},{3,7},{4,0},{5,1},{6,2},{7,3},{8,12},{9,13},{10,... | collective-permute-start | bytes 294920 | tf_op jit(solution)/shard_map/ppermute | solution.py:447
  146.0 3.1 %collective-permute-start.44 = (bf16[64,768]{1,0:T(8,128)(2,1)S(1)}, bf16[64,768]{1,0:T(8,128)(2,1)S(1)}, u32[]{:S(2)}, u32[]{:S(2)}) collective-permute-start(bf16[64,768]{1,0:T(8,128)(2,1)S(1)} %get-tuple-element.106), channel_id=1, source_target_pairs={{0,4},{1,5},{2,6},{3,7},{4,0},{5,1},{6,2},{7,3},{8,12},{9,13},{10,... | collective-permute-start | bytes 294920 | tf_op jit(solution)/shard_map/ppermute | solution.py:447
  150.4 3.3 %collective-permute-done.47.refs_12_ = bf16[64,768]{1,0:T(8,128)(2,1)S(1)} collective-permute-done((bf16[64,768]{1,0:T(8,128)(2,1)S(1)}, bf16[64,768]{1,0:T(8,128)(2,1)S(1)}, u32[]{:S(2)}, u32[]{:S(2)}) %collective-permute-start.47) | collective-permute-done | bytes 98336 | tf_op jit(solution)/shard_map/ppermute | solution.py:447
  153.8 3.8 %collective-permute-done.44.refs_9_ = bf16[64,768]{1,0:T(8,128)(2,1)S(1)} collective-permute-done((bf16[64,768]{1,0:T(8,128)(2,1)S(1)}, bf16[64,768]{1,0:T(8,128)(2,1)S(1)}, u32[]{:S(2)}, u32[]{:S(2)}) %collective-permute-start.44) | collective-permute-done | bytes 98336 | tf_op jit(solution)/shard_map/ppermute | solution.py:447
  (101 shorter events, 39.1 us)
Async XLA Ops:
  3.9 34.7 %collective-permute-start.11 = (bf16[1280,128]{1,0:T(8,128)(2,1)}, bf16[1280,128]{1,0:T(8,128)(2,1)S(1)}, u32[]{:S(2)}, u32[]{:S(2)}) collective-permute-start(bf16[1280,128]{1,0:T(8,128)(2,1)} %get-tuple-element.64.refs_1_), channel_id=1, source_target_pairs={{0,24},{8,16},{16,8},{24,0},{1,25},{9,17},{17,9},{25,1},{2,26},{10... | collective-permute-start | bytes 983048 | tf_op jit(solution)/shard_map/ppermute | solution.py:447
  7.9 30.7 %collective-permute-start.10 = (bf16[1280,128]{1,0:T(8,128)(2,1)}, bf16[1280,128]{1,0:T(8,128)(2,1)S(1)}, u32[]{:S(2)}, u32[]{:S(2)}) collective-permute-start(bf16[1280,128]{1,0:T(8,128)(2,1)} %get-tuple-element.64.refs_1_), channel_id=1, source_target_pairs={{0,16},{8,24},{16,0},{24,8},{1,17},{9,25},{17,1},{25,9},{2,18},{10... | collective-permute-start | bytes 983048 | tf_op jit(solution)/shard_map/ppermute | solution.py:447
  8.4 30.7 %collective-permute-start.9 = (bf16[1280,128]{1,0:T(8,128)(2,1)}, bf16[1280,128]{1,0:T(8,128)(2,1)S(1)}, u32[]{:S(2)}, u32[]{:S(2)}) collective-permute-start(bf16[1280,128]{1,0:T(8,128)(2,1)} %get-tuple-element.64.refs_1_), channel_id=1, source_target_pairs={{0,8},{8,0},{16,24},{24,16},{1,9},{9,1},{17,25},{25,17},{2,10},{10... | collective-permute-start | bytes 983048 | tf_op jit(solution)/shard_map/ppermute | solution.py:447
  8.6 8.4 %collective-permute-start.8 = (bf16[64,1024]{1,0:T(8,128)(2,1)}, bf16[64,1024]{1,0:T(8,128)(2,1)S(1)}, u32[]{:S(2)}, u32[]{:S(2)}) collective-permute-start(bf16[64,1024]{1,0:T(8,128)(2,1)} %get-tuple-element.61.refs_1_), channel_id=1, source_target_pairs={{0,6},{1,7},{2,4},{3,5},{4,2},{5,3},{6,0},{7,1},{8,14},{9,15},{10,... | collective-permute-start | bytes 393224 | tf_op jit(solution)/shard_map/ppermute | solution.py:447
  12.6 14.5 %collective-permute-start.7 = (bf16[64,1024]{1,0:T(8,128)(2,1)}, bf16[64,1024]{1,0:T(8,128)(2,1)S(1)}, u32[]{:S(2)}, u32[]{:S(2)}) collective-permute-start(bf16[64,1024]{1,0:T(8,128)(2,1)} %get-tuple-element.61.refs_1_), channel_id=1, source_target_pairs={{0,4},{1,5},{2,6},{3,7},{4,0},{5,1},{6,2},{7,3},{8,12},{9,13},{10,... | collective-permute-start | bytes 393224 | tf_op jit(solution)/shard_map/ppermute | solution.py:447
  16.9 19.2 %collective-permute-start.2 = (bf16[64,1152]{1,0:T(8,128)(2,1)}, bf16[64,1152]{1,0:T(8,128)(2,1)S(1)}, u32[]{:S(2)}, u32[]{:S(2)}) collective-permute-start(bf16[64,1152]{1,0:T(8,128)(2,1)} %get-tuple-element.58.refs_0_), channel_id=1, source_target_pairs={{0,6},{1,7},{2,4},{3,5},{4,2},{5,3},{6,0},{7,1},{8,14},{9,15},{10,... | collective-permute-start | bytes 442376 | tf_op jit(solution)/shard_map/ppermute | solution.py:447
  32.4 10.6 %collective-permute-start.1 = (bf16[64,1152]{1,0:T(8,128)(2,1)}, bf16[64,1152]{1,0:T(8,128)(2,1)S(1)}, u32[]{:S(2)}, u32[]{:S(2)}) collective-permute-start(bf16[64,1152]{1,0:T(8,128)(2,1)} %get-tuple-element.58.refs_0_), channel_id=1, source_target_pairs={{0,4},{1,5},{2,6},{3,7},{4,0},{5,1},{6,2},{7,3},{8,12},{9,13},{10,... | collective-permute-start | bytes 442376 | tf_op jit(solution)/shard_map/ppermute | solution.py:447
  38.6 45.6 %collective-permute-start.3 = (bf16[1,2048,256]{2,1,0:T(8,128)(2,1)}, bf16[1,2048,256]{2,1,0:T(8,128)(2,1)S(1)}, u32[]{:S(2)}, u32[]{:S(2)}) collective-permute-start(bf16[1,2048,256]{2,1,0:T(8,128)(2,1)} %refs_2_.5), channel_id=1, source_target_pairs={{0,1},{1,0},{2,3},{3,2},{4,5},{5,4},{6,7},{7,6},{8,9},{9,8},{10,11... | collective-permute-start | bytes 3145736 | tf_op jit(solution)/shard_map/ppermute | solution.py:447
  38.7 46.8 %collective-permute-start.4 = (bf16[1,2048,256]{2,1,0:T(8,128)(2,1)}, bf16[1,2048,256]{2,1,0:T(8,128)(2,1)S(1)}, u32[]{:S(2)}, u32[]{:S(2)}) collective-permute-start(bf16[1,2048,256]{2,1,0:T(8,128)(2,1)} %refs_3_.7), channel_id=1, source_target_pairs={{0,1},{1,0},{2,3},{3,2},{4,5},{5,4},{6,7},{7,6},{8,9},{9,8},{10,11... | collective-permute-start | bytes 3145736 | tf_op jit(solution)/shard_map/ppermute | solution.py:447
  39.2 48.0 %collective-permute-start.5 = (bf16[1,256,2048]{2,1,0:T(8,128)(2,1)}, bf16[1,256,2048]{2,1,0:T(8,128)(2,1)S(1)}, u32[]{:S(2)}, u32[]{:S(2)}) collective-permute-start(bf16[1,256,2048]{2,1,0:T(8,128)(2,1)} %refs_4_.7), channel_id=1, source_target_pairs={{0,1},{1,0},{2,3},{3,2},{4,5},{5,4},{6,7},{7,6},{8,9},{9,8},{10,11... | collective-permute-start | bytes 3145736 | tf_op jit(solution)/shard_map/ppermute | solution.py:447
  52.3 10.0 %collective-permute-start.24 = (bf16[144,1024]{1,0:T(8,128)(2,1)S(1)}, bf16[144,1024]{1,0:T(8,128)(2,1)S(1)}, u32[]{:S(2)}, u32[]{:S(2)}) collective-permute-start(bf16[144,1024]{1,0:T(8,128)(2,1)S(1)} %get-tuple-element.79), channel_id=1, source_target_pairs={{0,8},{8,0},{16,24},{24,16},{1,9},{9,1},{17,25},{25,17},{2,10},{10... | collective-permute-start | bytes 884744 | tf_op jit(solution)/shard_map/ppermute | solution.py:447
  55.2 10.8 %collective-permute-start.25 = (bf16[144,1024]{1,0:T(8,128)(2,1)S(1)}, bf16[144,1024]{1,0:T(8,128)(2,1)S(1)}, u32[]{:S(2)}, u32[]{:S(2)}) collective-permute-start(bf16[144,1024]{1,0:T(8,128)(2,1)S(1)} %get-tuple-element.80), channel_id=1, source_target_pairs={{0,16},{8,24},{16,0},{24,8},{1,17},{9,25},{17,1},{25,9},{2,18},{10... | collective-permute-start | bytes 884744 | tf_op jit(solution)/shard_map/ppermute | solution.py:447
  71.2 8.0 %collective-permute-start.22 = (bf16[144,1152]{1,0:T(8,128)(2,1)S(1)}, bf16[144,1152]{1,0:T(8,128)(2,1)S(1)}, u32[]{:S(2)}, u32[]{:S(2)}) collective-permute-start(bf16[144,1152]{1,0:T(8,128)(2,1)S(1)} %get-tuple-element.77), channel_id=1, source_target_pairs={{0,8},{8,0},{16,24},{24,16},{1,9},{9,1},{17,25},{25,17},{2,10},{10... | collective-permute-start | bytes 995336 | tf_op jit(solution)/shard_map/ppermute | solution.py:447
  72.6 9.7 %collective-permute-start.23 = (bf16[144,1152]{1,0:T(8,128)(2,1)S(1)}, bf16[144,1152]{1,0:T(8,128)(2,1)S(1)}, u32[]{:S(2)}, u32[]{:S(2)}) collective-permute-start(bf16[144,1152]{1,0:T(8,128)(2,1)S(1)} %get-tuple-element.78), channel_id=1, source_target_pairs={{0,16},{8,24},{16,0},{24,8},{1,17},{9,25},{17,1},{25,9},{2,18},{10... | collective-permute-start | bytes 995336 | tf_op jit(solution)/shard_map/ppermute | solution.py:447
  79.1 11.6 %collective-permute-start.26 = (bf16[144,1024]{1,0:T(8,128)(2,1)S(1)}, bf16[144,1024]{1,0:T(8,128)(2,1)S(1)}, u32[]{:S(2)}, u32[]{:S(2)}) collective-permute-start(bf16[144,1024]{1,0:T(8,128)(2,1)S(1)} %get-tuple-element.81), channel_id=1, source_target_pairs={{0,8},{8,0},{16,24},{24,16},{1,9},{9,1},{17,25},{25,17},{2,10},{10... | collective-permute-start | bytes 884744 | tf_op jit(solution)/shard_map/ppermute | solution.py:447
  82.3 26.3 %collective-permute-start.27 = (bf16[144,1024]{1,0:T(8,128)(2,1)S(1)}, bf16[144,1024]{1,0:T(8,128)(2,1)S(1)}, u32[]{:S(2)}, u32[]{:S(2)}) collective-permute-start(bf16[144,1024]{1,0:T(8,128)(2,1)S(1)} %get-tuple-element.82), channel_id=1, source_target_pairs={{0,16},{8,24},{16,0},{24,8},{1,17},{9,25},{17,1},{25,9},{2,18},{10... | collective-permute-start | bytes 884744 | tf_op jit(solution)/shard_map/ppermute | solution.py:447
  84.3 30.7 %collective-permute-start.19 = (bf16[144,1152]{1,0:T(8,128)(2,1)S(1)}, bf16[144,1152]{1,0:T(8,128)(2,1)S(1)}, u32[]{:S(2)}, u32[]{:S(2)}) collective-permute-start(bf16[144,1152]{1,0:T(8,128)(2,1)S(1)} %get-tuple-element.70), channel_id=1, source_target_pairs={{0,24},{8,16},{16,8},{24,0},{1,25},{9,17},{17,9},{25,1},{2,26},{10... | collective-permute-start | bytes 995336 | tf_op jit(solution)/shard_map/ppermute | solution.py:447
  85.5 29.5 %collective-permute-start.20 = (bf16[144,1024]{1,0:T(8,128)(2,1)S(1)}, bf16[144,1024]{1,0:T(8,128)(2,1)S(1)}, u32[]{:S(2)}, u32[]{:S(2)}) collective-permute-start(bf16[144,1024]{1,0:T(8,128)(2,1)S(1)} %get-tuple-element.71), channel_id=1, source_target_pairs={{0,24},{8,16},{16,8},{24,0},{1,25},{9,17},{17,9},{25,1},{2,26},{10... | collective-permute-start | bytes 884744 | tf_op jit(solution)/shard_map/ppermute | solution.py:447
  87.2 30.0 %collective-permute-start.21 = (bf16[144,1024]{1,0:T(8,128)(2,1)S(1)}, bf16[144,1024]{1,0:T(8,128)(2,1)S(1)}, u32[]{:S(2)}, u32[]{:S(2)}) collective-permute-start(bf16[144,1024]{1,0:T(8,128)(2,1)S(1)} %get-tuple-element.72), channel_id=1, source_target_pairs={{0,24},{8,16},{16,8},{24,0},{1,25},{9,17},{17,9},{25,1},{2,26},{10... | collective-permute-start | bytes 884744 | tf_op jit(solution)/shard_map/ppermute | solution.py:447
  112.3 8.3 %collective-permute-start.31 = (bf16[72,512]{1,0:T(8,128)(2,1)S(1)}, bf16[72,512]{1,0:T(8,128)(2,1)S(1)}, u32[]{:S(2)}, u32[]{:S(2)}) collective-permute-start(bf16[72,512]{1,0:T(8,128)(2,1)S(1)} %get-tuple-element.91), channel_id=1, source_target_pairs={{0,2},{1,3},{2,0},{3,1},{4,6},{5,7},{6,4},{7,5},{8,10},{9,11},{10,... | collective-permute-start | bytes 221192 | tf_op jit(solution)/shard_map/ppermute | solution.py:447
  112.3 10.8 %collective-permute-start.32 = (bf16[72,512]{1,0:T(8,128)(2,1)S(1)}, bf16[72,512]{1,0:T(8,128)(2,1)S(1)}, u32[]{:S(2)}, u32[]{:S(2)}) collective-permute-start(bf16[72,512]{1,0:T(8,128)(2,1)S(1)} %get-tuple-element.92), channel_id=1, source_target_pairs={{0,4},{1,5},{2,6},{3,7},{4,0},{5,1},{6,2},{7,3},{8,12},{9,13},{10,... | collective-permute-start | bytes 221192 | tf_op jit(solution)/shard_map/ppermute | solution.py:447
  114.9 15.5 %collective-permute-start.40 = (bf16[144,768]{1,0:T(8,128)(2,1)S(1)}, bf16[144,768]{1,0:T(8,128)(2,1)S(1)}, u32[]{:S(2)}, u32[]{:S(2)}) collective-permute-start(bf16[144,768]{1,0:T(8,128)(2,1)S(1)} %get-tuple-element.101), channel_id=1, source_target_pairs={{0,8},{8,0},{16,24},{24,16},{1,9},{9,1},{17,25},{25,17},{2,10},{10... | collective-permute-start | bytes 663560 | tf_op jit(solution)/shard_map/ppermute | solution.py:447
  115.0 15.7 %collective-permute-start.41 = (bf16[144,768]{1,0:T(8,128)(2,1)S(1)}, bf16[144,768]{1,0:T(8,128)(2,1)S(1)}, u32[]{:S(2)}, u32[]{:S(2)}) collective-permute-start(bf16[144,768]{1,0:T(8,128)(2,1)S(1)} %get-tuple-element.102), channel_id=1, source_target_pairs={{0,16},{8,24},{16,0},{24,8},{1,17},{9,25},{17,1},{25,9},{2,18},{10... | collective-permute-start | bytes 663560 | tf_op jit(solution)/shard_map/ppermute | solution.py:447
  119.2 12.3 %collective-permute-start.42 = (bf16[144,768]{1,0:T(8,128)(2,1)S(1)}, bf16[144,768]{1,0:T(8,128)(2,1)S(1)}, u32[]{:S(2)}, u32[]{:S(2)}) collective-permute-start(bf16[144,768]{1,0:T(8,128)(2,1)S(1)} %get-tuple-element.103), channel_id=1, source_target_pairs={{0,24},{8,16},{16,8},{24,0},{1,25},{9,17},{17,9},{25,1},{2,26},{10... | collective-permute-start | bytes 663560 | tf_op jit(solution)/shard_map/ppermute | solution.py:447
  126.8 12.6 %collective-permute-start.38 = (bf16[144,768]{1,0:T(8,128)(2,1)S(1)}, bf16[144,768]{1,0:T(8,128)(2,1)S(1)}, u32[]{:S(2)}, u32[]{:S(2)}) collective-permute-start(bf16[144,768]{1,0:T(8,128)(2,1)S(1)} %get-tuple-element.97), channel_id=1, source_target_pairs={{0,16},{8,24},{16,0},{24,8},{1,17},{9,25},{17,1},{25,9},{2,18},{10... | collective-permute-start | bytes 663560 | tf_op jit(solution)/shard_map/ppermute | solution.py:447
  128.1 12.2 %collective-permute-start.39 = (bf16[144,768]{1,0:T(8,128)(2,1)S(1)}, bf16[144,768]{1,0:T(8,128)(2,1)S(1)}, u32[]{:S(2)}, u32[]{:S(2)}) collective-permute-start(bf16[144,768]{1,0:T(8,128)(2,1)S(1)} %get-tuple-element.98), channel_id=1, source_target_pairs={{0,24},{8,16},{16,8},{24,0},{1,25},{9,17},{17,9},{25,1},{2,26},{10... | collective-permute-start | bytes 663560 | tf_op jit(solution)/shard_map/ppermute | solution.py:447
  130.4 11.5 %collective-permute-start.37 = (bf16[144,768]{1,0:T(8,128)(2,1)S(1)}, bf16[144,768]{1,0:T(8,128)(2,1)S(1)}, u32[]{:S(2)}, u32[]{:S(2)}) collective-permute-start(bf16[144,768]{1,0:T(8,128)(2,1)S(1)} %get-tuple-element.84.refs_15_), channel_id=1, source_target_pairs={{0,8},{8,0},{16,24},{24,16},{1,9},{9,1},{17,25},{25,17},{2,10},{10... | collective-permute-start | bytes 663560 | tf_op jit(solution)/shard_map/ppermute | solution.py:447
  136.7 12.4 %collective-permute-start.46 = (bf16[64,768]{1,0:T(8,128)(2,1)S(1)}, bf16[64,768]{1,0:T(8,128)(2,1)S(1)}, u32[]{:S(2)}, u32[]{:S(2)}) collective-permute-start(bf16[64,768]{1,0:T(8,128)(2,1)S(1)} %get-tuple-element.108), channel_id=1, source_target_pairs={{0,2},{1,3},{2,0},{3,1},{4,6},{5,7},{6,4},{7,5},{8,10},{9,11},{10,... | collective-permute-start | bytes 294920 | tf_op jit(solution)/shard_map/ppermute | solution.py:447
  141.9 11.9 %collective-permute-start.47 = (bf16[64,768]{1,0:T(8,128)(2,1)S(1)}, bf16[64,768]{1,0:T(8,128)(2,1)S(1)}, u32[]{:S(2)}, u32[]{:S(2)}) collective-permute-start(bf16[64,768]{1,0:T(8,128)(2,1)S(1)} %get-tuple-element.109), channel_id=1, source_target_pairs={{0,4},{1,5},{2,6},{3,7},{4,0},{5,1},{6,2},{7,3},{8,12},{9,13},{10,... | collective-permute-start | bytes 294920 | tf_op jit(solution)/shard_map/ppermute | solution.py:447
  144.6 9.1 %collective-permute-start.48 = (bf16[64,768]{1,0:T(8,128)(2,1)S(1)}, bf16[64,768]{1,0:T(8,128)(2,1)S(1)}, u32[]{:S(2)}, u32[]{:S(2)}) collective-permute-start(bf16[64,768]{1,0:T(8,128)(2,1)S(1)} %get-tuple-element.110), channel_id=1, source_target_pairs={{0,6},{1,7},{2,4},{3,5},{4,2},{5,3},{6,0},{7,1},{8,14},{9,15},{10,... | collective-permute-start | bytes 294920 | tf_op jit(solution)/shard_map/ppermute | solution.py:447
  146.0 11.5 %collective-permute-start.44 = (bf16[64,768]{1,0:T(8,128)(2,1)S(1)}, bf16[64,768]{1,0:T(8,128)(2,1)S(1)}, u32[]{:S(2)}, u32[]{:S(2)}) collective-permute-start(bf16[64,768]{1,0:T(8,128)(2,1)S(1)} %get-tuple-element.106), channel_id=1, source_target_pairs={{0,4},{1,5},{2,6},{3,7},{4,0},{5,1},{6,2},{7,3},{8,12},{9,13},{10,... | collective-permute-start | bytes 294920 | tf_op jit(solution)/shard_map/ppermute | solution.py:447
  149.1 8.5 %collective-permute-start.45 = (bf16[64,768]{1,0:T(8,128)(2,1)S(1)}, bf16[64,768]{1,0:T(8,128)(2,1)S(1)}, u32[]{:S(2)}, u32[]{:S(2)}) collective-permute-start(bf16[64,768]{1,0:T(8,128)(2,1)S(1)} %get-tuple-element.107), channel_id=1, source_target_pairs={{0,6},{1,7},{2,4},{3,5},{4,2},{5,3},{6,0},{7,1},{8,14},{9,15},{10,... | collective-permute-start | bytes 294920 | tf_op jit(solution)/shard_map/ppermute | solution.py:447
  (28 other events, 459.0 us)
